TPU v7x, 32 devices: a whole 2x2x4 slice. The times are simulated.
32 devices in a mesh: ep: 32 (over z, y, x, core).
Axes of the slice: x: 2, y: 2, z: 4, core: 2. Of those that a mesh axis runs over, the one named last changes fastest.
Arguments:
- tokens: bfloat16 [32, 2048], P('ep'), may hold values from -6 to 6
- mixer_gain: float32 [2048], replicated, may hold values from 0.1 to 1.9
- query_weight: bfloat16 [2048, 2048], P(None, 'ep'), may hold values from -0.125 to 0.125
- key_weight: bfloat16 [2048, 2048], P(None, 'ep'), may hold values from -0.125 to 0.125
- value_weight: bfloat16 [2048, 2048], P(None, 'ep'), may hold values from -0.125 to 0.125
- outgate_weight: bfloat16 [2048, 2048], P(None, 'ep'), may hold values from -0.125 to 0.125
- input_weight: bfloat16 [2048, 4], replicated, may hold values from -0.125 to 0.125
- forget_weight: bfloat16 [2048, 4], replicated, may hold values from -0.125 to 0.125
- forget_bias: float32 [4], replicated, may hold values from 0 to 4
- memory_matrix: float32 [32, 4, 512, 512], P('ep'), may hold values from -0.3 to 0.3
- memory_norm: float32 [32, 4, 512], P('ep'), may hold values from -0.3 to 0.3
- memory_max: float32 [32, 4], P('ep'), may hold values from -2 to 2
- mixer_out: bfloat16 [2048, 2048], P(None, 'ep'), may hold values from -0.125 to 0.125
- expert_gain: float32 [2048], replicated, may hold values from 0.1 to 1.9
- expert_gate: bfloat16 [32, 2048, 1024], P('ep'), may hold values from -0.125 to 0.125
- expert_up: bfloat16 [32, 2048, 1024], P('ep'), may hold values from -0.125 to 0.125
- expert_down: bfloat16 [32, 1024, 2048], P('ep'), may hold values from -0.1875 to 0.1875
- route_group: int32 [32], P('ep'), may hold values from 0 to 3
- route_member: int32 [32, 2], P('ep'), may hold values from 0 to 7, as said below
- group_weight: float32 [32], P('ep'), may hold values from 0.25 to 1
- member_weight: float32 [32, 2], P('ep'), may hold values from 0.1 to 1
Outputs:
- layer_out: bfloat16 [32, 2048], P('ep')
- next_matrix: float32 [32, 4, 512, 512], P('ep')
- next_norm: float32 [32, 4, 512], P('ep')
- next_max: float32 [32, 4], P('ep')
Inputs may be any that keep to these rules, and one draw needn't show every extreme that they name: A row's 2 experts, numbered route_group * 8 + route_member, are different members of the one group that route_group names. No expert is named by more than 4 rows in all, and one expert is named by exactly 4 rows.
All inputs are finite; a program needn't handle non-finite values.
Results may differ from a plain program's by a relative error of at most 0.013.
Values may be sent and summed in bfloat16 or wider, within the bound.
No kernel may reach another device: no remote copies, remote signals or barrier semaphores. Data moves between devices by JAX's collectives and lax.ppermute only.
A program may use at most 64 MiB of HBM per device.

v0:
```python
import jax
import jax.numpy as jnp
from jax import lax
from jax.sharding import PartitionSpec as P

GROUPS = 4
CAPACITY = 4


norm_eps = 1e-06


def root_norm(values, gain):
    return values * lax.rsqrt(jnp.mean(values * values, axis=-1, keepdims=True) + norm_eps) * gain


def run_expert(slot_rows, gate_mat, up_mat, down_mat):
    gate_part = jnp.dot(slot_rows, gate_mat, preferred_element_type=jnp.float32)
    up_part = jnp.dot(slot_rows, up_mat, preferred_element_type=jnp.float32)
    hidden = (jax.nn.silu(gate_part) * up_part).astype(jnp.bfloat16)
    return jnp.dot(hidden, down_mat, preferred_element_type=jnp.float32).astype(jnp.bfloat16)


def local(
    tokens,
    mixer_gain,
    query_weight,
    key_weight,
    value_weight,
    outgate_weight,
    input_weight,
    forget_weight,
    forget_bias,
    memory_matrix,
    memory_norm,
    memory_max,
    mixer_out,
    expert_gain,
    expert_gate,
    expert_up,
    expert_down,
    route_group,
    route_member,
    group_weight,
    member_weight,
):
    devices = lax.axis_size("ep")
    local_rows = tokens.shape[0]
    width = tokens.shape[1]
    columns = query_weight.shape[1]
    heads = memory_matrix.shape[1]
    head_dim = memory_matrix.shape[2]
    members = devices * expert_gate.shape[0] // GROUPS
    stacked = jnp.concatenate([query_weight, key_weight, value_weight, outgate_weight], axis=1)
    piece = lax.all_gather(tokens, "ep", axis=0, tiled=True)
    normed = root_norm(piece.astype(jnp.float32), mixer_gain).astype(jnp.bfloat16)
    result = jnp.dot(normed, stacked, preferred_element_type=jnp.float32).astype(jnp.bfloat16)
    result = result.reshape(piece.shape[0], 4, columns)
    parts = lax.all_to_all(result, "ep", split_axis=0, concat_axis=2, tiled=True)
    resid = tokens.astype(jnp.float32)
    own_normed = root_norm(resid, mixer_gain).astype(jnp.bfloat16)
    input_pre = jnp.dot(own_normed, input_weight, preferred_element_type=jnp.float32)
    forget_pre = (
        jnp.dot(own_normed, forget_weight, preferred_element_type=jnp.float32) + forget_bias
    )
    log_forget = jax.nn.log_sigmoid(forget_pre)
    next_max = jnp.maximum(log_forget + memory_max, input_pre)
    keep = jnp.exp(log_forget + memory_max - next_max)
    admit = jnp.exp(input_pre - next_max)
    query_heads = parts[:, 0].astype(jnp.float32).reshape(local_rows, heads, head_dim)
    key_heads = parts[:, 1].astype(jnp.float32).reshape(local_rows, heads, head_dim) * head_dim ** (
        -0.5
    )
    value_heads = parts[:, 2].astype(jnp.float32).reshape(local_rows, heads, head_dim)
    carried = jnp.einsum(
        "shij,shj->shi", memory_matrix, query_heads, precision=lax.Precision.HIGHEST
    )
    score = jnp.sum(key_heads * query_heads, axis=-1)
    numer = keep[..., None] * carried + (admit * score)[..., None] * value_heads
    denom = keep * jnp.sum(memory_norm * query_heads, axis=-1) + admit * score
    head_out = numer / jnp.maximum(jnp.abs(denom), jnp.exp(-next_max))[..., None]
    gated = (
        head_out.reshape(local_rows, width) * jax.nn.sigmoid(parts[:, 3].astype(jnp.float32))
    ).astype(jnp.bfloat16)
    next_matrix = (
        keep[..., None, None] * memory_matrix
        + admit[..., None, None] * value_heads[..., :, None] * key_heads[..., None, :]
    )
    next_norm = keep[..., None] * memory_norm + admit[..., None] * key_heads
    proj_cols = jnp.dot(
        lax.all_gather(gated, "ep", axis=0, tiled=True),
        mixer_out,
        preferred_element_type=jnp.float32,
    ).astype(jnp.bfloat16)
    slot_index = jnp.arange(CAPACITY, dtype=jnp.int32)
    chosen_local = route_group[:, None] * members + route_member
    row_numbers = jnp.arange(local_rows, dtype=jnp.int32)
    local_weight = group_weight[:, None] * member_weight
    projected = lax.all_to_all(proj_cols, "ep", split_axis=0, concat_axis=1, tiled=True)
    middle = (resid + projected.astype(jnp.float32)).astype(jnp.bfloat16)
    expert_in = root_norm(middle.astype(jnp.float32), expert_gain).astype(jnp.bfloat16)
    targets = jnp.arange(devices, dtype=jnp.int32)
    hit = jnp.any(chosen_local[:, :, None] == targets[None, None, :], axis=1)
    outgoing = jnp.where(hit.T[:, :, None], expert_in[None, :, :], jnp.zeros((), jnp.bfloat16))
    present = hit.T.astype(jnp.bfloat16)
    incoming, flags = (
        lax.all_to_all(outgoing, "ep", split_axis=0, concat_axis=0, tiled=True),
        lax.all_to_all(present, "ep", split_axis=0, concat_axis=0, tiled=True),
    )
    flat_rows = incoming.reshape(devices * local_rows, width)
    live = (flags.reshape(devices * local_rows) > 0.5).astype(jnp.int32)
    position = jnp.cumsum(live) - 1
    select = ((position[None, :] == slot_index[:, None]) & (live[None, :] > 0)).astype(jnp.bfloat16)
    slot_rows = jnp.dot(select, flat_rows, preferred_element_type=jnp.float32).astype(jnp.bfloat16)
    finished = run_expert(slot_rows, expert_gate[0], expert_up[0], expert_down[0])
    back_rows = jnp.dot(select.T, finished, preferred_element_type=jnp.float32).astype(jnp.bfloat16)
    returned = lax.all_to_all(
        back_rows.reshape(devices, local_rows, width), "ep", split_axis=0, concat_axis=0, tiled=True
    )
    picked = returned[chosen_local.T, row_numbers[None, :]]
    mixture = jnp.sum(local_weight.T[:, :, None] * picked.astype(jnp.float32), axis=0)
    layer_out = (middle.astype(jnp.float32) + mixture).astype(jnp.bfloat16)
    return (layer_out, next_matrix, next_norm, next_max)


def solution(mesh):
    placed = (
        P("ep", None),
        P(),
        P(None, "ep"),
        P(None, "ep"),
        P(None, "ep"),
        P(None, "ep"),
        P(),
        P(),
        P(),
        P("ep", None, None, None),
        P("ep", None, None),
        P("ep", None),
        P(None, "ep"),
        P(),
        P("ep", None, None),
        P("ep", None, None),
        P("ep", None, None),
        P("ep"),
        P("ep", None),
        P("ep"),
        P("ep", None),
    )
    return jax.shard_map(
        local,
        mesh=mesh,
        in_specs=placed,
        out_specs=(P("ep", None), P("ep", None, None, None), P("ep", None, None), P("ep", None)),
        check_vma=False,
    )
```

profile of v0, /device:TPU:0, one launch (start us, length us, event | category | flops | bytes accessed | tf_op | source)
XLA Modules:
  0.0 155.1 jit_solution(15445792464496646408)
XLA Ops:
  0.7 44.3 %all-gather = bf16[32,1,2048]{2,1,0:T(2,128)(2,1)S(1)} all-gather(bf16[1,1,2048]{2,1,0:T(2,128)(2,1)} %bitcast.134), channel_id=1, replica_groups=mesh['ep'=32] {'ep'}, dimensions={0}, use_global_device_ids=true | all-gather | bytes 135168 | tf_op jit(solution)/shard_map/all_gather | solution.py:55
  45.6 1.6 %convolution_convert_fusion.2 = bf16[32,256]{1,0:T(8,128)(2,1)S(1)} fusion(bf16[2048,64]{0,1:T(8,128)(2,1)} %param.26, bf16[2048,64]{0,1:T(8,128)(2,1)} %param.25, bf16[2048,64]{0,1:T(8,128)(2,1)} %param.24, bf16[2048,64]{0,1:T(8,128)(2,1)} %param.23, f32[32,1,2048]{2,1,0:T(1,128)S(1)} %convert_element_type.241, f32[2048]{0:T(1024)} %param.22, ...), kind=kOutput, calls=%fused_computation.14 | convolution fusion | flops 37953536 | bytes 1335424 | tf_op jit(solution)/shard_map/dot_general | solution.py:57
  47.3 0.7 reshape.614
  48.0 2.5 %all-to-all-start = ((bf16[32,2,128]{2,1,0:T(2,128)(2,1)}), bf16[32,2,128]{2,1,0:T(2,128)(2,1)S(1)}, u32[]{:S(2)}, u32[]{:S(2)}) async-start(bf16[32,2,128]{2,1,0:T(2,128)(2,1)} %reshape.614), calls=%async_computation | async-start | bytes 32768 | tf_op jit(solution)/shard_map/all_to_all | solution.py:59
  53.8 3.9 %all-to-all-done = bf16[32,2,128]{2,1,0:T(2,128)(2,1)S(1)} async-done(((bf16[32,2,128]{2,1,0:T(2,128)(2,1)}), bf16[32,2,128]{2,1,0:T(2,128)(2,1)S(1)}, u32[]{:S(2)}, u32[]{:S(2)}) %all-to-all-start) | async-done | bytes 16416 | tf_op jit(solution)/shard_map/all_to_all | solution.py:59
  58.0 4.1 %fusion.6 = f32[4,1,512]{2,1,0:T(1,128)S(1)} fusion(bf16[4,512,1]{1,2,0:T(2,128)(2,1)S(1)} %bitcast.137, f32[1,4,512,512]{3,2,1,0:T(8,128)} %param.30), kind=kOutput, calls=%fused_computation.7 | convolution fusion | flops 12582912 | bytes 4206592 | tf_op jit(solution)/shard_map/shij,shj->shi/dot_general | solution.py:75
  62.2 0.8 multiply_reduce_fusion.3
  63.1 38.6 %all-gather.1 = bf16[32,1,2048]{2,1,0:T(2,128)(2,1)S(1)} all-gather(bf16[1,1,2048]{2,1,0:T(2,128)(2,1)S(1)} %convert_bitcast_fusion), channel_id=1, replica_groups=mesh['ep'=32] {'ep'}, dimensions={0}, use_global_device_ids=true | all-gather | bytes 135168 | tf_op jit(solution)/shard_map/all_gather | solution.py:91
  102.6 2.5 %all-to-all-start.1 = ((bf16[32,1,64]{2,1,0:T(2,128)(2,1)}), bf16[32,1,64]{2,1,0:T(2,128)(2,1)S(1)}, u32[]{:S(2)}, u32[]{:S(2)}) async-start(bf16[32,1,64]{2,1,0:T(2,128)(2,1)} %copy.45), calls=%async_computation.1 | async-start | bytes 32768 | tf_op jit(solution)/shard_map/all_to_all | solution.py:99
  105.4 0.7 copy.46
  106.1 6.2 %all-to-all-done.1 = bf16[32,1,64]{2,1,0:T(2,128)(2,1)S(1)} async-done(((bf16[32,1,64]{2,1,0:T(2,128)(2,1)}), bf16[32,1,64]{2,1,0:T(2,128)(2,1)S(1)}, u32[]{:S(2)}, u32[]{:S(2)}) %all-to-all-start.1) | async-done | bytes 4128 | tf_op jit(solution)/shard_map/all_to_all | solution.py:99
  112.3 2.6 %all-to-all-start.2 = ((bf16[32,1,1]{2,1,0:T(2,128)(2,1)}), bf16[32,1,1]{2,1,0:T(2,128)(2,1)S(1)}, u32[]{:S(2)}, u32[]{:S(2)}) async-start(bf16[32,1,1]{2,1,0:T(2,128)(2,1)} %copy.46), calls=%async_computation.2 | async-start | bytes 32768 | tf_op jit(solution)/shard_map/all_to_all | solution.py:108
  117.1 1.4 reduce.34
  118.5 0.7 reshape.616
  119.2 2.8 %all-to-all-done.2 = bf16[32,1,1]{2,1,0:T(2,128)(2,1)S(1)} async-done(((bf16[32,1,1]{2,1,0:T(2,128)(2,1)}), bf16[32,1,1]{2,1,0:T(2,128)(2,1)S(1)}, u32[]{:S(2)}, u32[]{:S(2)}) %all-to-all-start.2) | async-done | bytes 96 | tf_op jit(solution)/shard_map/all_to_all | solution.py:108
  122.0 3.1 %all-to-all-start.3 = ((bf16[32,2,1024]{2,1,0:T(2,128)(2,1)}), bf16[32,2,1024]{2,1,0:T(2,128)(2,1)S(1)}, u32[]{:S(2)}, u32[]{:S(2)}) async-start(bf16[32,2,1024]{2,1,0:T(2,128)(2,1)} %reshape.616), calls=%async_computation.3 | async-start | bytes 262144 | tf_op jit(solution)/shard_map/all_to_all | solution.py:107
  125.9 7.4 %all-to-all-done.3 = bf16[32,2,1024]{2,1,0:T(2,128)(2,1)S(1)} async-done(((bf16[32,2,1024]{2,1,0:T(2,128)(2,1)}), bf16[32,2,1024]{2,1,0:T(2,128)(2,1)S(1)}, u32[]{:S(2)}, u32[]{:S(2)}) %all-to-all-start.3) | async-done | bytes 131104 | tf_op jit(solution)/shard_map/all_to_all | solution.py:107
  133.6 2.8 %fusion.4 = f32[4,1024]{1,0:T(4,128)S(1)} fusion(bf16[4,2048]{1,0:T(4,128)(2,1)S(1)} %convolution_convert_fusion.1, bf16[1,2048,1024]{2,1,0:T(8,128)(2,1)} %param.35), kind=kOutput, calls=%fused_computation.5 | convolution fusion | flops 16777216 | bytes 4227072 | tf_op jit(solution)/shard_map/dot_general | solution.py:18
  136.4 4.7 %fusion.9 = bf16[4,2048]{1,0:T(4,128)(2,1)S(1)} fusion(bf16[1,1024,2048]{2,1,0:T(8,128)(2,1)} %param.37, bf16[4,2048]{1,0:T(4,128)(2,1)S(1)} %convolution_convert_fusion.1, bf16[1,2048,1024]{2,1,0:T(8,128)(2,1)} %param.36, f32[4,1024]{1,0:T(4,128)S(1)} %fusion.4), kind=kOutput, calls=%fused_computation.12 | convolution fusion | flops 33587200 | bytes 8437760 | tf_op jit(solution)/shard_map/dot_general | solution.py:21
  141.4 0.7 reduce.35
  142.0 0.7 reshape.618
  142.8 2.6 %all-to-all-start.4 = ((bf16[32,2,1024]{2,1,0:T(2,128)(2,1)}), bf16[32,2,1024]{2,1,0:T(2,128)(2,1)S(1)}, u32[]{:S(2)}, u32[]{:S(2)}) async-start(bf16[32,2,1024]{2,1,0:T(2,128)(2,1)} %reshape.618), calls=%async_computation.4 | async-start | bytes 262144 | tf_op jit(solution)/shard_map/all_to_all | solution.py:117
  145.3 4.7 %multiply_add_fusion = f32[1,4,512,512]{3,2,1,0:T(8,128)} fusion(f32[1,4,512,512]{3,2,1,0:T(8,128)} %param.30, f32[4,512]{1,0:T(4,128)S(1)} %mul.289, f32[4,512]{1,0:T(4,128)S(1)} %get-tuple-element.15, f32[4]{0:T(128)S(1)} %fusion.68), kind=kLoop, calls=%fused_computation.9 | loop fusion | flops 3145728 | bytes 8405008 | tf_op jit(solution)/shard_map/add | solution.py:86
  150.1 3.5 %all-to-all-done.4 = bf16[32,2,1024]{2,1,0:T(2,128)(2,1)S(1)} async-done(((bf16[32,2,1024]{2,1,0:T(2,128)(2,1)}), bf16[32,2,1024]{2,1,0:T(2,128)(2,1)S(1)}, u32[]{:S(2)}, u32[]{:S(2)}) %all-to-all-start.4) | async-done | bytes 131104 | tf_op jit(solution)/shard_map/all_to_all | solution.py:117
  (73 shorter events, 7.7 us)
Async XLA Ops:
  0.6 101.1 %copy-start = (bf16[2048,64]{0,1:T(8,128)(2,1)S(1)}, bf16[2048,64]{0,1:T(8,128)(2,1)}, u32[]{:S(2)}) copy-start(bf16[2048,64]{0,1:T(8,128)(2,1)} %param.33) | copy-start | bytes 786436
  0.6 49.9 %copy-start.1 = (bf16[1,2048]{1,0:T(2,128)(2,1)S(1)}, bf16[1,2048]{1,0:T(2,128)(2,1)}, u32[]{:S(2)}) copy-start(bf16[1,2048]{1,0:T(2,128)(2,1)} %param.21) | copy-start | bytes 12292
  0.7 52.7 %copy-start.2 = (f32[2048]{0:T(1024)S(1)}, f32[2048]{0:T(1024)}, u32[]{:S(2)}) copy-start(f32[2048]{0:T(1024)} %param.22) | copy-start | bytes 24580
  0.7 51.2 %copy-start.8 = (s32[1,2]{1,0:T(1,128)S(1)}, s32[1,2]{1,0:T(1,128)}, u32[]{:S(2)}) copy-start(s32[1,2]{1,0:T(1,128)} %param.39) | copy-start | bytes 28
  0.7 52.7 %copy-start.9 = (f32[1,4]{1,0:T(1,128)S(1)}, f32[1,4]{1,0:T(1,128)}, u32[]{:S(2)}) copy-start(f32[1,4]{1,0:T(1,128)} %param.32) | copy-start | bytes 52
  0.7 52.7 %copy-start.10 = (f32[4]{0:T(128)S(1)}, f32[4]{0:T(128)}, u32[]{:S(2)}) copy-start(f32[4]{0:T(128)} %param.29) | copy-start | bytes 52
  0.7 52.7 %copy-start.6 = (bf16[2048,4]{0,1:T(4,128)(2,1)S(1)}, bf16[2048,4]{0,1:T(4,128)(2,1)}, u32[]{:S(2)}) copy-start(bf16[2048,4]{0,1:T(4,128)(2,1)} %param.28) | copy-start | bytes 49156
  0.7 52.9 %copy-start.7 = (bf16[2048,4]{0,1:T(4,128)(2,1)S(1)}, bf16[2048,4]{0,1:T(4,128)(2,1)}, u32[]{:S(2)}) copy-start(bf16[2048,4]{0,1:T(4,128)(2,1)} %param.27) | copy-start | bytes 49156
  0.7 53.0 %copy-start.11 = (f32[1,2]{1,0:T(1,128)S(1)}, f32[1,2]{1,0:T(1,128)}, u32[]{:S(2)}) copy-start(f32[1,2]{1,0:T(1,128)} %param.41) | copy-start | bytes 28
  45.5 16.6 %copy-start.3 = (f32[1,4,512]{2,1,0:T(4,128)S(1)}, f32[1,4,512]{2,1,0:T(4,128)}, u32[]{:S(2)}) copy-start(f32[1,4,512]{2,1,0:T(4,128)} %param.31) | copy-start | bytes 24580
  45.5 70.8 %copy-start.4 = (f32[2048]{0:T(1024)S(1)}, f32[2048]{0:T(1024)}, u32[]{:S(2)}) copy-start(f32[2048]{0:T(1024)} %param.34) | copy-start | bytes 24580
  48.0 9.7 %all-to-all-start = ((bf16[32,2,128]{2,1,0:T(2,128)(2,1)}), bf16[32,2,128]{2,1,0:T(2,128)(2,1)S(1)}, u32[]{:S(2)}, u32[]{:S(2)}) async-start(bf16[32,2,128]{2,1,0:T(2,128)(2,1)} %reshape.614), calls=%async_computation | async-start | bytes 32768 | tf_op jit(solution)/shard_map/all_to_all | solution.py:59
  53.7 82.7 %copy-start.5 = (f32[1,4]{1,0:T(1,128)}, f32[1,4]{1,0:T(1,128)S(1)}, u32[]{:S(2)}) copy-start(f32[1,4]{1,0:T(1,128)S(1)} %get-tuple-element.11) | copy-start | bytes 52
  102.6 9.7 %all-to-all-start.1 = ((bf16[32,1,64]{2,1,0:T(2,128)(2,1)}), bf16[32,1,64]{2,1,0:T(2,128)(2,1)S(1)}, u32[]{:S(2)}, u32[]{:S(2)}) async-start(bf16[32,1,64]{2,1,0:T(2,128)(2,1)} %copy.45), calls=%async_computation.1 | async-start | bytes 32768 | tf_op jit(solution)/shard_map/all_to_all | solution.py:99
  112.3 9.7 %all-to-all-start.2 = ((bf16[32,1,1]{2,1,0:T(2,128)(2,1)}), bf16[32,1,1]{2,1,0:T(2,128)(2,1)S(1)}, u32[]{:S(2)}, u32[]{:S(2)}) async-start(bf16[32,1,1]{2,1,0:T(2,128)(2,1)} %copy.46), calls=%async_computation.2 | async-start | bytes 32768 | tf_op jit(solution)/shard_map/all_to_all | solution.py:108
  122.0 11.3 %all-to-all-start.3 = ((bf16[32,2,1024]{2,1,0:T(2,128)(2,1)}), bf16[32,2,1024]{2,1,0:T(2,128)(2,1)S(1)}, u32[]{:S(2)}, u32[]{:S(2)}) async-start(bf16[32,2,1024]{2,1,0:T(2,128)(2,1)} %reshape.616), calls=%async_computation.3 | async-start | bytes 262144 | tf_op jit(solution)/shard_map/all_to_all | solution.py:107
  142.8 10.8 %all-to-all-start.4 = ((bf16[32,2,1024]{2,1,0:T(2,128)(2,1)}), bf16[32,2,1024]{2,1,0:T(2,128)(2,1)S(1)}, u32[]{:S(2)}, u32[]{:S(2)}) async-start(bf16[32,2,1024]{2,1,0:T(2,128)(2,1)} %reshape.618), calls=%async_computation.4 | async-start | bytes 262144 | tf_op jit(solution)/shard_map/all_to_all | solution.py:117
where the time goes:
time: 156 us; the launch traced here: 155 us
  blocking collectives  83 us (53%)
  waiting for transfers between devices  23.7 us (15%)
  matrix products  14.3 us (9%)
  starting transfers between devices  13.3 us (9%)
  other arithmetic  11.7 us (8%)
  local copies, waits for them, and re-layouts  5.47 us (4%)
  between operations  3.69 us (2%)
    all_gather x1, blocking collectives, local(): piece = lax.all_gather(tokens, 'ep', axis=0, tiled=True)  44.3 us
    all_gather x1, blocking collectives, local(): lax.all_gather(gated, 'ep', axis=0, tiled=True)  38.6 us
    all_to_all x1, waiting for transfers between devices, local(): lax.all_to_all(outgoing, 'ep', split_axis=0, concat_axis=0, tiled=True)  7.35 us
    all_to_all x1, waiting for transfers between devices, local(): lax.all_to_all(proj_cols, 'ep', split_axis=0, concat_axis=1, tiled=True)  6.21 us
    add x1, other arithmetic, local(): keep[..., None, None] * memory_matrix  4.74 us
    dot_general x1, matrix products, run_expert(): jnp.dot(hidden, down_mat, preferred_element_type=jnp.float32)  4.68 us
    dot_general x1, matrix products, local(): jnp.einsum('shij,shj->shi', memory_matrix, query_heads, precision=lax.Pre...  4.15 us
    all_to_all x1, waiting for transfers between devices, local(): lax.all_to_all(result, 'ep', split_axis=0, concat_axis=2, tiled=True)  3.87 us
  transfers between devices with their start and end apart: 5, of which 5 were waited for; matrix products, arithmetic and copies ran while one was open for 7% of the time, Pallas kernels for 0%

commit v1 on v0

v1 whole, which is shorter than its diff:
```python
import jax
import jax.numpy as jnp
from jax import lax
from jax.sharding import PartitionSpec as P

GROUPS = 4
CAPACITY = 4
LANES = 128


norm_eps = 1e-06


def root_norm(values, gain):
    return values * lax.rsqrt(jnp.mean(values * values, axis=-1, keepdims=True) + norm_eps) * gain


def run_expert(slot_rows, gate_mat, up_mat, down_mat):
    gate_part = jnp.dot(slot_rows, gate_mat, preferred_element_type=jnp.float32)
    up_part = jnp.dot(slot_rows, up_mat, preferred_element_type=jnp.float32)
    hidden = (jax.nn.silu(gate_part) * up_part).astype(jnp.bfloat16)
    return jnp.dot(hidden, down_mat, preferred_element_type=jnp.float32).astype(jnp.bfloat16)


def exchange(blocks):
    return lax.all_to_all(blocks, "ep", split_axis=0, concat_axis=0, tiled=True)


def local(
    tokens,
    mixer_gain,
    query_weight,
    key_weight,
    value_weight,
    outgate_weight,
    input_weight,
    forget_weight,
    forget_bias,
    memory_matrix,
    memory_norm,
    memory_max,
    mixer_out,
    expert_gain,
    expert_gate,
    expert_up,
    expert_down,
    route_group,
    route_member,
    group_weight,
    member_weight,
):
    devices = lax.axis_size("ep")
    width = tokens.shape[1]
    columns = query_weight.shape[1]
    heads = memory_matrix.shape[1]
    head_dim = memory_matrix.shape[2]
    members = devices // GROUPS
    picks = route_member.shape[1]
    assert tokens.shape[0] == 1 and expert_gate.shape[0] == 1

    route = jnp.concatenate([route_group[:, None], route_member], axis=1).astype(jnp.bfloat16)
    route = jnp.pad(route, ((0, 0), (0, 2 * LANES - 1 - picks)))
    row = jnp.concatenate([tokens, route], axis=1)
    gathered = exchange(jnp.broadcast_to(row, (devices, row.shape[1])))
    rows = gathered[:, :width]
    ids = gathered[:, width:width + 1 + picks].astype(jnp.int32)
    chosen = ids[:, :1] * members + ids[:, 1:]

    targets = jnp.arange(devices, dtype=jnp.int32)
    hit = jnp.any(chosen[:, :, None] == targets[None, None, :], axis=1)
    hit_bf = hit.astype(jnp.bfloat16)
    upto = (targets[:, None] <= targets[None, :]).astype(jnp.bfloat16)
    place = jnp.dot(hit_bf.T, upto, preferred_element_type=jnp.float32) - 1.0
    slots = jnp.arange(CAPACITY, dtype=jnp.float32)
    take = hit.T[:, None, :] & (place[:, None, :] == slots[None, :, None])
    own = (targets[:, None] == targets[None, :])[:, None, :]
    take = jnp.concatenate([take, own], axis=1).astype(jnp.bfloat16)

    stacked = jnp.concatenate([query_weight, key_weight, value_weight, outgate_weight], axis=1)
    normed = root_norm(rows.astype(jnp.float32), mixer_gain).astype(jnp.bfloat16)
    result = jnp.dot(normed, stacked, preferred_element_type=jnp.float32).astype(jnp.bfloat16)
    parts = exchange(result).reshape(devices, 4, columns).transpose(1, 0, 2).reshape(4, heads, head_dim)

    resid = tokens.astype(jnp.float32)
    own_normed = root_norm(resid, mixer_gain).astype(jnp.bfloat16)
    input_pre = jnp.dot(own_normed, input_weight, preferred_element_type=jnp.float32)
    forget_pre = (
        jnp.dot(own_normed, forget_weight, preferred_element_type=jnp.float32) + forget_bias
    )
    log_forget = jax.nn.log_sigmoid(forget_pre)
    next_max = jnp.maximum(log_forget + memory_max, input_pre)
    keep = jnp.exp(log_forget + memory_max - next_max)
    admit = jnp.exp(input_pre - next_max)

    parts = parts.astype(jnp.float32)
    query_heads = parts[0][None]
    key_heads = parts[1][None] * head_dim ** (-0.5)
    value_heads = parts[2][None]
    carried = jnp.einsum(
        "shij,shj->shi", memory_matrix, query_heads, precision=lax.Precision.HIGHEST
    )
    score = jnp.sum(key_heads * query_heads, axis=-1)
    numer = keep[..., None] * carried + (admit * score)[..., None] * value_heads
    denom = keep * jnp.sum(memory_norm * query_heads, axis=-1) + admit * score
    head_out = numer / jnp.maximum(jnp.abs(denom), jnp.exp(-next_max))[..., None]
    gated = (head_out * jax.nn.sigmoid(parts[3][None])).reshape(1, width).astype(jnp.bfloat16)
    next_matrix = (
        keep[..., None, None] * memory_matrix
        + admit[..., None, None] * value_heads[..., :, None] * key_heads[..., None, :]
    )
    next_norm = keep[..., None] * memory_norm + admit[..., None] * key_heads

    gated_rows = exchange(jnp.broadcast_to(gated, (devices, width)))

    proj_cols = jnp.dot(gated_rows, mixer_out, preferred_element_type=jnp.float32).astype(jnp.bfloat16)
    outgoing = jnp.dot(
        take.reshape(devices * (CAPACITY + 1), devices), proj_cols, preferred_element_type=jnp.float32
    ).astype(jnp.bfloat16)
    incoming = exchange(outgoing.reshape(devices, (CAPACITY + 1) * columns))
    projected = incoming.reshape(devices, CAPACITY + 1, columns).transpose(1, 0, 2)
    projected = projected.reshape(CAPACITY + 1, width).astype(jnp.float32)
    me = lax.axis_index("ep")
    mine = lax.dynamic_index_in_dim(take, me, axis=0, keepdims=False)
    slot_resid = jnp.dot(mine, rows, preferred_element_type=jnp.float32)
    middle = (slot_resid + projected).astype(jnp.bfloat16)
    expert_in = root_norm(middle[:CAPACITY].astype(jnp.float32), expert_gain).astype(jnp.bfloat16)
    finished = run_expert(expert_in, expert_gate[0], expert_up[0], expert_down[0])

    back_rows = jnp.dot(
        mine[:CAPACITY].T, finished, preferred_element_type=jnp.float32
    ).astype(jnp.bfloat16)
    returned = exchange(back_rows)
    local_chosen = route_group[:, None] * members + route_member
    local_weight = group_weight[:, None] * member_weight
    weights = jnp.sum(
        jnp.where(local_chosen[:, :, None] == targets[None, None, :], local_weight[:, :, None], 0.0), axis=1
    )
    mixture = jnp.sum(weights.T * returned.astype(jnp.float32), axis=0, keepdims=True)
    layer_out = (middle[CAPACITY:].astype(jnp.float32) + mixture).astype(jnp.bfloat16)
    return (layer_out, next_matrix, next_norm, next_max)


def solution(mesh):
    placed = (
        P("ep", None),
        P(),
        P(None, "ep"),
        P(None, "ep"),
        P(None, "ep"),
        P(None, "ep"),
        P(),
        P(),
        P(),
        P("ep", None, None, None),
        P("ep", None, None),
        P("ep", None),
        P(None, "ep"),
        P(),
        P("ep", None, None),
        P("ep", None, None),
        P("ep", None, None),
        P("ep"),
        P("ep", None),
        P("ep"),
        P("ep", None),
    )
    return jax.shard_map(
        local,
        mesh=mesh,
        in_specs=placed,
        out_specs=(P("ep", None), P("ep", None, None, None), P("ep", None, None), P("ep", None)),
        check_vma=False,
    )
```

time: 156 us -> 89 us (0.57)
  blocking collectives: 83 us -> 0 us
  other arithmetic: 11.7 us -> 16.9 us
  starting transfers between devices: 13.3 us -> 18.4 us
  waiting for transfers between devices: 23.7 us -> 27.9 us
  matrix products: 14.3 us -> 16.1 us
    all_gather x2 -> x0, blocking collectives: 83 us -> none  [the longest x1 44.3 us: local(): piece = lax.all_gather(tokens, 'ep', axis=0, tiled=True)]
    all_to_all x5, starting transfers between devices: 13.3 us -> 18.4 us  [exchange(): return lax.all_to_all(blocks, 'ep', split_axis=0, concat_axis=0, tiled=True)]
    all_to_all x5, waiting for transfers between devices: 23.7 us -> 27.9 us  [exchange(): return lax.all_to_all(blocks, 'ep', split_axis=0, concat_axis=0, tiled=True)]
    broadcast_in_dim x0 -> x2, other arithmetic: none -> 2.87 us  [the longest x1 1.49 us: local(): gathered = exchange(jnp.broadcast_to(row, (devices, row.shape[1])))]
    all_to_all x0 -> x4, other arithmetic: none -> 2.21 us  [exchange(): return lax.all_to_all(blocks, 'ep', split_axis=0, concat_axis=0, tiled=True)]
    select_n x3 -> x0, other arithmetic: 1.64 us -> none  [the longest x2 1.63 us: local(): jnp.where(hit.T[:, :, None], expert_in[None, :, :], jnp.zeros((), jnp.bfl...]
    unnamed x32 -> x21, local copies, waits for them, and re-layouts: 2.59 us -> 4.03 us
  transfers between devices with their start and end apart: 5 -> 5, of which waited for: 5 -> 5; matrix products, arithmetic and copies ran while one was open for 7% -> 11% of each run, Pallas kernels for 0% -> 0%
where the time goes in v1:
time: 89 us; the launch traced here: 88.2 us
  waiting for transfers between devices  27.9 us (31%)
  starting transfers between devices  18.4 us (21%)
  other arithmetic  16.9 us (19%)
  matrix products  16.1 us (18%)
  local copies, waits for them, and re-layouts  5.93 us (7%)
  between operations  2.99 us (3%)
    all_to_all x5, waiting for transfers between devices, exchange(): return lax.all_to_all(blocks, 'ep', split_axis=0, concat_axis=0, tiled=True)  27.9 us
    all_to_all x5, starting transfers between devices, exchange(): return lax.all_to_all(blocks, 'ep', split_axis=0, concat_axis=0, tiled=True)  18.4 us
    add x1, other arithmetic, local(): keep[..., None, None] * memory_matrix  4.76 us
    dot_general x1, matrix products, run_expert(): jnp.dot(hidden, down_mat, preferred_element_type=jnp.float32)  4.71 us
    dot_general x1, matrix products, local(): jnp.einsum('shij,shj->shi', memory_matrix, query_heads, precision=lax.Pre...  4.15 us
    unnamed x21, local copies, waits for them, and re-layouts  4.03 us
    dot_general x1, matrix products, run_expert(): gate_part = jnp.dot(slot_rows, gate_mat, preferred_element_type=jnp.float32)  2.88 us
    all_to_all x4, other arithmetic, exchange(): return lax.all_to_all(blocks, 'ep', split_axis=0, concat_axis=0, tiled=True)  2.21 us
  transfers between devices with their start and end apart: 5, of which 5 were waited for; matrix products, arithmetic and copies ran while one was open for 11% of the time, Pallas kernels for 0%

profile of v1, /device:TPU:0, one launch (start us, length us, event | category | flops | bytes accessed | tf_op | source)
XLA Modules:
  0.0 88.2 jit_solution(2869536994301549399)
XLA Ops:
  1.3 0.7 add_bitcast_fusion
  3.6 1.5 %reduce.9 = bf16[32,2304]{1,0:T(8,128)(2,1)S(1)} reduce(bf16[32,1,2304]{2,1,0:T(2,128)(2,1)S(1)} %broadcast_in_dim.16, bf16[]{:T(256)} %broadcast.177), dimensions={1}, to_apply=%broadcast_in_dim.16.reduce_sub_computation | reduce | bytes 294914 | tf_op jit(solution)/shard_map/broadcast_in_dim | solution.py:64
  5.8 7.3 %all-to-all-start = ((bf16[32,2,1152]{2,1,0:T(2,128)(2,1)}), bf16[32,2,1152]{2,1,0:T(2,128)(2,1)S(1)}, u32[]{:S(2)}, u32[]{:S(2)}) async-start(bf16[32,2,1152]{2,1,0:T(2,128)(2,1)} %reshape.322), calls=%async_computation | async-start | bytes 294912 | tf_op jit(solution)/shard_map/all_to_all | solution.py:26
  13.1 1.3 %multiply_reduce_fusion.2 = f32[]{:T(128)} fusion(bf16[1,2048]{1,0:T(2,128)(2,1)} %param.21), kind=kLoop, calls=%fused_computation.81 | loop fusion | flops 6143 | bytes 4100 | tf_op jit(solution)/shard_map/reduce_sum | solution.py:15
  17.2 0.9 bitcast_add_fusion.1
  18.1 0.9 broadcast_multiply_fusion.1
  19.0 2.5 %all-to-all-done = bf16[32,2,1152]{2,1,0:T(2,128)(2,1)S(1)} async-done(((bf16[32,2,1152]{2,1,0:T(2,128)(2,1)}), bf16[32,2,1152]{2,1,0:T(2,128)(2,1)S(1)}, u32[]{:S(2)}, u32[]{:S(2)}) %all-to-all-start) | async-done | bytes 147488 | tf_op jit(solution)/shard_map/all_to_all | solution.py:26
  22.0 1.6 %fusion.13 = bf16[32,1,256]{2,0,1:T(8,128)(2,1)S(1)} fusion(bf16[2048,64]{0,1:T(8,128)(2,1)} %param.26, bf16[2048,64]{0,1:T(8,128)(2,1)} %param.25, bf16[2048,64]{0,1:T(8,128)(2,1)} %param.24, bf16[2048,64]{0,1:T(8,128)(2,1)} %param.23, f32[2048]{0:T(1024)} %param.22, f32[32]{0:T(128)S(1)} %add_rsqrt_fusion.1, bf16[32,2304]{1,0:T(8,128)(2,1)S(1)} %bitcast.130), kind=kOutput, calls=%fused_computation.16 | convolution fusion | flops 38019072 | bytes 1204736 | tf_op jit(solution)/shard_map/dot_general | solution.py:81
  24.9 3.4 %all-to-all-start.1 = ((bf16[32,2,128]{2,1,0:T(2,128)(2,1)}), bf16[32,2,128]{2,1,0:T(2,128)(2,1)S(1)}, u32[]{:S(2)}, u32[]{:S(2)}) async-start(bf16[32,2,128]{2,1,0:T(2,128)(2,1)} %reshape.324), calls=%async_computation.1 | async-start | bytes 32768 | tf_op jit(solution)/shard_map/all_to_all | solution.py:26
  28.6 6.8 %all-to-all-done.1 = bf16[32,2,128]{2,1,0:T(2,128)(2,1)S(1)} async-done(((bf16[32,2,128]{2,1,0:T(2,128)(2,1)}), bf16[32,2,128]{2,1,0:T(2,128)(2,1)S(1)}, u32[]{:S(2)}, u32[]{:S(2)}) %all-to-all-start.1) | async-done | bytes 16416 | tf_op jit(solution)/shard_map/all_to_all | solution.py:26
  36.1 4.2 %fusion.6 = f32[4,1,512]{2,1,0:T(1,128)S(1)} fusion(bf16[4,512,1]{1,2,0:T(2,128)(2,1)S(1)} %reshape.318, f32[1,4,512,512]{3,2,1,0:T(8,128)} %param.30), kind=kOutput, calls=%fused_computation.6 | convolution fusion | flops 12582912 | bytes 4206592 | tf_op jit(solution)/shard_map/shij,shj->shi/dot_general | solution.py:99
  40.2 0.8 multiply_reduce_fusion.1
  41.3 1.4 %reduce.11 = bf16[32,2048]{1,0:T(8,128)(2,1)S(1)} reduce(bf16[32,1,2048]{2,1,0:T(2,128)(2,1)S(1)} %broadcast_in_dim.18, bf16[]{:T(256)} %broadcast.177), dimensions={1}, to_apply=%broadcast_in_dim.18.reduce_sub_computation | reduce | bytes 262146 | tf_op jit(solution)/shard_map/broadcast_in_dim | solution.py:113
  42.7 0.7 reshape.326
  43.4 2.6 %all-to-all-start.2 = ((bf16[32,2,1024]{2,1,0:T(2,128)(2,1)}), bf16[32,2,1024]{2,1,0:T(2,128)(2,1)S(1)}, u32[]{:S(2)}, u32[]{:S(2)}) async-start(bf16[32,2,1024]{2,1,0:T(2,128)(2,1)} %reshape.326), calls=%async_computation.2 | async-start | bytes 262144 | tf_op jit(solution)/shard_map/all_to_all | solution.py:26
  46.3 8.0 %all-to-all-done.2 = bf16[32,2,1024]{2,1,0:T(2,128)(2,1)S(1)} async-done(((bf16[32,2,1024]{2,1,0:T(2,128)(2,1)}), bf16[32,2,1024]{2,1,0:T(2,128)(2,1)S(1)}, u32[]{:S(2)}, u32[]{:S(2)}) %all-to-all-start.2) | async-done | bytes 131104 | tf_op jit(solution)/shard_map/all_to_all | solution.py:26
  55.0 0.8 reduce.12
  56.5 2.6 %all-to-all-start.3 = ((bf16[32,2,160]{2,1,0:T(2,128)(2,1)}), bf16[32,2,160]{2,1,0:T(2,128)(2,1)S(1)}, u32[]{:S(2)}, u32[]{:S(2)}) async-start(bf16[32,2,160]{2,1,0:T(2,128)(2,1)} %reshape.328), calls=%async_computation.3 | async-start | bytes 65536 | tf_op jit(solution)/shard_map/all_to_all | solution.py:26
  59.1 7.2 %all-to-all-done.3 = bf16[32,2,160]{2,1,0:T(2,128)(2,1)S(1)} async-done(((bf16[32,2,160]{2,1,0:T(2,128)(2,1)}), bf16[32,2,160]{2,1,0:T(2,128)(2,1)S(1)}, u32[]{:S(2)}, u32[]{:S(2)}) %all-to-all-start.3) | async-done | bytes 20512 | tf_op jit(solution)/shard_map/all_to_all | solution.py:26
  67.0 2.9 %fusion.4 = f32[4,1024]{1,0:T(4,128)S(1)} fusion(bf16[1,2048,1024]{2,1,0:T(8,128)(2,1)} %param.35, f32[2048]{0:T(1024)S(1)} %copy-done.1, f32[4]{0:T(128)S(1)} %add_rsqrt_fusion, bf16[5,2048]{1,0:T(8,128)(2,1)S(1)} %fusion.9), kind=kOutput, calls=%fused_computation.4 | convolution fusion | flops 16809984 | bytes 4235776 | tf_op jit(solution)/shard_map/dot_general | solution.py:19
  69.9 4.7 %fusion.10 = bf16[4,2048]{1,0:T(4,128)(2,1)S(1)} fusion(bf16[1,1024,2048]{2,1,0:T(8,128)(2,1)} %param.37, bf16[1,2048,1024]{2,1,0:T(8,128)(2,1)} %param.36, f32[4,1024]{1,0:T(4,128)S(1)} %fusion.4, f32[2048]{0:T(1024)S(1)} %copy-done.1, f32[4]{0:T(128)S(1)} %add_rsqrt_fusion, bf16[5,2048]{1,0:T(8,128)(2,1)S(1)} %fusion.9), kind=kOutput, calls=%fused_computation.13 | convolution fusion | flops 33619968 | bytes 8446464 | tf_op jit(solution)/shard_map/dot_general | solution.py:22
  76.3 2.6 %all-to-all-start.4 = ((bf16[32,2,1024]{2,1,0:T(2,128)(2,1)}), bf16[32,2,1024]{2,1,0:T(2,128)(2,1)S(1)}, u32[]{:S(2)}, u32[]{:S(2)}) async-start(bf16[32,2,1024]{2,1,0:T(2,128)(2,1)} %reshape.330), calls=%async_computation.4 | async-start | bytes 262144 | tf_op jit(solution)/shard_map/all_to_all | solution.py:26
  78.8 4.8 %multiply_add_fusion = f32[1,4,512,512]{3,2,1,0:T(8,128)} fusion(f32[1,4,512,512]{3,2,1,0:T(8,128)} %param.30, f32[4,512]{1,0:T(4,128)S(1)} %get-tuple-element.15, f32[4,512]{1,0:T(4,128)S(1)} %broadcast_multiply_fusion, f32[4]{0:T(128)S(1)} %fusion.71), kind=kLoop, calls=%fused_computation.8 | loop fusion | flops 3145728 | bytes 8405008 | tf_op jit(solution)/shard_map/add | solution.py:108
  83.6 3.4 %all-to-all-done.4 = bf16[32,2,1024]{2,1,0:T(2,128)(2,1)S(1)} async-done(((bf16[32,2,1024]{2,1,0:T(2,128)(2,1)}), bf16[32,2,1024]{2,1,0:T(2,128)(2,1)S(1)}, u32[]{:S(2)}, u32[]{:S(2)}) %all-to-all-start.4) | async-done | bytes 131104 | tf_op jit(solution)/shard_map/all_to_all | solution.py:26
  (73 shorter events, 11.8 us)
Async XLA Ops:
  0.6 53.7 %copy-start = (bf16[2048,64]{0,1:T(8,128)(2,1)S(1)}, bf16[2048,64]{0,1:T(8,128)(2,1)}, u32[]{:S(2)}) copy-start(bf16[2048,64]{0,1:T(8,128)(2,1)} %param.33) | copy-start | bytes 786436
  5.8 15.7 %all-to-all-start = ((bf16[32,2,1152]{2,1,0:T(2,128)(2,1)}), bf16[32,2,1152]{2,1,0:T(2,128)(2,1)S(1)}, u32[]{:S(2)}, u32[]{:S(2)}) async-start(bf16[32,2,1152]{2,1,0:T(2,128)(2,1)} %reshape.322), calls=%async_computation | async-start | bytes 294912 | tf_op jit(solution)/shard_map/all_to_all | solution.py:26
  19.0 22.1 %copy-start.3 = (f32[1,4]{1,0:T(1,128)}, f32[1,4]{1,0:T(1,128)S(1)}, u32[]{:S(2)}) copy-start(f32[1,4]{1,0:T(1,128)S(1)} %get-tuple-element.7) | copy-start | bytes 52
  22.0 18.2 %copy-start.2 = (f32[1,4,512]{2,1,0:T(4,128)S(1)}, f32[1,4,512]{2,1,0:T(4,128)}, u32[]{:S(2)}) copy-start(f32[1,4,512]{2,1,0:T(4,128)} %param.31) | copy-start | bytes 24580
  24.9 10.5 %all-to-all-start.1 = ((bf16[32,2,128]{2,1,0:T(2,128)(2,1)}), bf16[32,2,128]{2,1,0:T(2,128)(2,1)S(1)}, u32[]{:S(2)}, u32[]{:S(2)}) async-start(bf16[32,2,128]{2,1,0:T(2,128)(2,1)} %reshape.324), calls=%async_computation.1 | async-start | bytes 32768 | tf_op jit(solution)/shard_map/all_to_all | solution.py:26
  35.4 31.6 %copy-start.1 = (f32[2048]{0:T(1024)S(1)}, f32[2048]{0:T(1024)}, u32[]{:S(2)}) copy-start(f32[2048]{0:T(1024)} %param.34) | copy-start | bytes 24580
  43.4 10.8 %all-to-all-start.2 = ((bf16[32,2,1024]{2,1,0:T(2,128)(2,1)}), bf16[32,2,1024]{2,1,0:T(2,128)(2,1)S(1)}, u32[]{:S(2)}, u32[]{:S(2)}) async-start(bf16[32,2,1024]{2,1,0:T(2,128)(2,1)} %reshape.326), calls=%async_computation.2 | async-start | bytes 262144 | tf_op jit(solution)/shard_map/all_to_all | solution.py:26
  56.5 9.8 %all-to-all-start.3 = ((bf16[32,2,160]{2,1,0:T(2,128)(2,1)}), bf16[32,2,160]{2,1,0:T(2,128)(2,1)S(1)}, u32[]{:S(2)}, u32[]{:S(2)}) async-start(bf16[32,2,160]{2,1,0:T(2,128)(2,1)} %reshape.328), calls=%async_computation.3 | async-start | bytes 65536 | tf_op jit(solution)/shard_map/all_to_all | solution.py:26
  76.3 10.8 %all-to-all-start.4 = ((bf16[32,2,1024]{2,1,0:T(2,128)(2,1)}), bf16[32,2,1024]{2,1,0:T(2,128)(2,1)S(1)}, u32[]{:S(2)}, u32[]{:S(2)}) async-start(bf16[32,2,1024]{2,1,0:T(2,128)(2,1)} %reshape.330), calls=%async_computation.4 | async-start | bytes 262144 | tf_op jit(solution)/shard_map/all_to_all | solution.py:26

commit v2 on v0

v2 whole, which is shorter than its diff:
```python
import jax
import jax.numpy as jnp
from jax import lax
from jax.experimental import pallas as pl
from jax.experimental.pallas import tpu as pltpu
from jax.sharding import PartitionSpec as P

GROUPS = 4
CAPACITY = 4
LANES = 128
SLOTS = 8
MIB = 1 << 20
F32 = jnp.float32
BF16 = jnp.bfloat16
NT = (((1,), (1,)), ((), ()))


norm_eps = 1e-06


def root_norm(values, gain):
    return values * lax.rsqrt(jnp.mean(values * values, axis=-1, keepdims=True) + norm_eps) * gain


def exchange(blocks):
    count, width = blocks.shape
    halves = blocks.reshape(count, 2, width // 2)
    return lax.all_to_all(halves, "ep", split_axis=0, concat_axis=0, tiled=True).reshape(count, width)


VMEM_SPEC = pl.BlockSpec(memory_space=pltpu.VMEM)
SMEM_SPEC = pl.BlockSpec(memory_space=pltpu.SMEM)
HBM_SPEC = pl.BlockSpec(memory_space=pltpu.HBM)


def call(body, outs, ins, scratch=(), limit=8 * MIB, flops=10_000_000, moved=1_000_000):
    return pl.pallas_call(
        body,
        out_shape=outs,
        in_specs=ins,
        out_specs=jax.tree.map(lambda _: VMEM_SPEC, outs),
        scratch_shapes=scratch,
        compiler_params=pltpu.CompilerParams(vmem_limit_bytes=limit),
        cost_estimate=pl.CostEstimate(flops=flops, bytes_accessed=moved, transcendentals=0),
    )


def in_hbm(array):
    return pltpu.with_memory_space_constraint(array, pltpu.HBM)


def shaped(shape, dtype=F32):
    return jax.ShapeDtypeStruct(shape, dtype)


def feature_rows(ref, offset, columns):
    group = LANES // columns
    count = ref.shape[1] // group
    tile, lane = divmod(offset, LANES)
    pieces = [
        ref[tile, pl.ds(g, count, stride=group), :][:, lane:lane + columns] for g in range(group)
    ]
    return jnp.concatenate(pieces, axis=1)


def spill(ref, values):
    for t in range(ref.shape[0]):
        part = values[:, t * LANES:(t + 1) * LANES]
        ref[t, :, :part.shape[1]] = part


def diagonal(n):
    i = lax.broadcasted_iota(jnp.int32, (n, n), 0)
    j = lax.broadcasted_iota(jnp.int32, (n, n), 1)
    return i == j


def to_column(row):
    n = row.shape[1]
    spread = jnp.broadcast_to(row, (n, n))
    return jnp.sum(jnp.where(diagonal(n), spread, 0.0), axis=1, keepdims=True)


def to_row(col):
    n = col.shape[0]
    spread = jnp.broadcast_to(col, (n, n))
    return jnp.sum(jnp.where(diagonal(n), spread, 0.0), axis=0, keepdims=True)


def fetch_columns_body(
    group_ref, member_ref, wq, wk, wv, wo, wi, wf, gain,
    stacked, wi_out, wf_out, gain_out, ids_out, sems,
):
    columns = wq.shape[0]
    copies = [
        pltpu.make_async_copy(w, stacked.at[pl.ds(n * columns, columns)], sems.at[n])
        for n, w in enumerate((wq, wk, wv, wo))
    ]
    copies += [
        pltpu.make_async_copy(a, b, sems.at[4 + n])
        for n, (a, b) in enumerate(((wi, wi_out), (wf, wf_out), (gain, gain_out)))
    ]
    for c in copies:
        c.start()
    lane = lax.broadcasted_iota(jnp.int32, ids_out.shape, 1)
    ids = jnp.where(lane == 0, group_ref[0], 0)
    for k in range(member_ref.shape[0]):
        ids = jnp.where(lane == 1 + k, member_ref[k], ids)
    ids_out[...] = ids.astype(F32)
    for c in copies:
        c.wait()


def fetch_cell_body(mem, norm, most, bias, mem_out, norm_out, most_out, bias_out, sems):
    early = mem_out.shape[0]
    copies = [
        pltpu.make_async_copy(a, b, sems.at[n])
        for n, (a, b) in enumerate(
            ((mem.at[pl.ds(0, early)], mem_out), (norm, norm_out), (most, most_out), (bias, bias_out))
        )
    ]
    for c in copies:
        c.start()
    for c in copies:
        c.wait()


def columns_body(rows_ref, ids_ref, gain_ref, stacked, wi, wf, out_ref, pre_ref):
    heads = wi.shape[0]
    count = rows_ref.shape[0]
    total = stacked.shape[0]
    normed = root_norm(rows_ref[...].astype(F32), gain_ref[...]).astype(BF16)
    cols = lax.dot_general(normed, stacked[...], NT, preferred_element_type=F32)
    out_ref[:, :total] = cols.astype(BF16)
    out_ref[:, total:] = jnp.broadcast_to(ids_ref[...], (count, ids_ref.shape[1])).astype(BF16)
    pre_ref[:heads, :] = lax.dot_general(wi[...], normed, NT, preferred_element_type=F32)
    pre_ref[heads:, :] = lax.dot_general(wf[...], normed, NT, preferred_element_type=F32)


def tables_body(
    me_ref, group_ref, member_ref, group_weight, member_weight, parts_ref,
    take_ref, mine_ref, spread_ref, weight_ref,
):
    count = parts_ref.shape[0]
    members = count // GROUPS
    picks = member_ref.shape[0]
    ids = parts_ref[:, parts_ref.shape[1] - LANES:].astype(F32)
    lane = lax.broadcasted_iota(jnp.int32, ids.shape, 1)

    def row_of(k):
        return to_row(jnp.sum(jnp.where(lane == k, ids, 0.0), axis=1, keepdims=True))

    group = row_of(0)
    expert = lax.broadcasted_iota(jnp.int32, (count, count), 0)
    token = lax.broadcasted_iota(jnp.int32, (count, count), 1)
    hit = jnp.zeros((count, count), F32)
    column = lax.broadcasted_iota(jnp.int32, (count, 1), 0)
    weight = jnp.zeros((count, 1), F32)
    for k in range(picks):
        chosen = (group * members + row_of(1 + k)).astype(jnp.int32)
        hit = jnp.where(expert == chosen, 1.0, hit)
        local = group_ref[0] * members + member_ref[k]
        weight += jnp.where(column == local, group_weight[0] * member_weight[k], 0.0)
    weight_ref[...] = weight
    upto = jnp.where(expert <= token, 1.0, 0.0).astype(BF16)
    place = jnp.dot(hit.astype(BF16), upto, preferred_element_type=F32)
    slot = lax.broadcasted_iota(jnp.int32, (SLOTS, count), 0)
    lane = lax.broadcasted_iota(jnp.int32, (count, SLOTS), 1)
    mine = jnp.zeros((SLOTS, count), F32)
    spread = jnp.zeros((count, SLOTS), F32)
    for s in range(CAPACITY + 1):
        if s < CAPACITY:
            take = jnp.where(place == s + 1.0, hit, 0.0)
        else:
            take = jnp.where(expert == token, 1.0, 0.0)
        take_ref[s] = take.astype(BF16)
        row = jnp.sum(jnp.where(expert == me_ref[0], take, 0.0), axis=0, keepdims=True)
        mine = jnp.where(slot == s, row, mine)
        if s < CAPACITY:
            spread = jnp.where(lane == s, to_column(row), spread)
    mine_ref[...] = mine.astype(BF16)
    spread_ref[...] = spread.astype(BF16)


def cell_body(
    me_ref, parts_ref, pre_ref, max_ref, bias_ref, norm_ref, early_ref, mem_ref,
    gated_ref, norm_out, max_out, value_out, key_out, keep_out,
    mem, wide, tall, sems,
):
    heads, head_dim = norm_ref.shape
    early = early_ref.shape[0]
    copies = [
        pltpu.make_async_copy(mem_ref.at[early + h], mem.at[h], sems.at[h]) for h in range(heads - early)
    ]
    for c in copies:
        c.start()

    columns = (parts_ref.shape[1] - LANES) // 4
    tiles = head_dim // LANES
    rows = heads * tiles
    spill(wide, parts_ref[:, :4 * columns].astype(F32))
    for n in range(4):
        tall[n * rows:(n + 1) * rows, :] = feature_rows(wide, n * columns, columns)

    def heads_of(n):
        return jnp.concatenate(
            [tall[pl.ds(n * rows + p, heads, stride=tiles), :] for p in range(tiles)], axis=1
        )

    query, key, value, outgate = (heads_of(n) for n in range(4))
    key = key * head_dim ** (-0.5)

    pre = pre_ref[...]
    lane = lax.broadcasted_iota(jnp.int32, pre.shape, 1)
    pre = jnp.sum(jnp.where(lane == me_ref[0], pre, 0.0), axis=1, keepdims=True)
    input_pre = pre[:heads]
    forget_pre = pre[heads:] + to_column(bias_ref[...])
    log_forget = jnp.minimum(forget_pre, 0.0) - jnp.log1p(jnp.exp(-jnp.abs(forget_pre)))
    carry = log_forget + to_column(max_ref[...])
    next_max = jnp.maximum(carry, input_pre)
    keep = jnp.exp(carry - next_max)
    admit = jnp.exp(input_pre - next_max)

    norm = norm_ref[...]
    score = admit * jnp.sum(key * query, axis=1, keepdims=True)
    denom = keep * jnp.sum(norm * query, axis=1, keepdims=True) + score
    scale = 1.0 / jnp.maximum(jnp.abs(denom), jnp.exp(-next_max))
    opened = jax.nn.sigmoid(outgate)
    norm_out[...] = keep * norm + admit * key
    max_out[...] = to_row(next_max)
    value_out[...] = admit * value
    key_out[...] = key
    keep_out[...] = jnp.broadcast_to(keep, keep_out.shape)

    count = gated_ref.shape[0]
    left = jnp.concatenate([query, jnp.zeros((8 - heads, head_dim), F32)], axis=0) if heads < 8 else query
    left = left.astype(BF16)
    for h in range(heads):
        if h < early:
            block = early_ref[h]
        else:
            copies[h - early].wait()
            block = mem[h - early]
        high = block.astype(BF16)
        low = (block - high.astype(F32)).astype(BF16)
        carried = lax.dot_general(left, high, NT, preferred_element_type=F32)
        carried = carried + lax.dot_general(left, low, NT, preferred_element_type=F32)
        carried = carried[h:h + 1]
        numer = keep[h:h + 1] * carried + score[h:h + 1] * value[h:h + 1]
        gated = numer * scale[h:h + 1] * opened[h:h + 1]
        gated_ref[:, h * head_dim:(h + 1) * head_dim] = jnp.broadcast_to(
            gated, (count, head_dim)
        ).astype(BF16)


def project_body(gated_ref, weight_ref, take_ref, out_ref):
    proj = lax.dot_general(gated_ref[...], weight_ref[...], NT, preferred_element_type=F32).astype(BF16)
    blocks = [
        jnp.dot(take_ref[s], proj, preferred_element_type=F32) for s in range(take_ref.shape[0])
    ]
    out_ref[...] = jnp.concatenate(blocks, axis=1).astype(BF16)


def expert_body(
    in_ref, rows_ref, mine_ref, spread_ref, gain_ref, gate_ref, up_ref, down_ref,
    out_ref, middle_ref,
    gate, up, down, wide, tall, sems,
):
    width, hidden_dim = gate_ref.shape
    steps = sems.shape[1]
    wide_step = width // steps
    tall_step = hidden_dim // steps
    plan = []
    for n, (src, dst, step) in enumerate(
        ((gate_ref, gate, wide_step), (up_ref, up, wide_step), (down_ref, down, tall_step))
    ):
        plan.append([
            pltpu.make_async_copy(
                src.at[pl.ds(k * step, step)], dst.at[pl.ds(k * step, step)], sems.at[n, k]
            )
            for k in range(steps)
        ])
    for k in range(steps):
        plan[0][k].start()
        plan[1][k].start()
    for k in range(steps):
        plan[2][k].start()

    used = CAPACITY + 1
    columns = in_ref.shape[1] // used
    tiles = width // LANES
    spill(wide, in_ref[...].astype(F32))
    for s in range(used):
        tall[s * tiles:(s + 1) * tiles, :] = feature_rows(wide, s * columns, columns)
    tall[used * tiles:, :] = jnp.zeros((tall.shape[0] - used * tiles, LANES), F32)
    projected = jnp.concatenate(
        [tall[pl.ds(r, SLOTS, stride=tiles), :] for r in range(tiles)], axis=1
    )
    resid = jnp.dot(mine_ref[...], rows_ref[...], preferred_element_type=F32)
    middle = (resid + projected).astype(BF16).astype(F32)
    middle_ref[...] = middle[CAPACITY:CAPACITY + 1]
    left = root_norm(middle, gain_ref[...]).astype(BF16)

    gate_part = jnp.zeros((SLOTS, hidden_dim), F32)
    up_part = jnp.zeros((SLOTS, hidden_dim), F32)
    for k in range(steps):
        part = slice(k * wide_step, (k + 1) * wide_step)
        plan[0][k].wait()
        gate_part += jnp.dot(left[:, part], gate[part, :], preferred_element_type=F32)
        plan[1][k].wait()
        up_part += jnp.dot(left[:, part], up[part, :], preferred_element_type=F32)
    hidden = (gate_part / (1.0 + jnp.exp(-gate_part)) * up_part).astype(BF16)
    result = jnp.zeros((SLOTS, width), F32)
    for k in range(steps):
        part = slice(k * tall_step, (k + 1) * tall_step)
        plan[2][k].wait()
        result += jnp.dot(hidden[:, part], down[part, :], preferred_element_type=F32)
    out_ref[...] = jnp.dot(
        spread_ref[...], result.astype(BF16), preferred_element_type=F32
    ).astype(BF16)


def finish_body(returned_ref, weight_ref, middle_ref, out_ref):
    mixture = jnp.sum(weight_ref[...] * returned_ref[...].astype(F32), axis=0, keepdims=True)
    out_ref[...] = (middle_ref[...] + mixture).astype(BF16)


def local(
    tokens,
    mixer_gain,
    query_weight,
    key_weight,
    value_weight,
    outgate_weight,
    input_weight,
    forget_weight,
    forget_bias,
    memory_matrix,
    memory_norm,
    memory_max,
    mixer_out,
    expert_gain,
    expert_gate,
    expert_up,
    expert_down,
    route_group,
    route_member,
    group_weight,
    member_weight,
):
    devices = lax.axis_size("ep")
    width = tokens.shape[1]
    columns = query_weight.shape[1]
    heads, head_dim = memory_norm.shape[1:]
    hidden_dim = expert_gate.shape[2]
    assert tokens.shape[0] == 1 and expert_gate.shape[0] == 1
    me = lax.axis_index("ep").astype(jnp.int32)

    ids = (route_group, route_member.reshape(-1))

    rows = exchange(jnp.broadcast_to(tokens, (devices, width)))

    stacked, wi, wf, gain, id_row = call(
        fetch_columns_body,
        (
            shaped((4 * columns, width), BF16), shaped((heads, width), BF16),
            shaped((heads, width), BF16), shaped((1, width)), shaped((1, LANES)),
        ),
        [SMEM_SPEC] * 2 + [HBM_SPEC] * 7,
        [pltpu.SemaphoreType.DMA((7,))],
        limit=4 * MIB,
    )(
        *ids, in_hbm(query_weight.T), in_hbm(key_weight.T), in_hbm(value_weight.T),
        in_hbm(outgate_weight.T), in_hbm(input_weight.T), in_hbm(forget_weight.T),
        in_hbm(mixer_gain[None]),
    )
    cols, pre = call(
        columns_body,
        (shaped((devices, 4 * columns + LANES), BF16), shaped((2 * heads, devices))),
        [VMEM_SPEC] * 6,
    )(rows, id_row, gain, stacked, wi, wf)
    parts = exchange(cols)

    memory = memory_matrix.reshape(heads, head_dim, head_dim)
    tiles = width // LANES
    early = heads // 2
    early_memory, norm, most, bias = call(
        fetch_cell_body,
        (
            shaped((early, head_dim, head_dim)), shaped((heads, head_dim)),
            shaped((1, heads)), shaped((1, heads)),
        ),
        [HBM_SPEC] * 4,
        [pltpu.SemaphoreType.DMA((4,))],
        limit=24 * MIB,
    )(in_hbm(lax.optimization_barrier((memory, pre))[0]), in_hbm(memory_norm.reshape(heads, head_dim)), in_hbm(memory_max), in_hbm(forget_bias[None]))
    gated, next_norm, next_max, value, key, keep = call(
        cell_body,
        (
            shaped((devices, width), BF16), shaped((heads, head_dim)), shaped((1, heads)),
            shaped((heads, head_dim)), shaped((heads, head_dim)), shaped((heads, head_dim)),
        ),
        [SMEM_SPEC] + [VMEM_SPEC] * 6 + [HBM_SPEC],
        [
            pltpu.VMEM((heads - early, head_dim, head_dim), F32),
            pltpu.VMEM((pl.cdiv(4 * columns, LANES), devices, LANES), F32),
            pltpu.VMEM((4 * tiles, LANES), F32),
            pltpu.SemaphoreType.DMA((heads - early,)),
        ],
        limit=24 * MIB,
    )(me[None], parts, pre, most, bias, norm, early_memory, in_hbm(memory))
    gated_rows = exchange(gated)
    next_matrix = keep[:, :, None] * memory + value[:, :, None] * key[:, None, :]

    take, mine, spread, weights = call(
        tables_body,
        (
            shaped((CAPACITY + 1, devices, devices), BF16), shaped((SLOTS, devices), BF16),
            shaped((devices, SLOTS), BF16), shaped((devices, 1)),
        ),
        [SMEM_SPEC] * 5 + [VMEM_SPEC],
    )(me[None], *ids, group_weight, member_weight.reshape(-1), parts)

    outgoing = call(
        project_body, shaped((devices, (CAPACITY + 1) * columns), BF16), [VMEM_SPEC] * 3
    )(gated_rows, mixer_out.T, take)
    incoming = exchange(outgoing)

    back, middle = call(
        expert_body,
        (shaped((devices, width), BF16), shaped((1, width))),
        [VMEM_SPEC] * 5 + [HBM_SPEC] * 3,
        [
            pltpu.VMEM((width, hidden_dim), BF16),
            pltpu.VMEM((width, hidden_dim), BF16),
            pltpu.VMEM((hidden_dim, width), BF16),
            pltpu.VMEM((pl.cdiv((CAPACITY + 1) * columns, LANES), devices, LANES), F32),
            pltpu.VMEM((SLOTS * tiles, LANES), F32),
            pltpu.SemaphoreType.DMA((3, 4)),
        ],
        limit=24 * MIB,
    )(
        incoming, rows, mine, spread, expert_gain[None],
        in_hbm(expert_gate.reshape(width, hidden_dim)), in_hbm(expert_up.reshape(width, hidden_dim)),
        in_hbm(expert_down.reshape(hidden_dim, width)),
    )
    returned = exchange(back)
    layer_out = call(finish_body, shaped((1, width), BF16), [VMEM_SPEC] * 3)(returned, weights, middle)
    return (layer_out, next_matrix[None], next_norm[None], next_max)


def solution(mesh):
    placed = (
        P("ep", None),
        P(),
        P(None, "ep"),
        P(None, "ep"),
        P(None, "ep"),
        P(None, "ep"),
        P(),
        P(),
        P(),
        P("ep", None, None, None),
        P("ep", None, None),
        P("ep", None),
        P(None, "ep"),
        P(),
        P("ep", None, None),
        P("ep", None, None),
        P("ep", None, None),
        P("ep"),
        P("ep", None),
        P("ep"),
        P("ep", None),
    )
    return jax.shard_map(
        local,
        mesh=mesh,
        in_specs=placed,
        out_specs=(P("ep", None), P("ep", None, None, None), P("ep", None, None), P("ep", None)),
        check_vma=False,
    )
```

time: 156 us -> 70.5 us (0.45)
  blocking collectives: 83 us -> 8.95 us
  matrix products: 14.3 us -> 0 us
  Pallas kernels: 0 us -> 13.7 us
  other arithmetic: 11.7 us -> 4.68 us
  waiting for transfers between devices: 23.7 us -> 21.6 us
  starting transfers between devices: 13.3 us -> 15 us
  between operations: 3.69 us -> 2.1 us
    all_gather x2 -> x0, blocking collectives: 83 us -> none  [the longest x1 44.3 us: local(): piece = lax.all_gather(tokens, 'ep', axis=0, tiled=True)]
    dot_general x9 -> x0, matrix products: 14.3 us -> none  [the longest x1 4.68 us: run_expert(): jnp.dot(hidden, down_mat, preferred_element_type=jnp.float32)]
    pallas_call x0 -> x8, Pallas kernels: none -> 13.7 us  [the longest x1 5.12 us: local(): call(expert_body, (shaped((devices, width), BF16), shaped((1, width))), [...]
    all_to_all x0 -> x1, blocking collectives: none -> 8.95 us  [exchange(): lax.all_to_all(halves, 'ep', split_axis=0, concat_axis=0, tiled=True)]
    reshape x1 -> x6, local copies, waits for them, and re-layouts: 0.09 us -> 2.47 us  [the longest x4 2.28 us: exchange(): halves = blocks.reshape(count, 2, width // 2)]
    reduce_sum x5 -> x0, other arithmetic: 2.33 us -> none  [the longest x3 1.41 us: root_norm(): jnp.mean(values * values, axis=-1, keepdims=True) + norm_eps]
    all_to_all x5 -> x4, waiting for transfers between devices: 23.7 us -> 21.6 us  [exchange(): lax.all_to_all(halves, 'ep', split_axis=0, concat_axis=0, tiled=True)]
    unnamed x32 -> x13, local copies, waits for them, and re-layouts: 2.59 us -> 0.75 us
  transfers between devices with their start and end apart: 5 -> 4, of which waited for: 5 -> 4; matrix products, arithmetic and copies ran while one was open for 7% -> 6% of each run, Pallas kernels for 0% -> 6%
where the time goes in v2:
time: 70.5 us; the launch traced here: 70 us
  waiting for transfers between devices  21.6 us (31%)
  starting transfers between devices  15 us (21%)
  Pallas kernels  13.7 us (19%)
  blocking collectives  8.95 us (13%)
  other arithmetic  4.68 us (7%)
  local copies, waits for them, and re-layouts  3.96 us (6%)
  between operations  2.1 us (3%)
    all_to_all x4, waiting for transfers between devices, exchange(): lax.all_to_all(halves, 'ep', split_axis=0, concat_axis=0, tiled=True)  21.6 us
    all_to_all x4, starting transfers between devices, exchange(): lax.all_to_all(halves, 'ep', split_axis=0, concat_axis=0, tiled=True)  15 us
    all_to_all x1, blocking collectives, exchange(): lax.all_to_all(halves, 'ep', split_axis=0, concat_axis=0, tiled=True)  8.95 us
    pallas_call x1, Pallas kernels, local(): call(expert_body, (shaped((devices, width), BF16), shaped((1, width))), [...  5.12 us
    add x1, other arithmetic, local(): keep[:, :, None] * memory + value[:, :, None] * key[:, None, :]  3.95 us
    pallas_call x1, Pallas kernels, local(): call(cell_body, (shaped((devices, width), BF16), shaped((heads, head_dim)...  2.66 us
    reshape x4, local copies, waits for them, and re-layouts, exchange(): halves = blocks.reshape(count, 2, width // 2)  2.28 us
    pallas_call x1, Pallas kernels, local(): call(fetch_columns_body, (shaped((4 * columns, width), BF16), shaped((hea...  1.79 us
  transfers between devices with their start and end apart: 4, of which 4 were waited for; matrix products, arithmetic and copies ran while one was open for 6% of the time, Pallas kernels for 6%

profile of v2, /device:TPU:0, one launch (start us, length us, event | category | flops | bytes accessed | tf_op | source)
XLA Modules:
  0.0 70.0 jit_solution(8690188075818683378)
XLA Ops:
  0.6 0.7 %reduce = bf16[2048]{0:T(1024)(128)(2,1)S(1)} reduce(bf16[1,2048]{1,0:T(2,128)(2,1)} %param.21, bf16[]{:T(256)} %constant.15), dimensions={0}, to_apply=%param.21.reduce_sub_computation | reduce | bytes 8194 | tf_op args[0]
  1.4 0.7 %broadcast_in_dim.29 = bf16[32,2,1024]{2,1,0:T(2,128)(2,1)} broadcast(bf16[2,1024]{1,0:T(2,128)(2,1)S(1)} %broadcast_in_dim.28), dimensions={1,2} | broadcast | bytes 135168 | tf_op jit(solution)/shard_map/broadcast_in_dim | solution.py:361
  2.1 7.3 %all-to-all-start = ((bf16[32,2,1024]{2,1,0:T(2,128)(2,1)}), bf16[32,2,1024]{2,1,0:T(2,128)(2,1)S(1)}, u32[]{:S(2)}, u32[]{:S(2)}) async-start(bf16[32,2,1024]{2,1,0:T(2,128)(2,1)} %broadcast_in_dim.29), calls=%async_computation | async-start | bytes 262144 | tf_op jit(solution)/shard_map/all_to_all | solution.py:28
  10.1 0.6 copy-done.2
  10.7 1.8 %shard_map.228 = (bf16[256,2048]{1,0:T(8,128)(2,1)S(1)}, bf16[4,2048]{1,0:T(4,128)(2,1)S(1)}, bf16[4,2048]{1,0:T(4,128)(2,1)S(1)}, f32[1,2048]{1,0:T(1,128)S(1)}, f32[1,128]{1,0:T(1,128)S(1)}) custom-call(s32[1]{0:T(128)S(6)} %copy.28.group_ref, s32[2]{0:T(128)S(1)} %bitcast.31, bf16[64,2048]{1,0:T(8,128)(2,1)} %bitcast.42, bf16[64,2048]{1,0:T(8,128)(2,1)} %bitcast.43, ...), custom_call_target="tpu_custom_call" | custom-call | flops 10000000 | bytes 1000000 | tf_op jit(solution)/shard_map/pallas_call | solution.py:363
  12.5 5.1 %all-to-all-done = bf16[32,2,1024]{2,1,0:T(2,128)(2,1)S(1)} async-done(((bf16[32,2,1024]{2,1,0:T(2,128)(2,1)}), bf16[32,2,1024]{2,1,0:T(2,128)(2,1)S(1)}, u32[]{:S(2)}, u32[]{:S(2)}) %all-to-all-start) | async-done | bytes 131104 | tf_op jit(solution)/shard_map/all_to_all | solution.py:28
  17.7 0.5 shard_map.229
  18.2 0.7 %reshape.70 = bf16[32,2,192]{2,1,0:T(2,128)(2,1)} reshape(bf16[32,384]{1,0:T(8,128)(2,1)S(1)} %get-tuple-element.33) | data formatting | bytes 49152 | tf_op jit(solution)/shard_map/reshape | solution.py:27
  18.9 2.6 %all-to-all-start.1 = ((bf16[32,2,192]{2,1,0:T(2,128)(2,1)}), bf16[32,2,192]{2,1,0:T(2,128)(2,1)S(1)}, u32[]{:S(2)}, u32[]{:S(2)}) async-start(bf16[32,2,192]{2,1,0:T(2,128)(2,1)} %reshape.70), calls=%async_computation.1 | async-start | bytes 65536 | tf_op jit(solution)/shard_map/all_to_all | solution.py:28
  21.5 1.6 %shard_map.230 = (f32[2,512,512]{2,1,0:T(8,128)S(1)}, f32[4,512]{1,0:T(4,128)S(1)}, f32[1,4]{1,0:T(1,128)S(1)}, f32[1,4]{1,0:T(1,128)S(1)}) custom-call(f32[4,512,512]{2,1,0:T(8,128)} %bitcast.34, f32[4,512]{1,0:T(4,128)} %bitcast.49, f32[1,4]{1,0:T(1,128)} %most.1, f32[1,4]{1,0:T(1,128)} %bitcast.50), custom_call_target="tpu_custom_call" | custom-call | flops 10000000 | bytes 1000000 | tf_op jit(solution)/shard_map/pallas_call | solution.py:387
  23.2 5.6 %all-to-all-done.1 = bf16[32,2,192]{2,1,0:T(2,128)(2,1)S(1)} async-done(((bf16[32,2,192]{2,1,0:T(2,128)(2,1)}), bf16[32,2,192]{2,1,0:T(2,128)(2,1)S(1)}, u32[]{:S(2)}, u32[]{:S(2)}) %all-to-all-start.1) | async-done | bytes 24608 | tf_op jit(solution)/shard_map/all_to_all | solution.py:28
  28.8 2.7 %shard_map.231 = (bf16[32,2048]{1,0:T(8,128)(2,1)S(1)}, f32[4,512]{1,0:T(4,128)}, f32[1,4]{1,0:T(1,128)}, f32[4,512]{1,0:T(4,128)S(1)}, f32[4,512]{1,0:T(4,128)S(1)}, /*index=5*/f32[4,512]{1,0:T(4,128)S(1)}) custom-call(s32[1]{0:T(128)} %bitcast.me_ref, bf16[32,384]{1,0:T(8,128)(2,1)S(1)} %reshape.71.parts_ref, f32[8,32]{1,0:T(8,128)S(1)} %get-tuple-element.34.pre_ref, ...), custom_call_target="tpu_custom_call" | custom-call | flops 10000000 | bytes 1000000 | tf_op jit(solution)/shard_map/pallas_call | solution.py:397
  31.5 0.7 %reshape.74 = bf16[32,2,1024]{2,1,0:T(2,128)(2,1)} reshape(bf16[32,2048]{1,0:T(8,128)(2,1)S(1)} %get-tuple-element.40) | data formatting | bytes 262144 | tf_op jit(solution)/shard_map/reshape | solution.py:27
  32.2 2.6 %all-to-all-start.2 = ((bf16[32,2,1024]{2,1,0:T(2,128)(2,1)}), bf16[32,2,1024]{2,1,0:T(2,128)(2,1)S(1)}, u32[]{:S(2)}, u32[]{:S(2)}) async-start(bf16[32,2,1024]{2,1,0:T(2,128)(2,1)} %reshape.74), calls=%async_computation.2 | async-start | bytes 262144 | tf_op jit(solution)/shard_map/all_to_all | solution.py:28
  35.5 0.9 %shard_map.232 = (bf16[5,32,32]{2,1,0:T(8,128)(2,1)S(1)}, bf16[8,32]{1,0:T(8,128)(2,1)S(1)}, bf16[32,8]{1,0:T(8,128)(2,1)S(1)}, f32[32,1]{1,0:T(8,128)S(1)}) custom-call(s32[1]{0:T(128)} %bitcast.me_ref, s32[1]{0:T(128)S(6)} %copy.28.group_ref, s32[2]{0:T(128)S(1)} %bitcast.32, f32[1]{0:T(128)S(6)} %copy.29.group_weight, f32[2]{0:T(128)S(1)} %bitcast.33, ...), custom_call_target="tpu_custom_call" | custom-call | flops 10000000 | bytes 1000000 | tf_op jit(solution)/shard_map/pallas_call | solution.py:415
  36.4 6.7 %all-to-all-done.2 = bf16[32,2,1024]{2,1,0:T(2,128)(2,1)S(1)} async-done(((bf16[32,2,1024]{2,1,0:T(2,128)(2,1)}), bf16[32,2,1024]{2,1,0:T(2,128)(2,1)S(1)}, u32[]{:S(2)}, u32[]{:S(2)}) %all-to-all-start.2) | async-done | bytes 131104 | tf_op jit(solution)/shard_map/all_to_all | solution.py:28
  43.1 0.4 shard_map.233
  43.6 9.0 %all_to_all.25 = bf16[32,2,160]{2,1,0:T(2,128)(2,1)S(1)} all-to-all(bf16[32,2,160]{2,1,0:T(2,128)(2,1)S(1)} %reshape.77), channel_id=1, replica_groups=mesh['ep'=32] {'ep'}, dimensions={0} | all-to-all | bytes 40960 | tf_op jit(solution)/shard_map/all_to_all | solution.py:28
  52.6 5.1 %shard_map.234 = (bf16[32,2048]{1,0:T(8,128)(2,1)S(1)}, f32[1,2048]{1,0:T(1,128)S(1)}) custom-call(bf16[32,320]{1,0:T(8,128)(2,1)S(1)} %reshape.78.in_ref, bf16[32,2048]{1,0:T(8,128)(2,1)S(1)} %bitcast.26, bf16[8,32]{1,0:T(8,128)(2,1)S(1)} %get-tuple-element.42.mine_ref, bf16[32,8]{1,0:T(8,128)(2,1)S(1)} %get-tuple-element.43.spread_ref, ...), custom_call_target="tpu_custom_call" | custom-call | flops 10000000 | bytes 1000000 | tf_op jit(solution)/shard_map/pallas_call | solution.py:429
  57.8 0.7 %reshape.82 = bf16[32,2,1024]{2,1,0:T(2,128)(2,1)} reshape(bf16[32,2048]{1,0:T(8,128)(2,1)S(1)} %get-tuple-element.44) | data formatting | bytes 262144 | tf_op jit(solution)/shard_map/reshape | solution.py:27
  58.5 2.6 %all-to-all-start.4 = ((bf16[32,2,1024]{2,1,0:T(2,128)(2,1)}), bf16[32,2,1024]{2,1,0:T(2,128)(2,1)S(1)}, u32[]{:S(2)}, u32[]{:S(2)}) async-start(bf16[32,2,1024]{2,1,0:T(2,128)(2,1)} %reshape.82), calls=%async_computation.4 | async-start | bytes 262144 | tf_op jit(solution)/shard_map/all_to_all | solution.py:28
  61.1 4.0 %multiply_add_fusion = f32[1,4,512,512]{3,2,1,0:T(8,128)} fusion(f32[1,4,512,512]{3,2,1,0:T(8,128)} %param.30, f32[4,512]{1,0:T(4,128)S(1)} %get-tuple-element.49, f32[4,512]{1,0:T(4,128)S(1)} %get-tuple-element.48, f32[4,512]{1,0:T(4,128)S(1)} %get-tuple-element.47), kind=kLoop, calls=%fused_computation | loop fusion | flops 3145728 | bytes 8413184 | tf_op jit(solution)/shard_map/add | solution.py:413
  65.0 4.3 %all-to-all-done.4 = bf16[32,2,1024]{2,1,0:T(2,128)(2,1)S(1)} async-done(((bf16[32,2,1024]{2,1,0:T(2,128)(2,1)}), bf16[32,2,1024]{2,1,0:T(2,128)(2,1)S(1)}, u32[]{:S(2)}, u32[]{:S(2)}) %all-to-all-start.4) | async-done | bytes 131104 | tf_op jit(solution)/shard_map/all_to_all | solution.py:28
  69.3 0.7 %shard_map.235 = bf16[1,2048]{1,0:T(2,128)(2,1)} custom-call(bf16[32,2048]{1,0:T(8,128)(2,1)S(1)} %bitcast.28, f32[32,1]{1,0:T(8,128)S(1)} %get-tuple-element.45.weight_ref, f32[1,2048]{1,0:T(1,128)S(1)} %get-tuple-element.46.middle_ref), custom_call_target="tpu_custom_call" | custom-call | flops 10000000 | bytes 1000000 | tf_op jit(solution)/shard_map/pallas_call | solution.py:448
  (16 shorter events, 0.4 us)
Async XLA Ops:
  2.1 15.5 %all-to-all-start = ((bf16[32,2,1024]{2,1,0:T(2,128)(2,1)}), bf16[32,2,1024]{2,1,0:T(2,128)(2,1)S(1)}, u32[]{:S(2)}, u32[]{:S(2)}) async-start(bf16[32,2,1024]{2,1,0:T(2,128)(2,1)} %broadcast_in_dim.29), calls=%async_computation | async-start | bytes 262144 | tf_op jit(solution)/shard_map/all_to_all | solution.py:28
  10.1 0.7 copy-start.2
  18.9 9.8 %all-to-all-start.1 = ((bf16[32,2,192]{2,1,0:T(2,128)(2,1)}), bf16[32,2,192]{2,1,0:T(2,128)(2,1)S(1)}, u32[]{:S(2)}, u32[]{:S(2)}) async-start(bf16[32,2,192]{2,1,0:T(2,128)(2,1)} %reshape.70), calls=%async_computation.1 | async-start | bytes 65536 | tf_op jit(solution)/shard_map/all_to_all | solution.py:28
  23.1 12.3 %copy-start.3 = (s32[1,2]{1,0:T(1,128)S(1)}, s32[1,2]{1,0:T(1,128)}, u32[]{:S(2)}) copy-start(s32[1,2]{1,0:T(1,128)} %param.39) | copy-start | bytes 28
  23.1 12.3 %copy-start.4 = (f32[1,2]{1,0:T(1,128)S(1)}, f32[1,2]{1,0:T(1,128)}, u32[]{:S(2)}) copy-start(f32[1,2]{1,0:T(1,128)} %param.41) | copy-start | bytes 28
  23.2 19.9 %copy-start = (bf16[2048,64]{0,1:T(8,128)(2,1)S(1)}, bf16[2048,64]{0,1:T(8,128)(2,1)}, u32[]{:S(2)}) copy-start(bf16[2048,64]{0,1:T(8,128)(2,1)} %param.33) | copy-start | bytes 786436
  23.2 29.5 %copy-start.1 = (f32[2048]{0:T(1024)S(1)}, f32[2048]{0:T(1024)}, u32[]{:S(2)}) copy-start(f32[2048]{0:T(1024)} %param.34) | copy-start | bytes 24580
  32.2 10.8 %all-to-all-start.2 = ((bf16[32,2,1024]{2,1,0:T(2,128)(2,1)}), bf16[32,2,1024]{2,1,0:T(2,128)(2,1)S(1)}, u32[]{:S(2)}, u32[]{:S(2)}) async-start(bf16[32,2,1024]{2,1,0:T(2,128)(2,1)} %reshape.74), calls=%async_computation.2 | async-start | bytes 262144 | tf_op jit(solution)/shard_map/all_to_all | solution.py:28
  58.5 10.8 %all-to-all-start.4 = ((bf16[32,2,1024]{2,1,0:T(2,128)(2,1)}), bf16[32,2,1024]{2,1,0:T(2,128)(2,1)S(1)}, u32[]{:S(2)}, u32[]{:S(2)}) async-start(bf16[32,2,1024]{2,1,0:T(2,128)(2,1)} %reshape.82), calls=%async_computation.4 | async-start | bytes 262144 | tf_op jit(solution)/shard_map/all_to_all | solution.py:28

commit v3 on v2

--- a/solution.py
+++ b/solution.py
@@ -10,6 +10,7 @@
 LANES = 128
 SLOTS = 8
 MIB = 1 << 20
+AHEAD = 2_000_000_000
 F32 = jnp.float32
 BF16 = jnp.bfloat16
 NT = (((1,), (1,)), ((), ()))
@@ -87,60 +88,40 @@
     return jnp.sum(jnp.where(diagonal(n), spread, 0.0), axis=0, keepdims=True)
 
 
-def fetch_columns_body(
-    group_ref, member_ref, wq, wk, wv, wo, wi, wf, gain,
-    stacked, wi_out, wf_out, gain_out, ids_out, sems,
-):
-    columns = wq.shape[0]
-    copies = [
-        pltpu.make_async_copy(w, stacked.at[pl.ds(n * columns, columns)], sems.at[n])
-        for n, w in enumerate((wq, wk, wv, wo))
+def spread_body(me_ref, group_ref, weight_ref, row_ref, out_ref):
+    del me_ref, group_ref, weight_ref
+    out_ref[...] = jnp.broadcast_to(row_ref[...].astype(F32), out_ref.shape).astype(BF16)
+
+
+def columns_body(group_ref, member_ref, rows_ref, gain_ref, wq, wk, wv, wo, wi, wf, out_ref, pre_ref):
+    heads = wi.shape[0]
+    count = rows_ref.shape[0]
+    normed = root_norm(rows_ref[...].astype(F32), gain_ref[...]).astype(BF16)
+    cols = [
+        lax.dot_general(normed, w[...], NT, preferred_element_type=F32) for w in (wq, wk, wv, wo)
     ]
-    copies += [
-        pltpu.make_async_copy(a, b, sems.at[4 + n])
-        for n, (a, b) in enumerate(((wi, wi_out), (wf, wf_out), (gain, gain_out)))
-    ]
-    for c in copies:
-        c.start()
-    lane = lax.broadcasted_iota(jnp.int32, ids_out.shape, 1)
+    cols = jnp.concatenate(cols, axis=1).astype(BF16)
+    total = cols.shape[1]
+    out_ref[:, :total] = cols
+    lane = lax.broadcasted_iota(jnp.int32, (count, out_ref.shape[1] - total), 1)
     ids = jnp.where(lane == 0, group_ref[0], 0)
     for k in range(member_ref.shape[0]):
         ids = jnp.where(lane == 1 + k, member_ref[k], ids)
-    ids_out[...] = ids.astype(F32)
-    for c in copies:
-        c.wait()
-
-
-def fetch_cell_body(mem, norm, most, bias, mem_out, norm_out, most_out, bias_out, sems):
-    early = mem_out.shape[0]
-    copies = [
-        pltpu.make_async_copy(a, b, sems.at[n])
-        for n, (a, b) in enumerate(
-            ((mem.at[pl.ds(0, early)], mem_out), (norm, norm_out), (most, most_out), (bias, bias_out))
-        )
-    ]
-    for c in copies:
-        c.start()
-    for c in copies:
-        c.wait()
-
-
-def columns_body(rows_ref, ids_ref, gain_ref, stacked, wi, wf, out_ref, pre_ref):
-    heads = wi.shape[0]
-    count = rows_ref.shape[0]
-    total = stacked.shape[0]
-    normed = root_norm(rows_ref[...].astype(F32), gain_ref[...]).astype(BF16)
-    cols = lax.dot_general(normed, stacked[...], NT, preferred_element_type=F32)
-    out_ref[:, :total] = cols.astype(BF16)
-    out_ref[:, total:] = jnp.broadcast_to(ids_ref[...], (count, ids_ref.shape[1])).astype(BF16)
+    out_ref[:, total:] = ids.astype(F32).astype(BF16)
     pre_ref[:heads, :] = lax.dot_general(wi[...], normed, NT, preferred_element_type=F32)
     pre_ref[heads:, :] = lax.dot_general(wf[...], normed, NT, preferred_element_type=F32)
 
 
 def tables_body(
-    me_ref, group_ref, member_ref, group_weight, member_weight, parts_ref,
-    take_ref, mine_ref, spread_ref, weight_ref,
+    me_ref, group_ref, member_ref, group_weight, member_weight, parts_ref, norm_ref, max_ref, gate_ref,
+    take_ref, mine_ref, spread_ref, weight_ref, norm_out, max_out, early_ref,
+    sem,
 ):
+    fetch = pltpu.make_async_copy(gate_ref.at[pl.ds(0, early_ref.shape[0])], early_ref, sem)
+    fetch.start()
+    norm_out[...] = norm_ref[...]
+    max_out[...] = max_ref[...]
+
     count = parts_ref.shape[0]
     members = count // GROUPS
     picks = member_ref.shape[0]
@@ -180,18 +161,16 @@
             spread = jnp.where(lane == s, to_column(row), spread)
     mine_ref[...] = mine.astype(BF16)
     spread_ref[...] = spread.astype(BF16)
+    fetch.wait()
 
 
 def cell_body(
-    me_ref, parts_ref, pre_ref, max_ref, bias_ref, norm_ref, early_ref, mem_ref,
+    me_ref, parts_ref, pre_ref, max_ref, bias_ref, norm_ref, mem_ref,
     gated_ref, norm_out, max_out, value_out, key_out, keep_out,
     mem, wide, tall, sems,
 ):
     heads, head_dim = norm_ref.shape
-    early = early_ref.shape[0]
-    copies = [
-        pltpu.make_async_copy(mem_ref.at[early + h], mem.at[h], sems.at[h]) for h in range(heads - early)
-    ]
+    copies = [pltpu.make_async_copy(mem_ref.at[h], mem.at[h], sems.at[h]) for h in range(heads)]
     for c in copies:
         c.start()
 
@@ -236,11 +215,8 @@
     left = jnp.concatenate([query, jnp.zeros((8 - heads, head_dim), F32)], axis=0) if heads < 8 else query
     left = left.astype(BF16)
     for h in range(heads):
-        if h < early:
-            block = early_ref[h]
-        else:
-            copies[h - early].wait()
-            block = mem[h - early]
+        copies[h].wait()
+        block = mem[h]
         high = block.astype(BF16)
         low = (block - high.astype(F32)).astype(BF16)
         carried = lax.dot_general(left, high, NT, preferred_element_type=F32)
@@ -253,7 +229,8 @@
         ).astype(BF16)
 
 
-def project_body(gated_ref, weight_ref, take_ref, out_ref):
+def project_body(gated_ref, weight_ref, take_ref, done_ref, out_ref):
+    del done_ref
     proj = lax.dot_general(gated_ref[...], weight_ref[...], NT, preferred_element_type=F32).astype(BF16)
     blocks = [
         jnp.dot(take_ref[s], proj, preferred_element_type=F32) for s in range(take_ref.shape[0])
@@ -262,29 +239,32 @@
 
 
 def expert_body(
-    in_ref, rows_ref, mine_ref, spread_ref, gain_ref, gate_ref, up_ref, down_ref,
+    in_ref, rows_ref, mine_ref, spread_ref, gain_ref, early_ref, gate_ref, up_ref, down_ref,
     out_ref, middle_ref,
     gate, up, down, wide, tall, sems,
 ):
     width, hidden_dim = gate_ref.shape
     steps = sems.shape[1]
+    here = early_ref.shape[0] * steps // width
     wide_step = width // steps
     tall_step = hidden_dim // steps
-    plan = []
-    for n, (src, dst, step) in enumerate(
-        ((gate_ref, gate, wide_step), (up_ref, up, wide_step), (down_ref, down, tall_step))
-    ):
-        plan.append([
-            pltpu.make_async_copy(
-                src.at[pl.ds(k * step, step)], dst.at[pl.ds(k * step, step)], sems.at[n, k]
-            )
-            for k in range(steps)
-        ])
+
+    def chunk(n, src, dst, k, step, skip=0):
+        return pltpu.make_async_copy(
+            src.at[pl.ds(k * step, step)], dst.at[pl.ds(k * step - skip, step)], sems.at[n, k]
+        )
+
+    gates = [None] * here + [
+        chunk(0, gate_ref, gate, k, wide_step, early_ref.shape[0]) for k in range(here, steps)
+    ]
+    ups = [chunk(1, up_ref, up, k, wide_step) for k in range(steps)]
+    downs = [chunk(2, down_ref, down, k, tall_step) for k in range(steps)]
     for k in range(steps):
-        plan[0][k].start()
-        plan[1][k].start()
+        ups[k].start()
+        if k >= here:
+            gates[k].start()
     for k in range(steps):
-        plan[2][k].start()
+        downs[k].start()
 
     used = CAPACITY + 1
     columns = in_ref.shape[1] // used
@@ -301,19 +281,21 @@
     middle_ref[...] = middle[CAPACITY:CAPACITY + 1]
     left = root_norm(middle, gain_ref[...]).astype(BF16)
 
-    gate_part = jnp.zeros((SLOTS, hidden_dim), F32)
+    gate_part = jnp.dot(left[:, :here * wide_step], early_ref[...], preferred_element_type=F32)
     up_part = jnp.zeros((SLOTS, hidden_dim), F32)
     for k in range(steps):
         part = slice(k * wide_step, (k + 1) * wide_step)
-        plan[0][k].wait()
-        gate_part += jnp.dot(left[:, part], gate[part, :], preferred_element_type=F32)
-        plan[1][k].wait()
+        ups[k].wait()
         up_part += jnp.dot(left[:, part], up[part, :], preferred_element_type=F32)
+        if k >= here:
+            gates[k].wait()
+            block = gate[(k - here) * wide_step:(k - here + 1) * wide_step, :]
+            gate_part += jnp.dot(left[:, part], block, preferred_element_type=F32)
     hidden = (gate_part / (1.0 + jnp.exp(-gate_part)) * up_part).astype(BF16)
     result = jnp.zeros((SLOTS, width), F32)
     for k in range(steps):
         part = slice(k * tall_step, (k + 1) * tall_step)
-        plan[2][k].wait()
+        downs[k].wait()
         result += jnp.dot(hidden[:, part], down[part, :], preferred_element_type=F32)
     out_ref[...] = jnp.dot(
         spread_ref[...], result.astype(BF16), preferred_element_type=F32
@@ -354,84 +336,74 @@
     heads, head_dim = memory_norm.shape[1:]
     hidden_dim = expert_gate.shape[2]
     assert tokens.shape[0] == 1 and expert_gate.shape[0] == 1
-    me = lax.axis_index("ep").astype(jnp.int32)
+    me = lax.axis_index("ep").astype(jnp.int32)[None]
 
     ids = (route_group, route_member.reshape(-1))
 
-    rows = exchange(jnp.broadcast_to(tokens, (devices, width)))
-
-    stacked, wi, wf, gain, id_row = call(
-        fetch_columns_body,
-        (
-            shaped((4 * columns, width), BF16), shaped((heads, width), BF16),
-            shaped((heads, width), BF16), shaped((1, width)), shaped((1, LANES)),
-        ),
-        [SMEM_SPEC] * 2 + [HBM_SPEC] * 7,
-        [pltpu.SemaphoreType.DMA((7,))],
-        limit=4 * MIB,
-    )(
-        *ids, in_hbm(query_weight.T), in_hbm(key_weight.T), in_hbm(value_weight.T),
-        in_hbm(outgate_weight.T), in_hbm(input_weight.T), in_hbm(forget_weight.T),
-        in_hbm(mixer_gain[None]),
-    )
+    row = call(spread_body, shaped((devices, width), BF16), [SMEM_SPEC] * 3 + [VMEM_SPEC], flops=AHEAD)(
+        me, route_group, group_weight, tokens
+    )
+    rows = exchange(row)
+
     cols, pre = call(
         columns_body,
         (shaped((devices, 4 * columns + LANES), BF16), shaped((2 * heads, devices))),
-        [VMEM_SPEC] * 6,
-    )(rows, id_row, gain, stacked, wi, wf)
+        [SMEM_SPEC] * 2 + [VMEM_SPEC] * 8,
+        flops=AHEAD,
+    )(
+        *ids, rows, mixer_gain[None], query_weight.T, key_weight.T, value_weight.T, outgate_weight.T,
+        input_weight.T, forget_weight.T,
+    )
     parts = exchange(cols)
 
     memory = memory_matrix.reshape(heads, head_dim, head_dim)
     tiles = width // LANES
-    early = heads // 2
-    early_memory, norm, most, bias = call(
-        fetch_cell_body,
-        (
-            shaped((early, head_dim, head_dim)), shaped((heads, head_dim)),
-            shaped((1, heads)), shaped((1, heads)),
-        ),
-        [HBM_SPEC] * 4,
-        [pltpu.SemaphoreType.DMA((4,))],
-        limit=24 * MIB,
-    )(in_hbm(lax.optimization_barrier((memory, pre))[0]), in_hbm(memory_norm.reshape(heads, head_dim)), in_hbm(memory_max), in_hbm(forget_bias[None]))
     gated, next_norm, next_max, value, key, keep = call(
         cell_body,
         (
             shaped((devices, width), BF16), shaped((heads, head_dim)), shaped((1, heads)),
             shaped((heads, head_dim)), shaped((heads, head_dim)), shaped((heads, head_dim)),
         ),
-        [SMEM_SPEC] + [VMEM_SPEC] * 6 + [HBM_SPEC],
+        [SMEM_SPEC] + [VMEM_SPEC] * 5 + [HBM_SPEC],
         [
-            pltpu.VMEM((heads - early, head_dim, head_dim), F32),
+            pltpu.VMEM((heads, head_dim, head_dim), F32),
             pltpu.VMEM((pl.cdiv(4 * columns, LANES), devices, LANES), F32),
             pltpu.VMEM((4 * tiles, LANES), F32),
-            pltpu.SemaphoreType.DMA((heads - early,)),
+            pltpu.SemaphoreType.DMA((heads,)),
         ],
-        limit=24 * MIB,
-    )(me[None], parts, pre, most, bias, norm, early_memory, in_hbm(memory))
+        limit=12 * MIB,
+        flops=AHEAD,
+    )(
+        me, parts, pre, memory_max, forget_bias[None], memory_norm.reshape(heads, head_dim),
+        in_hbm(memory),
+    )
     gated_rows = exchange(gated)
+
     next_matrix = keep[:, :, None] * memory + value[:, :, None] * key[:, None, :]
-
-    take, mine, spread, weights = call(
+    next_matrix = lax.optimization_barrier(next_matrix[None])
+    gate = in_hbm(expert_gate.reshape(width, hidden_dim))
+    take, mine, spread, weights, next_norm, next_max, early = call(
         tables_body,
         (
             shaped((CAPACITY + 1, devices, devices), BF16), shaped((SLOTS, devices), BF16),
             shaped((devices, SLOTS), BF16), shaped((devices, 1)),
+            shaped((heads, head_dim)), shaped((1, heads)), shaped((width // 2, hidden_dim), BF16),
         ),
-        [SMEM_SPEC] * 5 + [VMEM_SPEC],
-    )(me[None], *ids, group_weight, member_weight.reshape(-1), parts)
+        [SMEM_SPEC] * 5 + [VMEM_SPEC] * 3 + [HBM_SPEC],
+        [pltpu.SemaphoreType.DMA],
+    )(me, *ids, group_weight, member_weight.reshape(-1), parts, next_norm, next_max, gate)
 
     outgoing = call(
-        project_body, shaped((devices, (CAPACITY + 1) * columns), BF16), [VMEM_SPEC] * 3
-    )(gated_rows, mixer_out.T, take)
+        project_body, shaped((devices, (CAPACITY + 1) * columns), BF16), [VMEM_SPEC] * 3 + [HBM_SPEC],
+    )(gated_rows, mixer_out.T, take, in_hbm(next_matrix))
     incoming = exchange(outgoing)
 
     back, middle = call(
         expert_body,
         (shaped((devices, width), BF16), shaped((1, width))),
-        [VMEM_SPEC] * 5 + [HBM_SPEC] * 3,
+        [VMEM_SPEC] * 6 + [HBM_SPEC] * 3,
         [
-            pltpu.VMEM((width, hidden_dim), BF16),
+            pltpu.VMEM((width - width // 2, hidden_dim), BF16),
             pltpu.VMEM((width, hidden_dim), BF16),
             pltpu.VMEM((hidden_dim, width), BF16),
             pltpu.VMEM((pl.cdiv((CAPACITY + 1) * columns, LANES), devices, LANES), F32),
@@ -440,13 +412,13 @@
         ],
         limit=24 * MIB,
     )(
-        incoming, rows, mine, spread, expert_gain[None],
-        in_hbm(expert_gate.reshape(width, hidden_dim)), in_hbm(expert_up.reshape(width, hidden_dim)),
+        incoming, rows, mine, spread, expert_gain[None], early, gate,
+        in_hbm(expert_up.reshape(width, hidden_dim)),
         in_hbm(expert_down.reshape(hidden_dim, width)),
     )
     returned = exchange(back)
     layer_out = call(finish_body, shaped((1, width), BF16), [VMEM_SPEC] * 3)(returned, weights, middle)
-    return (layer_out, next_matrix[None], next_norm[None], next_max)
+    return (layer_out, next_matrix, next_norm[None], next_max)
 
 
 def solution(mesh):

time: 70.5 us -> 70.9 us (level)
  blocking collectives: 8.95 us -> 45.7 us
  waiting for transfers between devices: 21.6 us -> 1.47 us
  starting transfers between devices: 15 us -> 2.57 us
  local copies, waits for them, and re-layouts: 3.96 us -> 2.13 us
  Pallas kernels: 13.7 us -> 12.4 us
  other arithmetic: 4.68 us -> 3.96 us
    all_to_all x1 -> x4, blocking collectives: 8.95 us -> 45.7 us  [exchange(): lax.all_to_all(halves, 'ep', split_axis=0, concat_axis=0, tiled=True)]
    all_to_all x4 -> x1, waiting for transfers between devices: 21.6 us -> 1.47 us  [exchange(): lax.all_to_all(halves, 'ep', split_axis=0, concat_axis=0, tiled=True)]
    all_to_all x4 -> x1, starting transfers between devices: 15 us -> 2.57 us  [exchange(): lax.all_to_all(halves, 'ep', split_axis=0, concat_axis=0, tiled=True)]
    pallas_call x2 -> x1, Pallas kernels: 3.43 us -> 0.01 us  [local(): call(spread_body, shaped((devices, width), BF16), [SMEM_SPEC] * 3 + [VMEM...]
    pallas_call x1, Pallas kernels: 0.87 us -> 2.75 us  [local(): call(tables_body, (shaped((CAPACITY + 1, devices, devices), BF16), shaped...]
    reshape x4 -> x5, local copies, waits for them, and re-layouts: 2.28 us -> 1.12 us  [exchange(): halves = blocks.reshape(count, 2, width // 2)]
    broadcast_in_dim x2 -> x0, local copies, waits for them, and re-layouts: 0.74 us -> none  [local(): rows = exchange(jnp.broadcast_to(tokens, (devices, width)))]
    unnamed x1 -> x0, other arithmetic: 0.73 us -> none
  transfers between devices with their start and end apart: 4 -> 1, of which waited for: 4 -> 1; matrix products, arithmetic and copies ran while one was open for 6% -> 6% of each run, Pallas kernels for 6% -> 4%
where the time goes in v3:
time: 70.9 us; the launch traced here: 70.6 us
  blocking collectives  45.7 us (64%)
  Pallas kernels  12.4 us (17%)
  other arithmetic  3.96 us (6%)
  starting transfers between devices  2.57 us (4%)
  between operations  2.29 us (3%)
  local copies, waits for them, and re-layouts  2.13 us (3%)
  waiting for transfers between devices  1.47 us (2%)
    all_to_all x4, blocking collectives, exchange(): lax.all_to_all(halves, 'ep', split_axis=0, concat_axis=0, tiled=True)  45.7 us
    pallas_call x1, Pallas kernels, local(): call(expert_body, (shaped((devices, width), BF16), shaped((1, width))), [...  4.52 us
    add x1, other arithmetic, local(): keep[:, :, None] * memory + value[:, :, None] * key[:, None, :]  3.96 us
    pallas_call x1, Pallas kernels, local(): call(cell_body, (shaped((devices, width), BF16), shaped((heads, head_dim)...  2.97 us
    pallas_call x1, Pallas kernels, local(): call(tables_body, (shaped((CAPACITY + 1, devices, devices), BF16), shaped...  2.75 us
    all_to_all x1, starting transfers between devices, exchange(): lax.all_to_all(halves, 'ep', split_axis=0, concat_axis=0, tiled=True)  2.57 us
    all_to_all x1, waiting for transfers between devices, exchange(): lax.all_to_all(halves, 'ep', split_axis=0, concat_axis=0, tiled=True)  1.47 us
  transfers between devices with their start and end apart: 1, of which 1 were waited for; matrix products, arithmetic and copies ran while one was open for 6% of the time, Pallas kernels for 4%

profile of v3, /device:TPU:0, one launch (start us, length us, event | category | flops | bytes accessed | tf_op | source)
XLA Modules:
  0.0 70.6 jit_solution(13101036774637918404)
XLA Ops:
  2.1 0.7 copy-done.10
  2.8 0.0 copy-start.12
  2.8 0.0 copy-start.13
  2.8 0.0 copy-start.14
  2.8 0.1 reshape.66
  2.9 15.3 %all_to_all.25 = bf16[32,2,1024]{2,1,0:T(2,128)(2,1)S(1)} all-to-all(bf16[32,2,1024]{2,1,0:T(2,128)(2,1)S(1)} %reshape.66), channel_id=1, replica_groups=mesh['ep'=32] {'ep'}, dimensions={0} | all-to-all | bytes 262144 | tf_op jit(solution)/shard_map/all_to_all | solution.py:29
  18.4 1.0 %shard_map.229 = (bf16[32,384]{1,0:T(8,128)(2,1)S(1)}, f32[8,32]{1,0:T(8,128)S(1)}) custom-call(s32[1]{0:T(128)S(6)} %copy.28.group_ref, s32[2]{0:T(128)S(1)} %bitcast.31, bf16[32,2048]{1,0:T(8,128)(2,1)S(1)} %bitcast.25, f32[1,2048]{1,0:T(1,128)S(1)} %bitcast.40, bf16[64,2048]{1,0:T(8,128)(2,1)S(1)} %bitcast.34, bf16[64,2048]{1,0:T(8,128)(2,1)S(1)} %bitcast.35, ...), custom_call_target="tpu_custom_call" | custom-call | flops 2000000000 | bytes 1000000 | tf_op jit(solution)/shard_map/pallas_call | solution.py:348
  19.4 0.1 reshape.68
  19.6 9.0 %all_to_all.26 = bf16[32,2,192]{2,1,0:T(2,128)(2,1)S(1)} all-to-all(bf16[32,2,192]{2,1,0:T(2,128)(2,1)S(1)} %reshape.68), channel_id=1, replica_groups=mesh['ep'=32] {'ep'}, dimensions={0} | all-to-all | bytes 49152 | tf_op jit(solution)/shard_map/all_to_all | solution.py:29
  28.6 0.1 reshape.69.parts_ref
  28.7 3.0 %shard_map.230 = (bf16[32,2048]{1,0:T(8,128)(2,1)S(1)}, f32[4,512]{1,0:T(4,128)S(1)}, f32[1,4]{1,0:T(1,128)S(1)}, f32[4,512]{1,0:T(4,128)S(1)}, f32[4,512]{1,0:T(4,128)S(1)}, /*index=5*/f32[4,512]{1,0:T(4,128)S(1)}) custom-call(s32[1]{0:T(128)} %bitcast.me_ref, bf16[32,384]{1,0:T(8,128)(2,1)S(1)} %reshape.69.parts_ref, ...), custom_call_target="tpu_custom_call" | custom-call | flops 2000000000 | bytes 1000000 | tf_op jit(solution)/shard_map/pallas_call | solution.py:361
  31.7 0.7 %reshape.72 = bf16[32,2,1024]{2,1,0:T(2,128)(2,1)} reshape(bf16[32,2048]{1,0:T(8,128)(2,1)S(1)} %get-tuple-element.23) | data formatting | bytes 262144 | tf_op jit(solution)/shard_map/reshape | solution.py:28
  32.4 2.6 %all-to-all-start.2 = ((bf16[32,2,1024]{2,1,0:T(2,128)(2,1)}), bf16[32,2,1024]{2,1,0:T(2,128)(2,1)S(1)}, u32[]{:S(2)}, u32[]{:S(2)}) async-start(bf16[32,2,1024]{2,1,0:T(2,128)(2,1)} %reshape.72), calls=%async_computation.2 | async-start | bytes 262144 | tf_op jit(solution)/shard_map/all_to_all | solution.py:29
  35.0 4.0 %multiply_add_fusion.done_ref = f32[1,4,512,512]{3,2,1,0:T(8,128)} fusion(f32[1,4,512,512]{3,2,1,0:T(8,128)} %param.30, f32[4,512]{1,0:T(4,128)S(1)} %get-tuple-element.29, f32[4,512]{1,0:T(4,128)S(1)} %get-tuple-element.28, f32[4,512]{1,0:T(4,128)S(1)} %get-tuple-element.27), kind=kLoop, calls=%fused_computation | loop fusion | flops 3145728 | bytes 8413184 | tf_op jit(solution)/shard_map/add | solution.py:382
  39.0 2.7 %shard_map.231 = (bf16[5,32,32]{2,1,0:T(8,128)(2,1)S(1)}, bf16[8,32]{1,0:T(8,128)(2,1)S(1)}, bf16[32,8]{1,0:T(8,128)(2,1)S(1)}, f32[32,1]{1,0:T(8,128)S(1)}, f32...) custom-call(s32[1]{0:T(128)} %bitcast.me_ref, s32[1]{0:T(128)S(6)} %copy.28.group_ref, ...), custom_call_target="tpu_custom_call" | custom-call | flops 10000000 | bytes 1000000 | tf_op jit(solution)/shard_map/pallas_call | solution.py:385
  41.7 1.5 %all-to-all-done.2 = bf16[32,2,1024]{2,1,0:T(2,128)(2,1)S(1)} async-done(((bf16[32,2,1024]{2,1,0:T(2,128)(2,1)}), bf16[32,2,1024]{2,1,0:T(2,128)(2,1)S(1)}, u32[]{:S(2)}, u32[]{:S(2)}) %all-to-all-start.2) | async-done | bytes 131104 | tf_op jit(solution)/shard_map/all_to_all | solution.py:29
  43.2 0.4 shard_map.232
  43.7 0.1 reshape.76
  43.7 11.4 %all_to_all.27 = bf16[32,2,160]{2,1,0:T(2,128)(2,1)S(1)} all-to-all(bf16[32,2,160]{2,1,0:T(2,128)(2,1)S(1)} %reshape.76), channel_id=1, replica_groups=mesh['ep'=32] {'ep'}, dimensions={0} | all-to-all | bytes 40960 | tf_op jit(solution)/shard_map/all_to_all | solution.py:29
  55.2 0.1 reshape.77.in_ref
  55.3 4.5 %shard_map.233 = (bf16[32,2048]{1,0:T(8,128)(2,1)S(1)}, f32[1,2048]{1,0:T(1,128)S(1)}) custom-call(bf16[32,320]{1,0:T(8,128)(2,1)S(1)} %reshape.77.in_ref, bf16[32,2048]{1,0:T(8,128)(2,1)S(1)} %bitcast.26, bf16[8,32]{1,0:T(8,128)(2,1)S(1)} %get-tuple-element.30.mine_ref, bf16[32,8]{1,0:T(8,128)(2,1)S(1)} %get-tuple-element.31.spread_ref, ...), custom_call_target="tpu_custom_call" | custom-call | flops 10000000 | bytes 1000000 | tf_op jit(solution)/shard_map/pallas_call | solution.py:401
  59.8 0.1 reshape.80
  59.9 9.9 %all_to_all.28 = bf16[32,2,1024]{2,1,0:T(2,128)(2,1)S(1)} all-to-all(bf16[32,2,1024]{2,1,0:T(2,128)(2,1)S(1)} %reshape.80), channel_id=1, replica_groups=mesh['ep'=32] {'ep'}, dimensions={0} | all-to-all | bytes 262144 | tf_op jit(solution)/shard_map/all_to_all | solution.py:29
  69.8 0.7 %shard_map.234 = bf16[1,2048]{1,0:T(2,128)(2,1)} custom-call(bf16[32,2048]{1,0:T(8,128)(2,1)S(1)} %bitcast.28, f32[32,1]{1,0:T(8,128)S(1)} %get-tuple-element.34.weight_ref, f32[1,2048]{1,0:T(1,128)S(1)} %get-tuple-element.35.middle_ref), custom_call_target="tpu_custom_call" | custom-call | flops 10000000 | bytes 1000000 | tf_op jit(solution)/shard_map/pallas_call | solution.py:420
  (30 shorter events, 0.1 us)
Async XLA Ops:
  0.6 17.7 %copy-start.2 = (s32[1,2]{1,0:T(1,128)S(1)}, s32[1,2]{1,0:T(1,128)}, u32[]{:S(2)}) copy-start(s32[1,2]{1,0:T(1,128)} %param.39) | copy-start | bytes 28
  0.6 17.7 %copy-start.9 = (bf16[2048,4]{0,1:T(4,128)(2,1)S(1)}, bf16[2048,4]{0,1:T(4,128)(2,1)}, u32[]{:S(2)}) copy-start(bf16[2048,4]{0,1:T(4,128)(2,1)} %param.28) | copy-start | bytes 49156
  0.7 17.7 %copy-start.8 = (bf16[2048,4]{0,1:T(4,128)(2,1)S(1)}, bf16[2048,4]{0,1:T(4,128)(2,1)}, u32[]{:S(2)}) copy-start(bf16[2048,4]{0,1:T(4,128)(2,1)} %param.27) | copy-start | bytes 49156
  0.7 17.7 %copy-start.7 = (bf16[2048,64]{0,1:T(8,128)(2,1)S(1)}, bf16[2048,64]{0,1:T(8,128)(2,1)}, u32[]{:S(2)}) copy-start(bf16[2048,64]{0,1:T(8,128)(2,1)} %param.26) | copy-start | bytes 786436
  0.7 17.7 %copy-start.6 = (bf16[2048,64]{0,1:T(8,128)(2,1)S(1)}, bf16[2048,64]{0,1:T(8,128)(2,1)}, u32[]{:S(2)}) copy-start(bf16[2048,64]{0,1:T(8,128)(2,1)} %param.25) | copy-start | bytes 786436
  0.7 17.7 %copy-start.5 = (bf16[2048,64]{0,1:T(8,128)(2,1)S(1)}, bf16[2048,64]{0,1:T(8,128)(2,1)}, u32[]{:S(2)}) copy-start(bf16[2048,64]{0,1:T(8,128)(2,1)} %param.24) | copy-start | bytes 786436
  0.7 17.7 %copy-start.4 = (bf16[2048,64]{0,1:T(8,128)(2,1)S(1)}, bf16[2048,64]{0,1:T(8,128)(2,1)}, u32[]{:S(2)}) copy-start(bf16[2048,64]{0,1:T(8,128)(2,1)} %param.23) | copy-start | bytes 786436
  2.1 0.7 copy-start.10
  2.8 15.6 %copy-start.11 = (f32[2048]{0:T(1024)S(1)}, f32[2048]{0:T(1024)}, u32[]{:S(2)}) copy-start(f32[2048]{0:T(1024)} %param.22) | copy-start | bytes 24580
  2.8 25.9 %copy-start.12 = (f32[1,4,512]{2,1,0:T(4,128)S(1)}, f32[1,4,512]{2,1,0:T(4,128)}, u32[]{:S(2)}) copy-start(f32[1,4,512]{2,1,0:T(4,128)} %param.31) | copy-start | bytes 24580
  2.8 25.9 %copy-start.13 = (f32[1,4]{1,0:T(1,128)S(1)}, f32[1,4]{1,0:T(1,128)}, u32[]{:S(2)}) copy-start(f32[1,4]{1,0:T(1,128)} %max_ref.1) | copy-start | bytes 52
  2.8 25.9 %copy-start.14 = (f32[4]{0:T(128)S(1)}, f32[4]{0:T(128)}, u32[]{:S(2)}) copy-start(f32[4]{0:T(128)} %param.29) | copy-start | bytes 52
  32.4 10.8 %all-to-all-start.2 = ((bf16[32,2,1024]{2,1,0:T(2,128)(2,1)}), bf16[32,2,1024]{2,1,0:T(2,128)(2,1)S(1)}, u32[]{:S(2)}, u32[]{:S(2)}) async-start(bf16[32,2,1024]{2,1,0:T(2,128)(2,1)} %reshape.72), calls=%async_computation.2 | async-start | bytes 262144 | tf_op jit(solution)/shard_map/all_to_all | solution.py:29
  35.0 4.0 %copy-start.3 = (f32[1,2]{1,0:T(1,128)S(1)}, f32[1,2]{1,0:T(1,128)}, u32[]{:S(2)}) copy-start(f32[1,2]{1,0:T(1,128)} %param.41) | copy-start | bytes 28
  39.0 4.3 %copy-start = (bf16[2048,64]{0,1:T(8,128)(2,1)S(1)}, bf16[2048,64]{0,1:T(8,128)(2,1)}, u32[]{:S(2)}) copy-start(bf16[2048,64]{0,1:T(8,128)(2,1)} %param.33) | copy-start | bytes 786436
  39.0 16.3 %copy-start.1 = (f32[2048]{0:T(1024)S(1)}, f32[2048]{0:T(1024)}, u32[]{:S(2)}) copy-start(f32[2048]{0:T(1024)} %param.34) | copy-start | bytes 24580

commit v4 on v3

--- a/solution.py
+++ b/solution.py
@@ -34,13 +34,14 @@
 HBM_SPEC = pl.BlockSpec(memory_space=pltpu.HBM)
 
 
-def call(body, outs, ins, scratch=(), limit=8 * MIB, flops=10_000_000, moved=1_000_000):
+def call(body, outs, ins, scratch=(), outputs=None, aliases={}, limit=8 * MIB, flops=10_000_000, moved=1_000_000):
     return pl.pallas_call(
         body,
         out_shape=outs,
         in_specs=ins,
-        out_specs=jax.tree.map(lambda _: VMEM_SPEC, outs),
+        out_specs=outputs or jax.tree.map(lambda _: VMEM_SPEC, outs),
         scratch_shapes=scratch,
+        input_output_aliases=aliases,
         compiler_params=pltpu.CompilerParams(vmem_limit_bytes=limit),
         cost_estimate=pl.CostEstimate(flops=flops, bytes_accessed=moved, transcendentals=0),
     )
@@ -97,10 +98,8 @@
     heads = wi.shape[0]
     count = rows_ref.shape[0]
     normed = root_norm(rows_ref[...].astype(F32), gain_ref[...]).astype(BF16)
-    cols = [
-        lax.dot_general(normed, w[...], NT, preferred_element_type=F32) for w in (wq, wk, wv, wo)
-    ]
-    cols = jnp.concatenate(cols, axis=1).astype(BF16)
+    stacked = jnp.concatenate([w[...] for w in (wq, wk, wv, wo)], axis=0)
+    cols = lax.dot_general(normed, stacked, NT, preferred_element_type=F32).astype(BF16)
     total = cols.shape[1]
     out_ref[:, :total] = cols
     lane = lax.broadcasted_iota(jnp.int32, (count, out_ref.shape[1] - total), 1)
@@ -112,16 +111,46 @@
     pre_ref[heads:, :] = lax.dot_general(wf[...], normed, NT, preferred_element_type=F32)
 
 
-def tables_body(
-    me_ref, group_ref, member_ref, group_weight, member_weight, parts_ref, norm_ref, max_ref, gate_ref,
-    take_ref, mine_ref, spread_ref, weight_ref, norm_out, max_out, early_ref,
-    sem,
+def window_body(
+    me_ref, group_ref, member_ref, group_weight, member_weight, parts_ref, norm_ref, max_ref,
+    value_ref, key_ref, keep_ref, mem_ref, gate_ref, begun_ref,
+    take_ref, mine_ref, spread_ref, weight_ref, norm_out, max_out, early_ref, next_ref,
+    old, new, sems,
 ):
-    fetch = pltpu.make_async_copy(gate_ref.at[pl.ds(0, early_ref.shape[0])], early_ref, sem)
+    del begun_ref
+    late = old.shape[0]
+    first = next_ref.shape[0] - late
+    loads = [
+        pltpu.make_async_copy(mem_ref.at[first + h], old.at[h], sems.at[0, h]) for h in range(late)
+    ]
+    stores = [
+        pltpu.make_async_copy(new.at[h], next_ref.at[first + h], sems.at[1, h]) for h in range(late)
+    ]
+    fetch = pltpu.make_async_copy(gate_ref.at[pl.ds(0, early_ref.shape[0])], early_ref, sems.at[0, late])
+    for c in loads:
+        c.start()
     fetch.start()
     norm_out[...] = norm_ref[...]
     max_out[...] = max_ref[...]
-
+    slot_tables(
+        me_ref, group_ref, member_ref, group_weight, member_weight, parts_ref,
+        take_ref, mine_ref, spread_ref, weight_ref,
+    )
+    turned = columns_of(value_ref[...])
+    for h in range(late):
+        row = slice(first + h, first + h + 1)
+        loads[h].wait()
+        new[h] = keep_ref[row] * old[h] + turned[:, row] * key_ref[row]
+        stores[h].start()
+    fetch.wait()
+    for c in stores:
+        c.wait()
+
+
+def slot_tables(
+    me_ref, group_ref, member_ref, group_weight, member_weight, parts_ref,
+    take_ref, mine_ref, spread_ref, weight_ref,
+):
     count = parts_ref.shape[0]
     members = count // GROUPS
     picks = member_ref.shape[0]
@@ -161,16 +190,17 @@
             spread = jnp.where(lane == s, to_column(row), spread)
     mine_ref[...] = mine.astype(BF16)
     spread_ref[...] = spread.astype(BF16)
-    fetch.wait()
 
 
 def cell_body(
     me_ref, parts_ref, pre_ref, max_ref, bias_ref, norm_ref, mem_ref,
-    gated_ref, norm_out, max_out, value_out, key_out, keep_out,
-    mem, wide, tall, sems,
+    gated_ref, norm_out, max_out, value_out, key_out, keep_out, next_ref,
+    mem, new, wide, tall, sems,
 ):
     heads, head_dim = norm_ref.shape
-    copies = [pltpu.make_async_copy(mem_ref.at[h], mem.at[h], sems.at[h]) for h in range(heads)]
+    first = new.shape[0]
+    copies = [pltpu.make_async_copy(mem_ref.at[h], mem.at[h], sems.at[0, h]) for h in range(heads)]
+    stores = [pltpu.make_async_copy(new.at[h], next_ref.at[h], sems.at[1, h]) for h in range(first)]
     for c in copies:
         c.start()
 
@@ -212,25 +242,43 @@
     keep_out[...] = jnp.broadcast_to(keep, keep_out.shape)
 
     count = gated_ref.shape[0]
-    left = jnp.concatenate([query, jnp.zeros((8 - heads, head_dim), F32)], axis=0) if heads < 8 else query
-    left = left.astype(BF16)
+    ones = jnp.ones((8, LANES), BF16)
+    turned = columns_of(admit * value)
     for h in range(heads):
         copies[h].wait()
-        block = mem[h]
-        high = block.astype(BF16)
-        low = (block - high.astype(F32)).astype(BF16)
-        carried = lax.dot_general(left, high, NT, preferred_element_type=F32)
-        carried = carried + lax.dot_general(left, low, NT, preferred_element_type=F32)
-        carried = carried[h:h + 1]
-        numer = keep[h:h + 1] * carried + score[h:h + 1] * value[h:h + 1]
+        sums = []
+        for r in range(0, head_dim, LANES):
+            block = mem[h, r:r + LANES, :]
+            product = block * query[h:h + 1]
+            sums.append(sum(product[:, p * LANES:(p + 1) * LANES] for p in range(tiles)))
+            if h < first:
+                new[h, r:r + LANES, :] = (
+                    keep[h:h + 1] * block + turned[r:r + LANES, h:h + 1] * key[h:h + 1]
+                )
+        if h < first:
+            stores[h].start()
+        sums = jnp.concatenate(sums, axis=0)
+        high = sums.astype(BF16)
+        low = (sums - high.astype(F32)).astype(BF16)
+        carried = lax.dot_general(ones, high, NT, preferred_element_type=F32)
+        carried = carried + lax.dot_general(ones, low, NT, preferred_element_type=F32)
+        numer = keep[h:h + 1] * carried[:1] + score[h:h + 1] * value[h:h + 1]
         gated = numer * scale[h:h + 1] * opened[h:h + 1]
         gated_ref[:, h * head_dim:(h + 1) * head_dim] = jnp.broadcast_to(
             gated, (count, head_dim)
         ).astype(BF16)
-
-
-def project_body(gated_ref, weight_ref, take_ref, done_ref, out_ref):
-    del done_ref
+    for c in stores:
+        c.wait()
+
+
+def columns_of(value):
+    heads = value.shape[0]
+    if heads < 8:
+        value = jnp.concatenate([value, jnp.zeros((8 - heads, value.shape[1]), F32)], axis=0)
+    return value.T
+
+
+def project_body(gated_ref, weight_ref, take_ref, out_ref):
     proj = lax.dot_general(gated_ref[...], weight_ref[...], NT, preferred_element_type=F32).astype(BF16)
     blocks = [
         jnp.dot(take_ref[s], proj, preferred_element_type=F32) for s in range(take_ref.shape[0])
@@ -358,20 +406,24 @@
 
     memory = memory_matrix.reshape(heads, head_dim, head_dim)
     tiles = width // LANES
-    gated, next_norm, next_max, value, key, keep = call(
+    first = heads // 2
+    gated, next_norm, next_max, value, key, keep, begun = call(
         cell_body,
         (
             shaped((devices, width), BF16), shaped((heads, head_dim)), shaped((1, heads)),
             shaped((heads, head_dim)), shaped((heads, head_dim)), shaped((heads, head_dim)),
+            shaped((heads, head_dim, head_dim)),
         ),
         [SMEM_SPEC] + [VMEM_SPEC] * 5 + [HBM_SPEC],
         [
             pltpu.VMEM((heads, head_dim, head_dim), F32),
+            pltpu.VMEM((first, head_dim, head_dim), F32),
             pltpu.VMEM((pl.cdiv(4 * columns, LANES), devices, LANES), F32),
             pltpu.VMEM((4 * tiles, LANES), F32),
-            pltpu.SemaphoreType.DMA((heads,)),
+            pltpu.SemaphoreType.DMA((2, heads)),
         ],
-        limit=12 * MIB,
+        outputs=[VMEM_SPEC] * 6 + [HBM_SPEC],
+        limit=16 * MIB,
         flops=AHEAD,
     )(
         me, parts, pre, memory_max, forget_bias[None], memory_norm.reshape(heads, head_dim),
@@ -379,23 +431,33 @@
     )
     gated_rows = exchange(gated)
 
-    next_matrix = keep[:, :, None] * memory + value[:, :, None] * key[:, None, :]
-    next_matrix = lax.optimization_barrier(next_matrix[None])
     gate = in_hbm(expert_gate.reshape(width, hidden_dim))
-    take, mine, spread, weights, next_norm, next_max, early = call(
-        tables_body,
+    early_rows = width // 2
+    take, mine, spread, weights, next_norm, next_max, early, next_matrix = call(
+        window_body,
         (
             shaped((CAPACITY + 1, devices, devices), BF16), shaped((SLOTS, devices), BF16),
             shaped((devices, SLOTS), BF16), shaped((devices, 1)),
-            shaped((heads, head_dim)), shaped((1, heads)), shaped((width // 2, hidden_dim), BF16),
+            shaped((heads, head_dim)), shaped((1, heads)), shaped((early_rows, hidden_dim), BF16),
+            shaped((heads, head_dim, head_dim)),
         ),
-        [SMEM_SPEC] * 5 + [VMEM_SPEC] * 3 + [HBM_SPEC],
-        [pltpu.SemaphoreType.DMA],
-    )(me, *ids, group_weight, member_weight.reshape(-1), parts, next_norm, next_max, gate)
+        [SMEM_SPEC] * 5 + [VMEM_SPEC] * 6 + [HBM_SPEC] * 3,
+        [
+            pltpu.VMEM((heads - first, head_dim, head_dim), F32),
+            pltpu.VMEM((heads - first, head_dim, head_dim), F32),
+            pltpu.SemaphoreType.DMA((2, heads - first + 1)),
+        ],
+        outputs=[VMEM_SPEC] * 7 + [HBM_SPEC],
+        aliases={13: 7},
+        limit=16 * MIB,
+    )(
+        me, *ids, group_weight, member_weight.reshape(-1), parts, next_norm, next_max,
+        value, key, keep, in_hbm(memory), gate, in_hbm(begun),
+    )
 
     outgoing = call(
-        project_body, shaped((devices, (CAPACITY + 1) * columns), BF16), [VMEM_SPEC] * 3 + [HBM_SPEC],
-    )(gated_rows, mixer_out.T, take, in_hbm(next_matrix))
+        project_body, shaped((devices, (CAPACITY + 1) * columns), BF16), [VMEM_SPEC] * 3
+    )(gated_rows, mixer_out.T, take)
     incoming = exchange(outgoing)
 
     back, middle = call(
@@ -403,7 +465,7 @@
         (shaped((devices, width), BF16), shaped((1, width))),
         [VMEM_SPEC] * 6 + [HBM_SPEC] * 3,
         [
-            pltpu.VMEM((width - width // 2, hidden_dim), BF16),
+            pltpu.VMEM((width - early_rows, hidden_dim), BF16),
             pltpu.VMEM((width, hidden_dim), BF16),
             pltpu.VMEM((hidden_dim, width), BF16),
             pltpu.VMEM((pl.cdiv((CAPACITY + 1) * columns, LANES), devices, LANES), F32),
@@ -418,7 +480,7 @@
     )
     returned = exchange(back)
     layer_out = call(finish_body, shaped((1, width), BF16), [VMEM_SPEC] * 3)(returned, weights, middle)
-    return (layer_out, next_matrix, next_norm[None], next_max)
+    return (layer_out, next_matrix[None], next_norm[None], next_max)
 
 
 def solution(mesh):

time: 70.9 us -> 68.4 us (0.965)
  other arithmetic: 3.96 us -> 0 us
  waiting for transfers between devices: 1.47 us -> 4.23 us
  blocking collectives: 45.7 us -> 43.2 us
  Pallas kernels: 12.4 us -> 13.6 us
    add x1 -> x0, other arithmetic: 3.96 us -> none  [local(): keep[:, :, None] * memory + value[:, :, None] * key[:, None, :]]
    all_to_all x1, waiting for transfers between devices: 1.47 us -> 4.23 us  [exchange(): lax.all_to_all(halves, 'ep', split_axis=0, concat_axis=0, tiled=True)]
    all_to_all x4, blocking collectives: 45.7 us -> 43.2 us  [exchange(): lax.all_to_all(halves, 'ep', split_axis=0, concat_axis=0, tiled=True)]
    pallas_call x1, Pallas kernels: 2.75 us -> 3.93 us  [local(): call(window_body, (shaped((CAPACITY + 1, devices, devices), BF16), shaped...]
  transfers between devices with their start and end apart: 1 -> 1, of which waited for: 1 -> 1; matrix products, arithmetic and copies ran while one was open for 6% -> 0% of each run, Pallas kernels for 4% -> 6%
where the time goes in v4:
time: 68.4 us; the launch traced here: 68 us
  blocking collectives  43.2 us (63%)
  Pallas kernels  13.6 us (20%)
  waiting for transfers between devices  4.23 us (6%)
  starting transfers between devices  2.57 us (4%)
  between operations  2.32 us (3%)
  local copies, waits for them, and re-layouts  2.08 us (3%)
    all_to_all x4, blocking collectives, exchange(): lax.all_to_all(halves, 'ep', split_axis=0, concat_axis=0, tiled=True)  43.2 us
    pallas_call x1, Pallas kernels, local(): call(expert_body, (shaped((devices, width), BF16), shaped((1, width))), [...  4.52 us
    all_to_all x1, waiting for transfers between devices, exchange(): lax.all_to_all(halves, 'ep', split_axis=0, concat_axis=0, tiled=True)  4.23 us
    pallas_call x1, Pallas kernels, local(): call(window_body, (shaped((CAPACITY + 1, devices, devices), BF16), shaped...  3.93 us
    pallas_call x1, Pallas kernels, local(): call(cell_body, (shaped((devices, width), BF16), shaped((heads, head_dim)...  2.94 us
    all_to_all x1, starting transfers between devices, exchange(): lax.all_to_all(halves, 'ep', split_axis=0, concat_axis=0, tiled=True)  2.57 us
  transfers between devices with their start and end apart: 1, of which 1 were waited for; matrix products, arithmetic and copies ran while one was open for 0% of the time, Pallas kernels for 6%

profile of v4, /device:TPU:0, one launch (start us, length us, event | category | flops | bytes accessed | tf_op | source)
XLA Modules:
  0.0 68.0 jit_solution(16000345318098383060)
XLA Ops:
  2.1 0.7 %copy-done.10 = bf16[1,2048]{1,0:T(2,128)(2,1)S(1)} copy-done((bf16[1,2048]{1,0:T(2,128)(2,1)S(1)}, bf16[1,2048]{1,0:T(2,128)(2,1)}, u32[]{:S(2)}) %copy-start.10) | copy-done | bytes 4120
  2.8 0.0 copy-start.12
  2.8 0.0 copy-start.13
  2.8 0.0 copy-start.14
  2.8 0.1 reshape.60
  2.9 15.3 %all_to_all.25 = bf16[32,2,1024]{2,1,0:T(2,128)(2,1)S(1)} all-to-all(bf16[32,2,1024]{2,1,0:T(2,128)(2,1)S(1)} %reshape.60), channel_id=1, replica_groups=mesh['ep'=32] {'ep'}, dimensions={0} | all-to-all | bytes 262144 | tf_op jit(solution)/shard_map/all_to_all | solution.py:29
  18.4 1.0 %shard_map.229 = (bf16[32,384]{1,0:T(8,128)(2,1)S(1)}, f32[8,32]{1,0:T(8,128)S(1)}) custom-call(s32[1]{0:T(128)S(6)} %copy.30.group_ref, s32[2]{0:T(128)S(1)} %bitcast.32, bf16[32,2048]{1,0:T(8,128)(2,1)S(1)} %bitcast.26, f32[1,2048]{1,0:T(1,128)S(1)} %bitcast.41, bf16[64,2048]{1,0:T(8,128)(2,1)S(1)} %bitcast.35, bf16[64,2048]{1,0:T(8,128)(2,1)S(1)} %bitcast.36, ...), custom_call_target="tpu_custom_call" | custom-call | flops 2000000000 | bytes 1000000 | tf_op jit(solution)/shard_map/pallas_call | solution.py:396
  19.4 0.1 reshape.62
  19.5 9.0 %all_to_all.26 = bf16[32,2,192]{2,1,0:T(2,128)(2,1)S(1)} all-to-all(bf16[32,2,192]{2,1,0:T(2,128)(2,1)S(1)} %reshape.62), channel_id=1, replica_groups=mesh['ep'=32] {'ep'}, dimensions={0} | all-to-all | bytes 49152 | tf_op jit(solution)/shard_map/all_to_all | solution.py:29
  28.6 0.1 reshape.63.parts_ref
  28.7 2.9 %shard_map.230 = (bf16[32,2048]{1,0:T(8,128)(2,1)S(1)}, f32[4,512]{1,0:T(4,128)S(1)}, f32[1,4]{1,0:T(1,128)S(1)}, f32[4,512]{1,0:T(4,128)S(1)}, f32[4,512]{1,0:T...) custom-call(s32[1]{0:T(128)} %bitcast.me_ref, bf16[32,384]{1,0:T(8,128)(2,1)S(1)} %reshape.63.parts_ref, ...), custom_call_target="tpu_custom_call" | custom-call | flops 2000000000 | bytes 1000000 | tf_op jit(solution)/shard_map/pallas_call | solution.py:410
  31.6 0.7 %reshape.66 = bf16[32,2,1024]{2,1,0:T(2,128)(2,1)} reshape(bf16[32,2048]{1,0:T(8,128)(2,1)S(1)} %get-tuple-element.25) | data formatting | bytes 262144 | tf_op jit(solution)/shard_map/reshape | solution.py:28
  32.4 2.6 %all-to-all-start.2 = ((bf16[32,2,1024]{2,1,0:T(2,128)(2,1)}), bf16[32,2,1024]{2,1,0:T(2,128)(2,1)S(1)}, u32[]{:S(2)}, u32[]{:S(2)}) async-start(bf16[32,2,1024]{2,1,0:T(2,128)(2,1)} %reshape.66), calls=%async_computation.2 | async-start | bytes 262144 | tf_op jit(solution)/shard_map/all_to_all | solution.py:29
  34.9 0.0 copy-start
  35.0 3.9 %shard_map.231 = (bf16[5,32,32]{2,1,0:T(8,128)(2,1)S(1)}, bf16[8,32]{1,0:T(8,128)(2,1)S(1)}, bf16[32,8]{1,0:T(8,128)(2,1)S(1)}, f32[32,1]{1,0:T(8,128)S(1)}, f32...) custom-call(s32[1]{0:T(128)} %bitcast.me_ref, ...), custom_call_target="tpu_custom_call", output_to_operand_aliasing={{7}: (13, {})} | custom-call | flops 10000000 | bytes 1000000 | tf_op jit(solution)/shard_map/pallas_call | solution.py:436
  38.9 4.2 %all-to-all-done.2 = bf16[32,2,1024]{2,1,0:T(2,128)(2,1)S(1)} async-done(((bf16[32,2,1024]{2,1,0:T(2,128)(2,1)}), bf16[32,2,1024]{2,1,0:T(2,128)(2,1)S(1)}, u32[]{:S(2)}, u32[]{:S(2)}) %all-to-all-start.2) | async-done | bytes 131104 | tf_op jit(solution)/shard_map/all_to_all | solution.py:29
  43.2 0.4 shard_map.232
  43.6 0.1 reshape.70
  43.7 9.0 %all_to_all.27 = bf16[32,2,160]{2,1,0:T(2,128)(2,1)S(1)} all-to-all(bf16[32,2,160]{2,1,0:T(2,128)(2,1)S(1)} %reshape.70), channel_id=1, replica_groups=mesh['ep'=32] {'ep'}, dimensions={0} | all-to-all | bytes 40960 | tf_op jit(solution)/shard_map/all_to_all | solution.py:29
  52.6 0.1 reshape.71.in_ref
  52.7 4.5 %shard_map.233 = (bf16[32,2048]{1,0:T(8,128)(2,1)S(1)}, f32[1,2048]{1,0:T(1,128)S(1)}) custom-call(bf16[32,320]{1,0:T(8,128)(2,1)S(1)} %reshape.71.in_ref, bf16[32,2048]{1,0:T(8,128)(2,1)S(1)} %bitcast.27, bf16[8,32]{1,0:T(8,128)(2,1)S(1)} %get-tuple-element.33.mine_ref, bf16[32,8]{1,0:T(8,128)(2,1)S(1)} %get-tuple-element.34.spread_ref, ...), custom_call_target="tpu_custom_call" | custom-call | flops 10000000 | bytes 1000000 | tf_op jit(solution)/shard_map/pallas_call | solution.py:463
  57.3 0.1 reshape.74
  57.4 9.9 %all_to_all.28 = bf16[32,2,1024]{2,1,0:T(2,128)(2,1)S(1)} all-to-all(bf16[32,2,1024]{2,1,0:T(2,128)(2,1)S(1)} %reshape.74), channel_id=1, replica_groups=mesh['ep'=32] {'ep'}, dimensions={0} | all-to-all | bytes 262144 | tf_op jit(solution)/shard_map/all_to_all | solution.py:29
  67.3 0.7 %shard_map.234 = bf16[1,2048]{1,0:T(2,128)(2,1)} custom-call(bf16[32,2048]{1,0:T(8,128)(2,1)S(1)} %bitcast.29, f32[32,1]{1,0:T(8,128)S(1)} %get-tuple-element.37.weight_ref, f32[1,2048]{1,0:T(1,128)S(1)} %get-tuple-element.38.middle_ref), custom_call_target="tpu_custom_call" | custom-call | flops 10000000 | bytes 1000000 | tf_op jit(solution)/shard_map/pallas_call | solution.py:482
  (29 shorter events, 0.1 us)
Async XLA Ops:
  0.6 17.7 %copy-start.2 = (s32[1,2]{1,0:T(1,128)S(1)}, s32[1,2]{1,0:T(1,128)}, u32[]{:S(2)}) copy-start(s32[1,2]{1,0:T(1,128)} %param.39) | copy-start | bytes 28
  0.6 17.7 %copy-start.9 = (bf16[2048,4]{0,1:T(4,128)(2,1)S(1)}, bf16[2048,4]{0,1:T(4,128)(2,1)}, u32[]{:S(2)}) copy-start(bf16[2048,4]{0,1:T(4,128)(2,1)} %param.28) | copy-start | bytes 49156
  0.7 17.7 %copy-start.8 = (bf16[2048,4]{0,1:T(4,128)(2,1)S(1)}, bf16[2048,4]{0,1:T(4,128)(2,1)}, u32[]{:S(2)}) copy-start(bf16[2048,4]{0,1:T(4,128)(2,1)} %param.27) | copy-start | bytes 49156
  0.7 17.7 %copy-start.7 = (bf16[2048,64]{0,1:T(8,128)(2,1)S(1)}, bf16[2048,64]{0,1:T(8,128)(2,1)}, u32[]{:S(2)}) copy-start(bf16[2048,64]{0,1:T(8,128)(2,1)} %param.26) | copy-start | bytes 786436
  0.7 17.7 %copy-start.6 = (bf16[2048,64]{0,1:T(8,128)(2,1)S(1)}, bf16[2048,64]{0,1:T(8,128)(2,1)}, u32[]{:S(2)}) copy-start(bf16[2048,64]{0,1:T(8,128)(2,1)} %param.25) | copy-start | bytes 786436
  0.7 17.7 %copy-start.5 = (bf16[2048,64]{0,1:T(8,128)(2,1)S(1)}, bf16[2048,64]{0,1:T(8,128)(2,1)}, u32[]{:S(2)}) copy-start(bf16[2048,64]{0,1:T(8,128)(2,1)} %param.24) | copy-start | bytes 786436
  0.7 17.7 %copy-start.4 = (bf16[2048,64]{0,1:T(8,128)(2,1)S(1)}, bf16[2048,64]{0,1:T(8,128)(2,1)}, u32[]{:S(2)}) copy-start(bf16[2048,64]{0,1:T(8,128)(2,1)} %param.23) | copy-start | bytes 786436
  2.1 0.7 %copy-start.10 = (bf16[1,2048]{1,0:T(2,128)(2,1)S(1)}, bf16[1,2048]{1,0:T(2,128)(2,1)}, u32[]{:S(2)}) copy-start(bf16[1,2048]{1,0:T(2,128)(2,1)} %row_ref.1) | copy-start | bytes 12292
  2.8 15.6 %copy-start.11 = (f32[2048]{0:T(1024)S(1)}, f32[2048]{0:T(1024)}, u32[]{:S(2)}) copy-start(f32[2048]{0:T(1024)} %param.22) | copy-start | bytes 24580
  2.8 25.8 %copy-start.12 = (f32[1,4,512]{2,1,0:T(4,128)S(1)}, f32[1,4,512]{2,1,0:T(4,128)}, u32[]{:S(2)}) copy-start(f32[1,4,512]{2,1,0:T(4,128)} %param.31) | copy-start | bytes 24580
  2.8 25.8 %copy-start.13 = (f32[1,4]{1,0:T(1,128)S(1)}, f32[1,4]{1,0:T(1,128)}, u32[]{:S(2)}) copy-start(f32[1,4]{1,0:T(1,128)} %max_ref.1) | copy-start | bytes 52
  2.8 25.8 %copy-start.14 = (f32[4]{0:T(128)S(1)}, f32[4]{0:T(128)}, u32[]{:S(2)}) copy-start(f32[4]{0:T(128)} %param.29) | copy-start | bytes 52
  19.4 15.5 %copy-start.3 = (f32[1,2]{1,0:T(1,128)S(1)}, f32[1,2]{1,0:T(1,128)}, u32[]{:S(2)}) copy-start(f32[1,2]{1,0:T(1,128)} %param.41) | copy-start | bytes 28
  32.4 10.8 %all-to-all-start.2 = ((bf16[32,2,1024]{2,1,0:T(2,128)(2,1)}), bf16[32,2,1024]{2,1,0:T(2,128)(2,1)S(1)}, u32[]{:S(2)}, u32[]{:S(2)}) async-start(bf16[32,2,1024]{2,1,0:T(2,128)(2,1)} %reshape.66), calls=%async_computation.2 | async-start | bytes 262144 | tf_op jit(solution)/shard_map/all_to_all | solution.py:29
  34.9 8.2 %copy-start = (bf16[2048,64]{0,1:T(8,128)(2,1)S(1)}, bf16[2048,64]{0,1:T(8,128)(2,1)}, u32[]{:S(2)}) copy-start(bf16[2048,64]{0,1:T(8,128)(2,1)} %param.33) | copy-start | bytes 786436
  35.0 17.8 %copy-start.1 = (f32[2048]{0:T(1024)S(1)}, f32[2048]{0:T(1024)}, u32[]{:S(2)}) copy-start(f32[2048]{0:T(1024)} %param.34) | copy-start | bytes 24580

commit v5 on v4

--- a/solution.py
+++ b/solution.py
@@ -1,3 +1,5 @@
+import functools
+
 import jax
 import jax.numpy as jnp
 from jax import lax
@@ -71,6 +73,13 @@
         ref[t, :, :part.shape[1]] = part
 
 
+def own_number(parts_ref):
+    ids = parts_ref[:, parts_ref.shape[1] - LANES:].astype(F32)
+    lane = lax.broadcasted_iota(jnp.int32, ids.shape, 1)
+    column = jnp.sum(jnp.where(lane == LANES - 1, ids, 0.0), axis=1, keepdims=True)
+    return column[:1].astype(jnp.int32)
+
+
 def diagonal(n):
     i = lax.broadcasted_iota(jnp.int32, (n, n), 0)
     j = lax.broadcasted_iota(jnp.int32, (n, n), 1)
@@ -89,12 +98,24 @@
     return jnp.sum(jnp.where(diagonal(n), spread, 0.0), axis=0, keepdims=True)
 
 
-def spread_body(me_ref, group_ref, weight_ref, row_ref, out_ref):
-    del me_ref, group_ref, weight_ref
+def group_body(group_ref, out_ref):
+    lane = lax.broadcasted_iota(jnp.int32, out_ref.shape, 1)
+    out_ref[...] = jnp.where(lane == 0, group_ref[0], 0)
+
+
+def spread_body(row_ref, group_ref, member_ref, member_weight_ref, out_ref, ids_ref, weights_ref):
     out_ref[...] = jnp.broadcast_to(row_ref[...].astype(F32), out_ref.shape).astype(BF16)
-
-
-def columns_body(group_ref, member_ref, rows_ref, gain_ref, wq, wk, wv, wo, wi, wf, out_ref, pre_ref):
+    lane = lax.broadcasted_iota(jnp.int32, ids_ref.shape, 1)
+    ids = group_ref[...]
+    weights = jnp.zeros(weights_ref.shape, F32)
+    for k in range(member_ref.shape[1]):
+        ids = jnp.where(lane == 1 + k, member_ref[:, k:k + 1], ids)
+        weights = jnp.where(lane == 1 + k, member_weight_ref[:, k:k + 1], weights)
+    ids_ref[...] = ids
+    weights_ref[...] = weights
+
+
+def columns_body(rows_ref, ids_ref, gain_ref, wq, wk, wv, wo, wi, wf, out_ref, pre_ref):
     heads = wi.shape[0]
     count = rows_ref.shape[0]
     normed = root_norm(rows_ref[...].astype(F32), gain_ref[...]).astype(BF16)
@@ -102,17 +123,17 @@
     cols = lax.dot_general(normed, stacked, NT, preferred_element_type=F32).astype(BF16)
     total = cols.shape[1]
     out_ref[:, :total] = cols
-    lane = lax.broadcasted_iota(jnp.int32, (count, out_ref.shape[1] - total), 1)
-    ids = jnp.where(lane == 0, group_ref[0], 0)
-    for k in range(member_ref.shape[0]):
-        ids = jnp.where(lane == 1 + k, member_ref[k], ids)
+    lane = lax.broadcasted_iota(jnp.int32, (count, LANES), 1)
+    number = lax.broadcasted_iota(jnp.int32, (count, LANES), 0)
+    ids = jnp.where(lane == LANES - 1, number, jnp.broadcast_to(ids_ref[...], (count, LANES)))
     out_ref[:, total:] = ids.astype(F32).astype(BF16)
     pre_ref[:heads, :] = lax.dot_general(wi[...], normed, NT, preferred_element_type=F32)
     pre_ref[heads:, :] = lax.dot_general(wf[...], normed, NT, preferred_element_type=F32)
 
 
 def window_body(
-    me_ref, group_ref, member_ref, group_weight, member_weight, parts_ref, norm_ref, max_ref,
+    picks,
+    group_weight, ids_ref, weights_ref, parts_ref, norm_ref, max_ref,
     value_ref, key_ref, keep_ref, mem_ref, gate_ref, begun_ref,
     take_ref, mine_ref, spread_ref, weight_ref, norm_out, max_out, early_ref, next_ref,
     old, new, sems,
@@ -133,7 +154,7 @@
     norm_out[...] = norm_ref[...]
     max_out[...] = max_ref[...]
     slot_tables(
-        me_ref, group_ref, member_ref, group_weight, member_weight, parts_ref,
+        group_weight, ids_ref, weights_ref, parts_ref, picks,
         take_ref, mine_ref, spread_ref, weight_ref,
     )
     turned = columns_of(value_ref[...])
@@ -148,12 +169,12 @@
 
 
 def slot_tables(
-    me_ref, group_ref, member_ref, group_weight, member_weight, parts_ref,
+    group_weight, local_ids, local_weights, parts_ref, picks,
     take_ref, mine_ref, spread_ref, weight_ref,
 ):
     count = parts_ref.shape[0]
     members = count // GROUPS
-    picks = member_ref.shape[0]
+    me = own_number(parts_ref)
     ids = parts_ref[:, parts_ref.shape[1] - LANES:].astype(F32)
     lane = lax.broadcasted_iota(jnp.int32, ids.shape, 1)
 
@@ -169,8 +190,8 @@
     for k in range(picks):
         chosen = (group * members + row_of(1 + k)).astype(jnp.int32)
         hit = jnp.where(expert == chosen, 1.0, hit)
-        local = group_ref[0] * members + member_ref[k]
-        weight += jnp.where(column == local, group_weight[0] * member_weight[k], 0.0)
+        local = local_ids[:, :1] * members + local_ids[:, 1 + k:2 + k]
+        weight += jnp.where(column == local, group_weight[0] * local_weights[:, 1 + k:2 + k], 0.0)
     weight_ref[...] = weight
     upto = jnp.where(expert <= token, 1.0, 0.0).astype(BF16)
     place = jnp.dot(hit.astype(BF16), upto, preferred_element_type=F32)
@@ -184,7 +205,7 @@
         else:
             take = jnp.where(expert == token, 1.0, 0.0)
         take_ref[s] = take.astype(BF16)
-        row = jnp.sum(jnp.where(expert == me_ref[0], take, 0.0), axis=0, keepdims=True)
+        row = jnp.sum(jnp.where(expert == me, take, 0.0), axis=0, keepdims=True)
         mine = jnp.where(slot == s, row, mine)
         if s < CAPACITY:
             spread = jnp.where(lane == s, to_column(row), spread)
@@ -193,7 +214,7 @@
 
 
 def cell_body(
-    me_ref, parts_ref, pre_ref, max_ref, bias_ref, norm_ref, mem_ref,
+    parts_ref, pre_ref, max_ref, bias_ref, norm_ref, mem_ref,
     gated_ref, norm_out, max_out, value_out, key_out, keep_out, next_ref,
     mem, new, wide, tall, sems,
 ):
@@ -221,7 +242,7 @@
 
     pre = pre_ref[...]
     lane = lax.broadcasted_iota(jnp.int32, pre.shape, 1)
-    pre = jnp.sum(jnp.where(lane == me_ref[0], pre, 0.0), axis=1, keepdims=True)
+    pre = jnp.sum(jnp.where(lane == own_number(parts_ref), pre, 0.0), axis=1, keepdims=True)
     input_pre = pre[:heads]
     forget_pre = pre[heads:] + to_column(bias_ref[...])
     log_forget = jnp.minimum(forget_pre, 0.0) - jnp.log1p(jnp.exp(-jnp.abs(forget_pre)))
@@ -384,22 +405,26 @@
     heads, head_dim = memory_norm.shape[1:]
     hidden_dim = expert_gate.shape[2]
     assert tokens.shape[0] == 1 and expert_gate.shape[0] == 1
-    me = lax.axis_index("ep").astype(jnp.int32)[None]
-
-    ids = (route_group, route_member.reshape(-1))
-
-    row = call(spread_body, shaped((devices, width), BF16), [SMEM_SPEC] * 3 + [VMEM_SPEC], flops=AHEAD)(
-        me, route_group, group_weight, tokens
-    )
+
+    picks = route_member.shape[1]
+    assert devices <= 256
+
+    group_row = call(group_body, shaped((1, LANES), jnp.int32), [SMEM_SPEC], flops=AHEAD)(route_group)
+    row, ids, local_weights = call(
+        spread_body,
+        (shaped((devices, width), BF16), shaped((1, LANES), jnp.int32), shaped((1, LANES))),
+        [VMEM_SPEC] * 4,
+        flops=AHEAD,
+    )(tokens, group_row, route_member, member_weight)
     rows = exchange(row)
 
     cols, pre = call(
         columns_body,
         (shaped((devices, 4 * columns + LANES), BF16), shaped((2 * heads, devices))),
-        [SMEM_SPEC] * 2 + [VMEM_SPEC] * 8,
+        [VMEM_SPEC] * 9,
         flops=AHEAD,
     )(
-        *ids, rows, mixer_gain[None], query_weight.T, key_weight.T, value_weight.T, outgate_weight.T,
+        rows, ids, mixer_gain[None], query_weight.T, key_weight.T, value_weight.T, outgate_weight.T,
         input_weight.T, forget_weight.T,
     )
     parts = exchange(cols)
@@ -414,7 +439,7 @@
             shaped((heads, head_dim)), shaped((heads, head_dim)), shaped((heads, head_dim)),
             shaped((heads, head_dim, head_dim)),
         ),
-        [SMEM_SPEC] + [VMEM_SPEC] * 5 + [HBM_SPEC],
+        [VMEM_SPEC] * 5 + [HBM_SPEC],
         [
             pltpu.VMEM((heads, head_dim, head_dim), F32),
             pltpu.VMEM((first, head_dim, head_dim), F32),
@@ -426,7 +451,7 @@
         limit=16 * MIB,
         flops=AHEAD,
     )(
-        me, parts, pre, memory_max, forget_bias[None], memory_norm.reshape(heads, head_dim),
+        parts, pre, memory_max, forget_bias[None], memory_norm.reshape(heads, head_dim),
         in_hbm(memory),
     )
     gated_rows = exchange(gated)
@@ -434,24 +459,24 @@
     gate = in_hbm(expert_gate.reshape(width, hidden_dim))
     early_rows = width // 2
     take, mine, spread, weights, next_norm, next_max, early, next_matrix = call(
-        window_body,
+        functools.partial(window_body, picks),
         (
             shaped((CAPACITY + 1, devices, devices), BF16), shaped((SLOTS, devices), BF16),
             shaped((devices, SLOTS), BF16), shaped((devices, 1)),
             shaped((heads, head_dim)), shaped((1, heads)), shaped((early_rows, hidden_dim), BF16),
             shaped((heads, head_dim, head_dim)),
         ),
-        [SMEM_SPEC] * 5 + [VMEM_SPEC] * 6 + [HBM_SPEC] * 3,
+        [SMEM_SPEC] + [VMEM_SPEC] * 8 + [HBM_SPEC] * 3,
         [
             pltpu.VMEM((heads - first, head_dim, head_dim), F32),
             pltpu.VMEM((heads - first, head_dim, head_dim), F32),
             pltpu.SemaphoreType.DMA((2, heads - first + 1)),
         ],
         outputs=[VMEM_SPEC] * 7 + [HBM_SPEC],
-        aliases={13: 7},
+        aliases={11: 7},
         limit=16 * MIB,
     )(
-        me, *ids, group_weight, member_weight.reshape(-1), parts, next_norm, next_max,
+        group_weight, ids, local_weights, parts, next_norm, next_max,
         value, key, keep, in_hbm(memory), gate, in_hbm(begun),
     )
 

time: 68.4 us -> 66.6 us (0.974)
  Pallas kernels: 13.6 us -> 12.7 us
    pallas_call x2 -> x3, Pallas kernels: 3.94 us -> 3.5 us  [the longest x1 3.42 us: local(): call(functools.partial(window_body, picks), (shaped((CAPACITY + 1, device...]
  transfers between devices with their start and end apart: 1 -> 1, of which waited for: 1 -> 1; matrix products, arithmetic and copies ran while one was open for 0% -> 0% of each run, Pallas kernels for 6% -> 5%
where the time goes in v5:
time: 66.6 us; the launch traced here: 66.3 us
  blocking collectives  43.2 us (65%)
  Pallas kernels  12.7 us (19%)
  waiting for transfers between devices  4.1 us (6%)
  starting transfers between devices  2.56 us (4%)
  between operations  2.25 us (3%)
  local copies, waits for them, and re-layouts  1.41 us (2%)
    all_to_all x4, blocking collectives, exchange(): lax.all_to_all(halves, 'ep', split_axis=0, concat_axis=0, tiled=True)  43.2 us
    pallas_call x1, Pallas kernels, local(): call(expert_body, (shaped((devices, width), BF16), shaped((1, width))), [...  4.52 us
    all_to_all x1, waiting for transfers between devices, exchange(): lax.all_to_all(halves, 'ep', split_axis=0, concat_axis=0, tiled=True)  4.1 us
    pallas_call x1, Pallas kernels, local(): call(functools.partial(window_body, picks), (shaped((CAPACITY + 1, device...  3.42 us
    pallas_call x1, Pallas kernels, local(): call(cell_body, (shaped((devices, width), BF16), shaped((heads, head_dim)...  3.05 us
    all_to_all x1, starting transfers between devices, exchange(): lax.all_to_all(halves, 'ep', split_axis=0, concat_axis=0, tiled=True)  2.56 us
  transfers between devices with their start and end apart: 1, of which 1 were waited for; matrix products, arithmetic and copies ran while one was open for 0% of the time, Pallas kernels for 5%

profile of v5, /device:TPU:0, one launch (start us, length us, event | category | flops | bytes accessed | tf_op | source)
XLA Modules:
  0.0 66.3 jit_solution(4855900956565513023)
XLA Ops:
  1.4 0.0 copy-start.2
  1.4 0.0 copy-start.3
  1.4 0.0 copy-start.6
  1.4 0.0 copy-start.7
  1.5 0.1 shard_map.229
  1.5 0.1 reshape.53
  1.6 15.3 %all_to_all.25 = bf16[32,2,1024]{2,1,0:T(2,128)(2,1)S(1)} all-to-all(bf16[32,2,1024]{2,1,0:T(2,128)(2,1)S(1)} %reshape.53), channel_id=1, replica_groups=mesh['ep'=32] {'ep'}, dimensions={0} | all-to-all | bytes 262144 | tf_op jit(solution)/shard_map/all_to_all | solution.py:31
  17.1 0.5 shard_map.230
  17.6 0.1 reshape.55
  17.7 9.0 %all_to_all.26 = bf16[32,2,192]{2,1,0:T(2,128)(2,1)S(1)} all-to-all(bf16[32,2,192]{2,1,0:T(2,128)(2,1)S(1)} %reshape.55), channel_id=1, replica_groups=mesh['ep'=32] {'ep'}, dimensions={0} | all-to-all | bytes 49152 | tf_op jit(solution)/shard_map/all_to_all | solution.py:31
  26.7 0.1 reshape.56.parts_ref
  26.8 3.1 %shard_map.231 = (bf16[32,2048]{1,0:T(8,128)(2,1)S(1)}, f32[4,512]{1,0:T(4,128)S(1)}, f32[1,4]{1,0:T(1,128)S(1)}, f32[4,512]{1,0:T(4,128)S(1)}, f32[4,512]{1,0:T...) custom-call(bf16[32,384]{1,0:T(8,128)(2,1)S(1)} %reshape.56.parts_ref, f32[8,32]{1,0:T(8,128)S(1)} %get-tuple-element.29.pre_ref, ...), custom_call_target="tpu_custom_call" | custom-call | flops 2000000000 | bytes 1000000 | tf_op jit(solution)/shard_map/pallas_call | solution.py:435
  29.9 0.7 %reshape.59 = bf16[32,2,1024]{2,1,0:T(2,128)(2,1)} reshape(bf16[32,2048]{1,0:T(8,128)(2,1)S(1)} %get-tuple-element.30) | data formatting | bytes 262144 | tf_op jit(solution)/shard_map/reshape | solution.py:30
  30.6 2.6 %all-to-all-start.2 = ((bf16[32,2,1024]{2,1,0:T(2,128)(2,1)}), bf16[32,2,1024]{2,1,0:T(2,128)(2,1)S(1)}, u32[]{:S(2)}, u32[]{:S(2)}) async-start(bf16[32,2,1024]{2,1,0:T(2,128)(2,1)} %reshape.59), calls=%async_computation.2 | async-start | bytes 262144 | tf_op jit(solution)/shard_map/all_to_all | solution.py:31
  33.9 3.4 %shard_map.232 = (bf16[5,32,32]{2,1,0:T(8,128)(2,1)S(1)}, bf16[8,32]{1,0:T(8,128)(2,1)S(1)}, bf16[32,8]{1,0:T(8,128)(2,1)S(1)}, f32[32,1]{1,0:T(8,128)S(1)}, f32...) custom-call(f32[1]{0:T(128)S(6)} %copy.31.group_weight, ...), custom_call_target="tpu_custom_call", output_to_operand_aliasing={{7}: (11, {})} | custom-call | flops 10000000 | bytes 1000000 | tf_op jit(solution)/shard_map/pallas_call | solution.py:461
  37.3 4.1 %all-to-all-done.2 = bf16[32,2,1024]{2,1,0:T(2,128)(2,1)S(1)} async-done(((bf16[32,2,1024]{2,1,0:T(2,128)(2,1)}), bf16[32,2,1024]{2,1,0:T(2,128)(2,1)S(1)}, u32[]{:S(2)}, u32[]{:S(2)}) %all-to-all-start.2) | async-done | bytes 131104 | tf_op jit(solution)/shard_map/all_to_all | solution.py:31
  41.4 0.4 shard_map.233
  41.8 0.1 reshape.62
  41.9 9.0 %all_to_all.27 = bf16[32,2,160]{2,1,0:T(2,128)(2,1)S(1)} all-to-all(bf16[32,2,160]{2,1,0:T(2,128)(2,1)S(1)} %reshape.62), channel_id=1, replica_groups=mesh['ep'=32] {'ep'}, dimensions={0} | all-to-all | bytes 40960 | tf_op jit(solution)/shard_map/all_to_all | solution.py:31
  50.9 0.1 reshape.63.in_ref
  51.0 4.5 %shard_map.234 = (bf16[32,2048]{1,0:T(8,128)(2,1)S(1)}, f32[1,2048]{1,0:T(1,128)S(1)}) custom-call(bf16[32,320]{1,0:T(8,128)(2,1)S(1)} %reshape.63.in_ref, bf16[32,2048]{1,0:T(8,128)(2,1)S(1)} %bitcast.24, bf16[8,32]{1,0:T(8,128)(2,1)S(1)} %get-tuple-element.39.mine_ref, bf16[32,8]{1,0:T(8,128)(2,1)S(1)} %get-tuple-element.40.spread_ref, ...), custom_call_target="tpu_custom_call" | custom-call | flops 10000000 | bytes 1000000 | tf_op jit(solution)/shard_map/pallas_call | solution.py:488
  55.5 0.1 reshape.66
  55.6 9.9 %all_to_all.28 = bf16[32,2,1024]{2,1,0:T(2,128)(2,1)S(1)} all-to-all(bf16[32,2,1024]{2,1,0:T(2,128)(2,1)S(1)} %reshape.66), channel_id=1, replica_groups=mesh['ep'=32] {'ep'}, dimensions={0} | all-to-all | bytes 262144 | tf_op jit(solution)/shard_map/all_to_all | solution.py:31
  65.5 0.7 %shard_map.235 = bf16[1,2048]{1,0:T(2,128)(2,1)} custom-call(bf16[32,2048]{1,0:T(8,128)(2,1)S(1)} %bitcast.26, f32[32,1]{1,0:T(8,128)S(1)} %get-tuple-element.43.weight_ref, f32[1,2048]{1,0:T(1,128)S(1)} %get-tuple-element.44.middle_ref), custom_call_target="tpu_custom_call" | custom-call | flops 10000000 | bytes 1000000 | tf_op jit(solution)/shard_map/pallas_call | solution.py:507
  (30 shorter events, 0.1 us)
Async XLA Ops:
  0.6 0.7 %copy-start.12 = (f32[1,2]{1,0:T(1,128)S(1)}, f32[1,2]{1,0:T(1,128)}, u32[]{:S(2)}) copy-start(f32[1,2]{1,0:T(1,128)} %member_weight_ref.1) | copy-start | bytes 28
  0.6 0.7 %copy-start.11 = (s32[1,2]{1,0:T(1,128)S(1)}, s32[1,2]{1,0:T(1,128)}, u32[]{:S(2)}) copy-start(s32[1,2]{1,0:T(1,128)} %member_ref.1) | copy-start | bytes 28
  0.7 0.7 %copy-start.8 = (bf16[1,2048]{1,0:T(2,128)(2,1)S(1)}, bf16[1,2048]{1,0:T(2,128)(2,1)}, u32[]{:S(2)}) copy-start(bf16[1,2048]{1,0:T(2,128)(2,1)} %row_ref.1) | copy-start | bytes 12292
  1.4 15.6 %copy-start.2 = (bf16[2048,64]{0,1:T(8,128)(2,1)S(1)}, bf16[2048,64]{0,1:T(8,128)(2,1)}, u32[]{:S(2)}) copy-start(bf16[2048,64]{0,1:T(8,128)(2,1)} %param.23) | copy-start | bytes 786436
  1.4 15.6 %copy-start.3 = (bf16[2048,64]{0,1:T(8,128)(2,1)S(1)}, bf16[2048,64]{0,1:T(8,128)(2,1)}, u32[]{:S(2)}) copy-start(bf16[2048,64]{0,1:T(8,128)(2,1)} %param.24) | copy-start | bytes 786436
  1.4 15.6 %copy-start.4 = (bf16[2048,64]{0,1:T(8,128)(2,1)S(1)}, bf16[2048,64]{0,1:T(8,128)(2,1)}, u32[]{:S(2)}) copy-start(bf16[2048,64]{0,1:T(8,128)(2,1)} %param.25) | copy-start | bytes 786436
  1.4 15.6 %copy-start.5 = (bf16[2048,64]{0,1:T(8,128)(2,1)S(1)}, bf16[2048,64]{0,1:T(8,128)(2,1)}, u32[]{:S(2)}) copy-start(bf16[2048,64]{0,1:T(8,128)(2,1)} %param.26) | copy-start | bytes 786436
  1.4 15.6 %copy-start.6 = (bf16[2048,4]{0,1:T(4,128)(2,1)S(1)}, bf16[2048,4]{0,1:T(4,128)(2,1)}, u32[]{:S(2)}) copy-start(bf16[2048,4]{0,1:T(4,128)(2,1)} %param.27) | copy-start | bytes 49156
  1.4 15.6 %copy-start.7 = (bf16[2048,4]{0,1:T(4,128)(2,1)S(1)}, bf16[2048,4]{0,1:T(4,128)(2,1)}, u32[]{:S(2)}) copy-start(bf16[2048,4]{0,1:T(4,128)(2,1)} %param.28) | copy-start | bytes 49156
  1.4 15.6 %copy-start.9 = (f32[2048]{0:T(1024)S(1)}, f32[2048]{0:T(1024)}, u32[]{:S(2)}) copy-start(f32[2048]{0:T(1024)} %param.22) | copy-start | bytes 24580
  1.5 25.3 %copy-start.10 = (f32[1,4,512]{2,1,0:T(4,128)S(1)}, f32[1,4,512]{2,1,0:T(4,128)}, u32[]{:S(2)}) copy-start(f32[1,4,512]{2,1,0:T(4,128)} %param.31) | copy-start | bytes 24580
  1.5 25.3 %copy-start.13 = (f32[1,4]{1,0:T(1,128)S(1)}, f32[1,4]{1,0:T(1,128)}, u32[]{:S(2)}) copy-start(f32[1,4]{1,0:T(1,128)} %max_ref.1) | copy-start | bytes 52
  1.5 25.3 %copy-start.14 = (f32[4]{0:T(128)S(1)}, f32[4]{0:T(128)}, u32[]{:S(2)}) copy-start(f32[4]{0:T(128)} %param.29) | copy-start | bytes 52
  30.6 10.8 %all-to-all-start.2 = ((bf16[32,2,1024]{2,1,0:T(2,128)(2,1)}), bf16[32,2,1024]{2,1,0:T(2,128)(2,1)S(1)}, u32[]{:S(2)}, u32[]{:S(2)}) async-start(bf16[32,2,1024]{2,1,0:T(2,128)(2,1)} %reshape.59), calls=%async_computation.2 | async-start | bytes 262144 | tf_op jit(solution)/shard_map/all_to_all | solution.py:31
  33.8 7.6 %copy-start = (bf16[2048,64]{0,1:T(8,128)(2,1)S(1)}, bf16[2048,64]{0,1:T(8,128)(2,1)}, u32[]{:S(2)}) copy-start(bf16[2048,64]{0,1:T(8,128)(2,1)} %param.33) | copy-start | bytes 786436
  33.8 17.1 %copy-start.1 = (f32[2048]{0:T(1024)S(1)}, f32[2048]{0:T(1024)}, u32[]{:S(2)}) copy-start(f32[2048]{0:T(1024)} %param.34) | copy-start | bytes 24580

commit v6 on v5

--- a/solution.py
+++ b/solution.py
@@ -27,8 +27,18 @@
 
 def exchange(blocks):
     count, width = blocks.shape
-    halves = blocks.reshape(count, 2, width // 2)
-    return lax.all_to_all(halves, "ep", split_axis=0, concat_axis=0, tiled=True).reshape(count, width)
+    return exchange_halves(blocks.reshape(count, 2, width // 2))
+
+
+def exchange_halves(halves):
+    count, _, half = halves.shape
+    return lax.all_to_all(halves, "ep", split_axis=0, concat_axis=0, tiled=True).reshape(count, 2 * half)
+
+
+def halves_of(row, count):
+    half = row.shape[1] // 2
+    pair = jnp.concatenate([row[:, :half], row[:, half:]], axis=0).astype(BF16)
+    return jnp.broadcast_to(pair[None], (count, 2, half))
 
 
 VMEM_SPEC = pl.BlockSpec(memory_space=pltpu.VMEM)
@@ -104,7 +114,7 @@
 
 
 def spread_body(row_ref, group_ref, member_ref, member_weight_ref, out_ref, ids_ref, weights_ref):
-    out_ref[...] = jnp.broadcast_to(row_ref[...].astype(F32), out_ref.shape).astype(BF16)
+    out_ref[...] = halves_of(row_ref[...].astype(F32), out_ref.shape[0])
     lane = lax.broadcasted_iota(jnp.int32, ids_ref.shape, 1)
     ids = group_ref[...]
     weights = jnp.zeros(weights_ref.shape, F32)
@@ -220,9 +230,20 @@
 ):
     heads, head_dim = norm_ref.shape
     first = new.shape[0]
-    copies = [pltpu.make_async_copy(mem_ref.at[h], mem.at[h], sems.at[0, h]) for h in range(heads)]
-    stores = [pltpu.make_async_copy(new.at[h], next_ref.at[h], sems.at[1, h]) for h in range(first)]
-    for c in copies:
+    parts_of = sems.shape[2]
+    rows_of = head_dim // parts_of
+    copies = [
+        [
+            pltpu.make_async_copy(
+                mem_ref.at[h, pl.ds(k * rows_of, rows_of)], mem.at[h, pl.ds(k * rows_of, rows_of)],
+                sems.at[0, h, k],
+            )
+            for k in range(parts_of)
+        ]
+        for h in range(heads)
+    ]
+    stores = [pltpu.make_async_copy(new.at[h], next_ref.at[h], sems.at[1, h, 0]) for h in range(first)]
+    for c in sum(copies, []):
         c.start()
 
     columns = (parts_ref.shape[1] - LANES) // 4
@@ -262,13 +283,14 @@
     key_out[...] = key
     keep_out[...] = jnp.broadcast_to(keep, keep_out.shape)
 
-    count = gated_ref.shape[0]
+    outs = []
     ones = jnp.ones((8, LANES), BF16)
     turned = columns_of(admit * value)
     for h in range(heads):
-        copies[h].wait()
         sums = []
         for r in range(0, head_dim, LANES):
+            if r % rows_of == 0:
+                copies[h][r // rows_of].wait()
             block = mem[h, r:r + LANES, :]
             product = block * query[h:h + 1]
             sums.append(sum(product[:, p * LANES:(p + 1) * LANES] for p in range(tiles)))
@@ -285,9 +307,8 @@
         carried = carried + lax.dot_general(ones, low, NT, preferred_element_type=F32)
         numer = keep[h:h + 1] * carried[:1] + score[h:h + 1] * value[h:h + 1]
         gated = numer * scale[h:h + 1] * opened[h:h + 1]
-        gated_ref[:, h * head_dim:(h + 1) * head_dim] = jnp.broadcast_to(
-            gated, (count, head_dim)
-        ).astype(BF16)
+        outs.append(gated)
+    gated_ref[...] = halves_of(jnp.concatenate(outs, axis=1), gated_ref.shape[0])
     for c in stores:
         c.wait()
 
@@ -412,11 +433,11 @@
     group_row = call(group_body, shaped((1, LANES), jnp.int32), [SMEM_SPEC], flops=AHEAD)(route_group)
     row, ids, local_weights = call(
         spread_body,
-        (shaped((devices, width), BF16), shaped((1, LANES), jnp.int32), shaped((1, LANES))),
+        (shaped((devices, 2, width // 2), BF16), shaped((1, LANES), jnp.int32), shaped((1, LANES))),
         [VMEM_SPEC] * 4,
         flops=AHEAD,
     )(tokens, group_row, route_member, member_weight)
-    rows = exchange(row)
+    rows = exchange_halves(row)
 
     cols, pre = call(
         columns_body,
@@ -431,11 +452,11 @@
 
     memory = memory_matrix.reshape(heads, head_dim, head_dim)
     tiles = width // LANES
-    first = heads // 2
+    first = max(heads // 4, 1)
     gated, next_norm, next_max, value, key, keep, begun = call(
         cell_body,
         (
-            shaped((devices, width), BF16), shaped((heads, head_dim)), shaped((1, heads)),
+            shaped((devices, 2, width // 2), BF16), shaped((heads, head_dim)), shaped((1, heads)),
             shaped((heads, head_dim)), shaped((heads, head_dim)), shaped((heads, head_dim)),
             shaped((heads, head_dim, head_dim)),
         ),
@@ -445,7 +466,7 @@
             pltpu.VMEM((first, head_dim, head_dim), F32),
             pltpu.VMEM((pl.cdiv(4 * columns, LANES), devices, LANES), F32),
             pltpu.VMEM((4 * tiles, LANES), F32),
-            pltpu.SemaphoreType.DMA((2, heads)),
+            pltpu.SemaphoreType.DMA((2, heads, 2)),
         ],
         outputs=[VMEM_SPEC] * 6 + [HBM_SPEC],
         limit=16 * MIB,
@@ -454,7 +475,7 @@
         parts, pre, memory_max, forget_bias[None], memory_norm.reshape(heads, head_dim),
         in_hbm(memory),
     )
-    gated_rows = exchange(gated)
+    gated_rows = exchange_halves(gated)
 
     gate = in_hbm(expert_gate.reshape(width, hidden_dim))
     early_rows = width // 2

time: 66.6 us -> 66.3 us (level)
  local copies, waits for them, and re-layouts: 1.41 us -> 0.61 us
  Pallas kernels: 12.7 us -> 13.4 us
    reshape x7 -> x5, local copies, waits for them, and re-layouts: 1.26 us -> 0.46 us  [the longest x3 0.27 us: exchange(): return exchange_halves(blocks.reshape(count, 2, width // 2))]
  transfers between devices with their start and end apart: 1 -> 1, of which waited for: 1 -> 1; matrix products, arithmetic and copies ran while one was open for 0% -> 0% of each run, Pallas kernels for 5% -> 6%
where the time goes in v6:
time: 66.3 us; the launch traced here: 66 us
  blocking collectives  43.4 us (65%)
  Pallas kernels  13.4 us (20%)
  waiting for transfers between devices  3.74 us (6%)
  starting transfers between devices  2.58 us (4%)
  between operations  2.24 us (3%)
    all_to_all x4, blocking collectives, exchange_halves(): lax.all_to_all(halves, 'ep', split_axis=0, concat_axis=0, tiled=True)  43.4 us
    pallas_call x1, Pallas kernels, local(): call(expert_body, (shaped((devices, width), BF16), shaped((1, width))), [...  4.52 us
    pallas_call x1, Pallas kernels, local(): call(functools.partial(window_body, picks), (shaped((CAPACITY + 1, device...  3.79 us
    all_to_all x1, waiting for transfers between devices, exchange_halves(): lax.all_to_all(halves, 'ep', split_axis=0, concat_axis=0, tiled=True)  3.74 us
    pallas_call x1, Pallas kernels, local(): call(cell_body, (shaped((devices, 2, width // 2), BF16), shaped((heads, h...  3.33 us
    all_to_all x1, starting transfers between devices, exchange_halves(): lax.all_to_all(halves, 'ep', split_axis=0, concat_axis=0, tiled=True)  2.58 us
  transfers between devices with their start and end apart: 1, of which 1 were waited for; matrix products, arithmetic and copies ran while one was open for 0% of the time, Pallas kernels for 6%

profile of v6, /device:TPU:0, one launch (start us, length us, event | category | flops | bytes accessed | tf_op | source)
XLA Modules:
  0.0 66.0 jit_solution(1593674847628634552)
XLA Ops:
  1.4 0.0 copy-start.2
  1.4 0.0 copy-start.3
  1.4 0.0 copy-start.6
  1.4 0.0 copy-start.7
  1.5 0.1 shard_map.229
  1.5 15.3 %all_to_all.25 = bf16[32,2,1024]{2,1,0:T(2,128)(2,1)S(1)} all-to-all(bf16[32,2,1024]{2,1,0:T(2,128)(2,1)S(1)} %get-tuple-element.26), channel_id=1, replica_groups=mesh['ep'=32] {'ep'}, dimensions={0} | all-to-all | bytes 262144 | tf_op jit(solution)/shard_map/all_to_all | solution.py:35
  17.0 0.5 shard_map.230
  17.5 0.1 reshape.48
  17.6 9.0 %all_to_all.26 = bf16[32,2,192]{2,1,0:T(2,128)(2,1)S(1)} all-to-all(bf16[32,2,192]{2,1,0:T(2,128)(2,1)S(1)} %reshape.48), channel_id=1, replica_groups=mesh['ep'=32] {'ep'}, dimensions={0} | all-to-all | bytes 49152 | tf_op jit(solution)/shard_map/all_to_all | solution.py:35
  26.6 0.1 reshape.49.parts_ref
  26.7 3.3 %shard_map.231 = (bf16[32,2,1024]{2,1,0:T(2,128)(2,1)}, f32[4,512]{1,0:T(4,128)S(1)}, f32[1,4]{1,0:T(1,128)S(1)}, f32[4,512]{1,0:T(4,128)S(1)}, f32[4,512]{1,0:T...) custom-call(bf16[32,384]{1,0:T(8,128)(2,1)S(1)} %reshape.49.parts_ref, f32[8,32]{1,0:T(8,128)S(1)} %get-tuple-element.29.pre_ref, ...), custom_call_target="tpu_custom_call" | custom-call | flops 2000000000 | bytes 1000000 | tf_op jit(solution)/shard_map/pallas_call | solution.py:456
  30.1 2.6 %all-to-all-start.2 = ((bf16[32,2,1024]{2,1,0:T(2,128)(2,1)}), bf16[32,2,1024]{2,1,0:T(2,128)(2,1)S(1)}, u32[]{:S(2)}, u32[]{:S(2)}) async-start(bf16[32,2,1024]{2,1,0:T(2,128)(2,1)} %get-tuple-element.30), calls=%async_computation.2 | async-start | bytes 262144 | tf_op jit(solution)/shard_map/all_to_all | solution.py:35
  33.3 0.0 copy-start
  33.3 0.0 copy-start.1
  33.3 3.8 %shard_map.232 = (bf16[5,32,32]{2,1,0:T(8,128)(2,1)S(1)}, bf16[8,32]{1,0:T(8,128)(2,1)S(1)}, bf16[32,8]{1,0:T(8,128)(2,1)S(1)}, f32[32,1]{1,0:T(8,128)S(1)}, f32...) custom-call(f32[1]{0:T(128)S(6)} %copy.31.group_weight, ...), custom_call_target="tpu_custom_call", output_to_operand_aliasing={{7}: (11, {})} | custom-call | flops 10000000 | bytes 1000000 | tf_op jit(solution)/shard_map/pallas_call | solution.py:482
  37.1 3.7 %all-to-all-done.2 = bf16[32,2,1024]{2,1,0:T(2,128)(2,1)S(1)} async-done(((bf16[32,2,1024]{2,1,0:T(2,128)(2,1)}), bf16[32,2,1024]{2,1,0:T(2,128)(2,1)S(1)}, u32[]{:S(2)}, u32[]{:S(2)}) %all-to-all-start.2) | async-done | bytes 131104 | tf_op jit(solution)/shard_map/all_to_all | solution.py:35
  40.9 0.4 shard_map.233
  41.3 0.1 reshape.54
  41.4 9.2 %all_to_all.27 = bf16[32,2,160]{2,1,0:T(2,128)(2,1)S(1)} all-to-all(bf16[32,2,160]{2,1,0:T(2,128)(2,1)S(1)} %reshape.54), channel_id=1, replica_groups=mesh['ep'=32] {'ep'}, dimensions={0} | all-to-all | bytes 40960 | tf_op jit(solution)/shard_map/all_to_all | solution.py:35
  50.6 0.1 reshape.55.in_ref
  50.7 4.5 %shard_map.234 = (bf16[32,2048]{1,0:T(8,128)(2,1)S(1)}, f32[1,2048]{1,0:T(1,128)S(1)}) custom-call(bf16[32,320]{1,0:T(8,128)(2,1)S(1)} %reshape.55.in_ref, bf16[32,2048]{1,0:T(8,128)(2,1)S(1)} %bitcast.24, bf16[8,32]{1,0:T(8,128)(2,1)S(1)} %get-tuple-element.39.mine_ref, bf16[32,8]{1,0:T(8,128)(2,1)S(1)} %get-tuple-element.40.spread_ref, ...), custom_call_target="tpu_custom_call" | custom-call | flops 10000000 | bytes 1000000 | tf_op jit(solution)/shard_map/pallas_call | solution.py:509
  55.2 0.1 reshape.58
  55.3 9.9 %all_to_all.28 = bf16[32,2,1024]{2,1,0:T(2,128)(2,1)S(1)} all-to-all(bf16[32,2,1024]{2,1,0:T(2,128)(2,1)S(1)} %reshape.58), channel_id=1, replica_groups=mesh['ep'=32] {'ep'}, dimensions={0} | all-to-all | bytes 262144 | tf_op jit(solution)/shard_map/all_to_all | solution.py:35
  65.2 0.7 %shard_map.235 = bf16[1,2048]{1,0:T(2,128)(2,1)} custom-call(bf16[32,2048]{1,0:T(8,128)(2,1)S(1)} %bitcast.26, f32[32,1]{1,0:T(8,128)S(1)} %get-tuple-element.43.weight_ref, f32[1,2048]{1,0:T(1,128)S(1)} %get-tuple-element.44.middle_ref), custom_call_target="tpu_custom_call" | custom-call | flops 10000000 | bytes 1000000 | tf_op jit(solution)/shard_map/pallas_call | solution.py:528
  (28 shorter events, 0.1 us)
Async XLA Ops:
  0.6 0.7 %copy-start.12 = (f32[1,2]{1,0:T(1,128)S(1)}, f32[1,2]{1,0:T(1,128)}, u32[]{:S(2)}) copy-start(f32[1,2]{1,0:T(1,128)} %member_weight_ref.1) | copy-start | bytes 28
  0.6 0.7 %copy-start.11 = (s32[1,2]{1,0:T(1,128)S(1)}, s32[1,2]{1,0:T(1,128)}, u32[]{:S(2)}) copy-start(s32[1,2]{1,0:T(1,128)} %member_ref.1) | copy-start | bytes 28
  0.7 0.7 %copy-start.8 = (bf16[1,2048]{1,0:T(2,128)(2,1)S(1)}, bf16[1,2048]{1,0:T(2,128)(2,1)}, u32[]{:S(2)}) copy-start(bf16[1,2048]{1,0:T(2,128)(2,1)} %row_ref.1) | copy-start | bytes 12292
  1.4 15.5 %copy-start.2 = (bf16[2048,64]{0,1:T(8,128)(2,1)S(1)}, bf16[2048,64]{0,1:T(8,128)(2,1)}, u32[]{:S(2)}) copy-start(bf16[2048,64]{0,1:T(8,128)(2,1)} %param.23) | copy-start | bytes 786436
  1.4 15.5 %copy-start.3 = (bf16[2048,64]{0,1:T(8,128)(2,1)S(1)}, bf16[2048,64]{0,1:T(8,128)(2,1)}, u32[]{:S(2)}) copy-start(bf16[2048,64]{0,1:T(8,128)(2,1)} %param.24) | copy-start | bytes 786436
  1.4 15.5 %copy-start.4 = (bf16[2048,64]{0,1:T(8,128)(2,1)S(1)}, bf16[2048,64]{0,1:T(8,128)(2,1)}, u32[]{:S(2)}) copy-start(bf16[2048,64]{0,1:T(8,128)(2,1)} %param.25) | copy-start | bytes 786436
  1.4 15.5 %copy-start.5 = (bf16[2048,64]{0,1:T(8,128)(2,1)S(1)}, bf16[2048,64]{0,1:T(8,128)(2,1)}, u32[]{:S(2)}) copy-start(bf16[2048,64]{0,1:T(8,128)(2,1)} %param.26) | copy-start | bytes 786436
  1.4 15.5 %copy-start.6 = (bf16[2048,4]{0,1:T(4,128)(2,1)S(1)}, bf16[2048,4]{0,1:T(4,128)(2,1)}, u32[]{:S(2)}) copy-start(bf16[2048,4]{0,1:T(4,128)(2,1)} %param.27) | copy-start | bytes 49156
  1.4 15.5 %copy-start.7 = (bf16[2048,4]{0,1:T(4,128)(2,1)S(1)}, bf16[2048,4]{0,1:T(4,128)(2,1)}, u32[]{:S(2)}) copy-start(bf16[2048,4]{0,1:T(4,128)(2,1)} %param.28) | copy-start | bytes 49156
  1.4 15.5 %copy-start.9 = (f32[2048]{0:T(1024)S(1)}, f32[2048]{0:T(1024)}, u32[]{:S(2)}) copy-start(f32[2048]{0:T(1024)} %param.22) | copy-start | bytes 24580
  1.5 25.2 %copy-start.10 = (f32[1,4,512]{2,1,0:T(4,128)S(1)}, f32[1,4,512]{2,1,0:T(4,128)}, u32[]{:S(2)}) copy-start(f32[1,4,512]{2,1,0:T(4,128)} %param.31) | copy-start | bytes 24580
  1.5 25.2 %copy-start.13 = (f32[1,4]{1,0:T(1,128)S(1)}, f32[1,4]{1,0:T(1,128)}, u32[]{:S(2)}) copy-start(f32[1,4]{1,0:T(1,128)} %max_ref.1) | copy-start | bytes 52
  1.5 25.2 %copy-start.14 = (f32[4]{0:T(128)S(1)}, f32[4]{0:T(128)}, u32[]{:S(2)}) copy-start(f32[4]{0:T(128)} %param.29) | copy-start | bytes 52
  30.1 10.8 %all-to-all-start.2 = ((bf16[32,2,1024]{2,1,0:T(2,128)(2,1)}), bf16[32,2,1024]{2,1,0:T(2,128)(2,1)S(1)}, u32[]{:S(2)}, u32[]{:S(2)}) async-start(bf16[32,2,1024]{2,1,0:T(2,128)(2,1)} %get-tuple-element.30), calls=%async_computation.2 | async-start | bytes 262144 | tf_op jit(solution)/shard_map/all_to_all | solution.py:35
  33.3 7.6 %copy-start = (bf16[2048,64]{0,1:T(8,128)(2,1)S(1)}, bf16[2048,64]{0,1:T(8,128)(2,1)}, u32[]{:S(2)}) copy-start(bf16[2048,64]{0,1:T(8,128)(2,1)} %param.33) | copy-start | bytes 786436
  33.3 17.4 %copy-start.1 = (f32[2048]{0:T(1024)S(1)}, f32[2048]{0:T(1024)}, u32[]{:S(2)}) copy-start(f32[2048]{0:T(1024)} %param.34) | copy-start | bytes 24580

commit v7 on v6

--- a/solution.py
+++ b/solution.py
@@ -220,7 +220,7 @@
         if s < CAPACITY:
             spread = jnp.where(lane == s, to_column(row), spread)
     mine_ref[...] = mine.astype(BF16)
-    spread_ref[...] = spread.astype(BF16)
+    spread_ref[...] = spread
 
 
 def cell_body(
@@ -334,7 +334,7 @@
     gate, up, down, wide, tall, sems,
 ):
     width, hidden_dim = gate_ref.shape
-    steps = sems.shape[1]
+    steps = sems.shape[1] - 1
     here = early_ref.shape[0] * steps // width
     wide_step = width // steps
     tall_step = hidden_dim // steps
@@ -348,13 +348,17 @@
         chunk(0, gate_ref, gate, k, wide_step, early_ref.shape[0]) for k in range(here, steps)
     ]
     ups = [chunk(1, up_ref, up, k, wide_step) for k in range(steps)]
-    downs = [chunk(2, down_ref, down, k, tall_step) for k in range(steps)]
+    cuts = [k * tall_step for k in range(steps)] + [hidden_dim - tall_step // 2, hidden_dim]
+    downs = [
+        pltpu.make_async_copy(down_ref.at[pl.ds(a, b - a)], down.at[pl.ds(a, b - a)], sems.at[2, k])
+        for k, (a, b) in enumerate(zip(cuts, cuts[1:]))
+    ]
     for k in range(steps):
         ups[k].start()
         if k >= here:
             gates[k].start()
-    for k in range(steps):
-        downs[k].start()
+    for c in downs:
+        c.start()
 
     used = CAPACITY + 1
     columns = in_ref.shape[1] // used
@@ -383,13 +387,15 @@
             gate_part += jnp.dot(left[:, part], block, preferred_element_type=F32)
     hidden = (gate_part / (1.0 + jnp.exp(-gate_part)) * up_part).astype(BF16)
     result = jnp.zeros((SLOTS, width), F32)
-    for k in range(steps):
-        part = slice(k * tall_step, (k + 1) * tall_step)
+    for k, (a, b) in enumerate(zip(cuts, cuts[1:])):
         downs[k].wait()
-        result += jnp.dot(hidden[:, part], down[part, :], preferred_element_type=F32)
-    out_ref[...] = jnp.dot(
-        spread_ref[...], result.astype(BF16), preferred_element_type=F32
-    ).astype(BF16)
+        result += jnp.dot(hidden[:, a:b], down[a:b, :], preferred_element_type=F32)
+    result = result.astype(BF16).astype(F32)
+    spread = spread_ref[...]
+    back = jnp.zeros(out_ref.shape, F32)
+    for s in range(CAPACITY):
+        back = jnp.where(spread[:, s:s + 1] > 0.5, result[s:s + 1], back)
+    out_ref[...] = back.astype(BF16)
 
 
 def finish_body(returned_ref, weight_ref, middle_ref, out_ref):
@@ -483,7 +489,7 @@
         functools.partial(window_body, picks),
         (
             shaped((CAPACITY + 1, devices, devices), BF16), shaped((SLOTS, devices), BF16),
-            shaped((devices, SLOTS), BF16), shaped((devices, 1)),
+            shaped((devices, SLOTS)), shaped((devices, 1)),
             shaped((heads, head_dim)), shaped((1, heads)), shaped((early_rows, hidden_dim), BF16),
             shaped((heads, head_dim, head_dim)),
         ),
@@ -516,7 +522,7 @@
             pltpu.VMEM((hidden_dim, width), BF16),
             pltpu.VMEM((pl.cdiv((CAPACITY + 1) * columns, LANES), devices, LANES), F32),
             pltpu.VMEM((SLOTS * tiles, LANES), F32),
-            pltpu.SemaphoreType.DMA((3, 4)),
+            pltpu.SemaphoreType.DMA((3, 5)),
         ],
         limit=24 * MIB,
     )(

time: 66.3 us -> 66.1 us (level)
  no operation moved by 1% of the time
where the time goes in v7:
time: 66.1 us; the launch traced here: 65.8 us
  blocking collectives  43.4 us (66%)
  Pallas kernels  13.2 us (20%)
  waiting for transfers between devices  3.74 us (6%)
  starting transfers between devices  2.58 us (4%)
  between operations  2.24 us (3%)
    all_to_all x4, blocking collectives, exchange_halves(): lax.all_to_all(halves, 'ep', split_axis=0, concat_axis=0, tiled=True)  43.4 us
    pallas_call x1, Pallas kernels, local(): call(expert_body, (shaped((devices, width), BF16), shaped((1, width))), [...  4.33 us
    pallas_call x1, Pallas kernels, local(): call(functools.partial(window_body, picks), (shaped((CAPACITY + 1, device...  3.79 us
    all_to_all x1, waiting for transfers between devices, exchange_halves(): lax.all_to_all(halves, 'ep', split_axis=0, concat_axis=0, tiled=True)  3.74 us
    pallas_call x1, Pallas kernels, local(): call(cell_body, (shaped((devices, 2, width // 2), BF16), shaped((heads, h...  3.33 us
    all_to_all x1, starting transfers between devices, exchange_halves(): lax.all_to_all(halves, 'ep', split_axis=0, concat_axis=0, tiled=True)  2.58 us
  transfers between devices with their start and end apart: 1, of which 1 were waited for; matrix products, arithmetic and copies ran while one was open for 0% of the time, Pallas kernels for 6%

profile of v7, /device:TPU:0, one launch (start us, length us, event | category | flops | bytes accessed | tf_op | source)
XLA Modules:
  0.0 65.8 jit_solution(6110342396372399791)
XLA Ops:
  1.4 0.0 copy-start.2
  1.4 0.0 copy-start.3
  1.4 0.0 copy-start.6
  1.4 0.0 copy-start.7
  1.5 0.1 shard_map.229
  1.5 15.3 %all_to_all.25 = bf16[32,2,1024]{2,1,0:T(2,128)(2,1)S(1)} all-to-all(bf16[32,2,1024]{2,1,0:T(2,128)(2,1)S(1)} %get-tuple-element.26), channel_id=1, replica_groups=mesh['ep'=32] {'ep'}, dimensions={0} | all-to-all | bytes 262144 | tf_op jit(solution)/shard_map/all_to_all | solution.py:35
  17.0 0.5 shard_map.230
  17.5 0.1 reshape.48
  17.6 9.0 %all_to_all.26 = bf16[32,2,192]{2,1,0:T(2,128)(2,1)S(1)} all-to-all(bf16[32,2,192]{2,1,0:T(2,128)(2,1)S(1)} %reshape.48), channel_id=1, replica_groups=mesh['ep'=32] {'ep'}, dimensions={0} | all-to-all | bytes 49152 | tf_op jit(solution)/shard_map/all_to_all | solution.py:35
  26.6 0.1 reshape.49.parts_ref
  26.7 3.3 %shard_map.231 = (bf16[32,2,1024]{2,1,0:T(2,128)(2,1)}, f32[4,512]{1,0:T(4,128)S(1)}, f32[1,4]{1,0:T(1,128)S(1)}, f32[4,512]{1,0:T(4,128)S(1)}, f32[4,512]{1,0:T...) custom-call(bf16[32,384]{1,0:T(8,128)(2,1)S(1)} %reshape.49.parts_ref, f32[8,32]{1,0:T(8,128)S(1)} %get-tuple-element.29.pre_ref, ...), custom_call_target="tpu_custom_call" | custom-call | flops 2000000000 | bytes 1000000 | tf_op jit(solution)/shard_map/pallas_call | solution.py:462
  30.1 2.6 %all-to-all-start.2 = ((bf16[32,2,1024]{2,1,0:T(2,128)(2,1)}), bf16[32,2,1024]{2,1,0:T(2,128)(2,1)S(1)}, u32[]{:S(2)}, u32[]{:S(2)}) async-start(bf16[32,2,1024]{2,1,0:T(2,128)(2,1)} %get-tuple-element.30), calls=%async_computation.2 | async-start | bytes 262144 | tf_op jit(solution)/shard_map/all_to_all | solution.py:35
  33.3 0.0 copy-start
  33.3 0.0 copy-start.1
  33.3 3.8 %shard_map.232 = (bf16[5,32,32]{2,1,0:T(8,128)(2,1)S(1)}, bf16[8,32]{1,0:T(8,128)(2,1)S(1)}, f32[32,8]{1,0:T(8,128)S(1)}, f32[32,1]{1,0:T(8,128)S(1)}, f32[4,512...) custom-call(f32[1]{0:T(128)S(6)} %copy.31.group_weight, ...), custom_call_target="tpu_custom_call", output_to_operand_aliasing={{7}: (11, {})} | custom-call | flops 10000000 | bytes 1000000 | tf_op jit(solution)/shard_map/pallas_call | solution.py:488
  37.1 3.7 %all-to-all-done.2 = bf16[32,2,1024]{2,1,0:T(2,128)(2,1)S(1)} async-done(((bf16[32,2,1024]{2,1,0:T(2,128)(2,1)}), bf16[32,2,1024]{2,1,0:T(2,128)(2,1)S(1)}, u32[]{:S(2)}, u32[]{:S(2)}) %all-to-all-start.2) | async-done | bytes 131104 | tf_op jit(solution)/shard_map/all_to_all | solution.py:35
  40.9 0.4 shard_map.233
  41.3 0.1 reshape.54
  41.4 9.2 %all_to_all.27 = bf16[32,2,160]{2,1,0:T(2,128)(2,1)S(1)} all-to-all(bf16[32,2,160]{2,1,0:T(2,128)(2,1)S(1)} %reshape.54), channel_id=1, replica_groups=mesh['ep'=32] {'ep'}, dimensions={0} | all-to-all | bytes 40960 | tf_op jit(solution)/shard_map/all_to_all | solution.py:35
  50.6 0.1 reshape.55.in_ref
  50.7 4.3 %shard_map.234 = (bf16[32,2048]{1,0:T(8,128)(2,1)S(1)}, f32[1,2048]{1,0:T(1,128)S(1)}) custom-call(bf16[32,320]{1,0:T(8,128)(2,1)S(1)} %reshape.55.in_ref, bf16[32,2048]{1,0:T(8,128)(2,1)S(1)} %bitcast.24, bf16[8,32]{1,0:T(8,128)(2,1)S(1)} %get-tuple-element.39.mine_ref, f32[32,8]{1,0:T(8,128)S(1)} %get-tuple-element.40.spread_ref, f32[1,2048]{1,0:T(1,128)S(1)} %bitcast.28, ...), custom_call_target="tpu_custom_call" | custom-call | flops 10000000 | bytes 1000000 | tf_op jit(solution)/shard_map/pallas_call | solution.py:515
  55.0 0.1 reshape.58
  55.1 9.9 %all_to_all.28 = bf16[32,2,1024]{2,1,0:T(2,128)(2,1)S(1)} all-to-all(bf16[32,2,1024]{2,1,0:T(2,128)(2,1)S(1)} %reshape.58), channel_id=1, replica_groups=mesh['ep'=32] {'ep'}, dimensions={0} | all-to-all | bytes 262144 | tf_op jit(solution)/shard_map/all_to_all | solution.py:35
  65.1 0.7 %shard_map.235 = bf16[1,2048]{1,0:T(2,128)(2,1)} custom-call(bf16[32,2048]{1,0:T(8,128)(2,1)S(1)} %bitcast.26, f32[32,1]{1,0:T(8,128)S(1)} %get-tuple-element.43.weight_ref, f32[1,2048]{1,0:T(1,128)S(1)} %get-tuple-element.44.middle_ref), custom_call_target="tpu_custom_call" | custom-call | flops 10000000 | bytes 1000000 | tf_op jit(solution)/shard_map/pallas_call | solution.py:534
  (28 shorter events, 0.1 us)
Async XLA Ops:
  0.6 0.7 %copy-start.12 = (f32[1,2]{1,0:T(1,128)S(1)}, f32[1,2]{1,0:T(1,128)}, u32[]{:S(2)}) copy-start(f32[1,2]{1,0:T(1,128)} %member_weight_ref.1) | copy-start | bytes 28
  0.6 0.7 %copy-start.11 = (s32[1,2]{1,0:T(1,128)S(1)}, s32[1,2]{1,0:T(1,128)}, u32[]{:S(2)}) copy-start(s32[1,2]{1,0:T(1,128)} %member_ref.1) | copy-start | bytes 28
  0.7 0.7 %copy-start.8 = (bf16[1,2048]{1,0:T(2,128)(2,1)S(1)}, bf16[1,2048]{1,0:T(2,128)(2,1)}, u32[]{:S(2)}) copy-start(bf16[1,2048]{1,0:T(2,128)(2,1)} %row_ref.1) | copy-start | bytes 12292
  1.4 15.5 %copy-start.2 = (bf16[2048,64]{0,1:T(8,128)(2,1)S(1)}, bf16[2048,64]{0,1:T(8,128)(2,1)}, u32[]{:S(2)}) copy-start(bf16[2048,64]{0,1:T(8,128)(2,1)} %param.23) | copy-start | bytes 786436
  1.4 15.5 %copy-start.3 = (bf16[2048,64]{0,1:T(8,128)(2,1)S(1)}, bf16[2048,64]{0,1:T(8,128)(2,1)}, u32[]{:S(2)}) copy-start(bf16[2048,64]{0,1:T(8,128)(2,1)} %param.24) | copy-start | bytes 786436
  1.4 15.5 %copy-start.4 = (bf16[2048,64]{0,1:T(8,128)(2,1)S(1)}, bf16[2048,64]{0,1:T(8,128)(2,1)}, u32[]{:S(2)}) copy-start(bf16[2048,64]{0,1:T(8,128)(2,1)} %param.25) | copy-start | bytes 786436
  1.4 15.5 %copy-start.5 = (bf16[2048,64]{0,1:T(8,128)(2,1)S(1)}, bf16[2048,64]{0,1:T(8,128)(2,1)}, u32[]{:S(2)}) copy-start(bf16[2048,64]{0,1:T(8,128)(2,1)} %param.26) | copy-start | bytes 786436
  1.4 15.5 %copy-start.6 = (bf16[2048,4]{0,1:T(4,128)(2,1)S(1)}, bf16[2048,4]{0,1:T(4,128)(2,1)}, u32[]{:S(2)}) copy-start(bf16[2048,4]{0,1:T(4,128)(2,1)} %param.27) | copy-start | bytes 49156
  1.4 15.5 %copy-start.7 = (bf16[2048,4]{0,1:T(4,128)(2,1)S(1)}, bf16[2048,4]{0,1:T(4,128)(2,1)}, u32[]{:S(2)}) copy-start(bf16[2048,4]{0,1:T(4,128)(2,1)} %param.28) | copy-start | bytes 49156
  1.4 15.5 %copy-start.9 = (f32[2048]{0:T(1024)S(1)}, f32[2048]{0:T(1024)}, u32[]{:S(2)}) copy-start(f32[2048]{0:T(1024)} %param.22) | copy-start | bytes 24580
  1.5 25.2 %copy-start.10 = (f32[1,4,512]{2,1,0:T(4,128)S(1)}, f32[1,4,512]{2,1,0:T(4,128)}, u32[]{:S(2)}) copy-start(f32[1,4,512]{2,1,0:T(4,128)} %param.31) | copy-start | bytes 24580
  1.5 25.2 %copy-start.13 = (f32[1,4]{1,0:T(1,128)S(1)}, f32[1,4]{1,0:T(1,128)}, u32[]{:S(2)}) copy-start(f32[1,4]{1,0:T(1,128)} %max_ref.1) | copy-start | bytes 52
  1.5 25.2 %copy-start.14 = (f32[4]{0:T(128)S(1)}, f32[4]{0:T(128)}, u32[]{:S(2)}) copy-start(f32[4]{0:T(128)} %param.29) | copy-start | bytes 52
  30.1 10.8 %all-to-all-start.2 = ((bf16[32,2,1024]{2,1,0:T(2,128)(2,1)}), bf16[32,2,1024]{2,1,0:T(2,128)(2,1)S(1)}, u32[]{:S(2)}, u32[]{:S(2)}) async-start(bf16[32,2,1024]{2,1,0:T(2,128)(2,1)} %get-tuple-element.30), calls=%async_computation.2 | async-start | bytes 262144 | tf_op jit(solution)/shard_map/all_to_all | solution.py:35
  33.3 7.6 %copy-start = (bf16[2048,64]{0,1:T(8,128)(2,1)S(1)}, bf16[2048,64]{0,1:T(8,128)(2,1)}, u32[]{:S(2)}) copy-start(bf16[2048,64]{0,1:T(8,128)(2,1)} %param.33) | copy-start | bytes 786436
  33.3 17.4 %copy-start.1 = (f32[2048]{0:T(1024)S(1)}, f32[2048]{0:T(1024)}, u32[]{:S(2)}) copy-start(f32[2048]{0:T(1024)} %param.34) | copy-start | bytes 24580
